TPU v7x, 128 devices: a whole 4x4x4 slice. The times are simulated.
128 devices in a mesh: kv: 16 (over z, y), tp: 8 (over x, core).
Axes of the slice: x: 4, y: 4, z: 4, core: 2. Of those that a mesh axis runs over, the one named last changes fastest.
Arguments:
- tokens: bfloat16 [256, 4096], P(None, ('kv', 'tp')), may hold values from -64 to 64
- mix_gain: float32 [4096], P('kv'), may hold values from 0.1 to 1.9
- w_query: bfloat16 [4096, 3072], P('kv', 'tp'), may hold values from -0.09375 to 0.09375
- w_key: bfloat16 [4096, 3072], P('kv', 'tp'), may hold values from -0.09375 to 0.09375
- w_value: bfloat16 [4096, 3072], P('kv', 'tp'), may hold values from -0.09375 to 0.09375
- w_gate: bfloat16 [4096, 3072], P('kv', 'tp'), may hold values from -0.09375 to 0.09375
- w_beta: bfloat16 [4096, 24], P('kv'), may hold values from -0.09375 to 0.09375
- w_decay: bfloat16 [4096, 24], P('kv'), may hold values from -0.09375 to 0.09375
- decay_rate: float32 [24], P('tp'), may hold values from 0.15 to 1.5
- out_gain: float32 [128], replicated, may hold values from 0.1 to 1.9
- state: float32 [256, 24, 128, 128], P('kv', 'tp'), may hold values from -0.6 to 0.6
- w_out: bfloat16 [3072, 4096], P('tp', 'kv'), may hold values from -0.109375 to 0.109375
- mlp_gain: float32 [4096], replicated, may hold values from 0.1 to 1.9
- w_up: bfloat16 [4096, 16384], P(None, ('kv', 'tp')), may hold values from -0.09375 to 0.09375
- w_down: bfloat16 [16384, 4096], P(('kv', 'tp')), may hold values from -0.1875 to 0.1875
Outputs:
- mixed: bfloat16 [256, 4096], P(None, ('kv', 'tp'))
- new_state: float32 [256, 24, 128, 128], P('kv', 'tp')
All inputs are finite; a program needn't handle non-finite values.
Results may differ from a plain program's by a relative error of at most 0.0063.
Values may be sent and summed in bfloat16 or wider, within the bound.
A program may use at most 64 MiB of HBM per device.

v0:
```python
import math

import jax
import jax.numpy as jnp
from jax import lax
from jax.sharding import Mesh
from jax.sharding import PartitionSpec as P

D = 4096
TP = ("tp_0", "tp_1")
KV = ("kv_0", "kv_1")
KV_TP = ("kv_0", "kv_1", "tp_0", "tp_1")


EPSILON = 1e-06


def side_by_side(arrays, axis, dim, along):
    widths = [math.prod(a.shape[along:]) for a in arrays]
    both = jnp.concatenate(
        [a.reshape(*a.shape[:along], w) for a, w in zip(arrays, widths)], axis=along
    )
    filled = lax.psum_scatter(both, axis, scatter_dimension=dim, tiled=True)
    pieces = jnp.split(filled, [sum(widths[:k]) for k in range(1, len(widths))], axis=along)
    return tuple(
        (b.reshape(*filled.shape[:along], *a.shape[along:]) for a, b in zip(arrays, pieces))
    )


def in_blocks(value, dim, count):
    shape = value.shape
    pieces = value.reshape(*shape[:dim], count, shape[dim] // count, *shape[dim + 1 :])
    return jnp.moveaxis(pieces, dim, 0)


def summed_on_arrival(value, axis, dim):
    count = lax.axis_size(axis)
    pieces = lax.all_to_all(in_blocks(value, dim, count), axis, 0, 0, tiled=True)
    return jnp.sum(pieces, axis=0)


def joined_along(pieces, dim):
    shape = list(pieces.shape[1:])
    shape[dim] *= pieces.shape[0]
    return jnp.moveaxis(pieces, 0, dim).reshape(shape)


def exchange_in_order(pieces, axes, sequence):
    inside = pieces.shape[1:]
    filled = pieces.reshape(*(lax.axis_size(a) for a in axes), *inside)
    for k in sequence:
        filled = lax.all_to_all(filled, axes[k], k, k, tiled=True)
    return filled.reshape(-1, *inside)


def exchange_by_chip(value, groups, sequence, split_dim, concat_dim):
    count = lax.axis_size(groups[0]) * lax.axis_size(groups[1])
    pieces = in_blocks(value, split_dim, count)
    return joined_along(exchange_in_order(pieces, groups, sequence), concat_dim)


def head_norm(values):
    return values * lax.rsqrt(jnp.sum(values * values, axis=-1, keepdims=True) + EPSILON)


def feed_forward(segment, mlp_gain, w_up, w_down):
    segment_f = segment.astype(jnp.float32)
    normed_mlp = (
        segment_f
        * lax.rsqrt(jnp.mean(segment_f * segment_f, axis=1, keepdims=True) + EPSILON)
        * mlp_gain[None, :]
    ).astype(jnp.bfloat16)
    hidden = jnp.square(
        jax.nn.relu(jnp.dot(normed_mlp, w_up, preferred_element_type=jnp.float32))
    ).astype(jnp.bfloat16)
    return jnp.dot(hidden, w_down, preferred_element_type=jnp.float32)


def local(
    tokens,
    mix_gain,
    w_query,
    w_key,
    w_value,
    w_gate,
    w_beta,
    w_decay,
    decay_rate,
    out_gain,
    state,
    w_out,
    mlp_gain,
    w_up,
    w_down,
):
    local_rows = state.shape[0]
    local_heads = decay_rate.shape[0]
    head_size = state.shape[2]
    all_heads = w_beta.shape[1]
    columns = lax.all_gather(tokens, TP, axis=1, tiled=True)
    columns_f = columns.astype(jnp.float32)
    normed = (columns_f * mix_gain[None, :]).astype(jnp.bfloat16)
    part_query = jnp.dot(normed, w_query, preferred_element_type=jnp.float32)
    part_key = jnp.dot(normed, w_key, preferred_element_type=jnp.float32)
    part_value = jnp.dot(normed, w_value, preferred_element_type=jnp.float32)
    part_gate = jnp.dot(normed, w_gate, preferred_element_type=jnp.float32)
    part_rates = jnp.dot(
        normed, jnp.concatenate([w_beta, w_decay], axis=1), preferred_element_type=jnp.float32
    )
    summed = side_by_side(
        (
            part_query,
            part_key,
            part_value,
            part_gate,
            part_rates,
            jnp.sum(columns_f * columns_f, axis=1),
        ),
        KV,
        0,
        1,
    )
    own_squares = summed[5]
    row_scale = lax.rsqrt(own_squares / D + EPSILON)[:, None]
    shape_heads = (local_rows, local_heads, head_size)
    query = head_norm(jax.nn.silu((summed[0] * row_scale).reshape(shape_heads))) * head_size ** (
        -0.5
    )
    key = head_norm(jax.nn.silu((summed[1] * row_scale).reshape(shape_heads)))
    value = jax.nn.silu((summed[2] * row_scale).reshape(shape_heads))
    gate_raw = (summed[3] * row_scale).reshape(shape_heads)
    rates = summed[4] * row_scale
    head_start = lax.axis_index(TP) * local_heads
    beta = jax.nn.sigmoid(lax.dynamic_slice_in_dim(rates, head_start, local_heads, 1))
    decay_raw = lax.dynamic_slice_in_dim(rates, all_heads + head_start, local_heads, 1)
    decay = jnp.exp(-decay_rate[None, :] * jax.nn.softplus(decay_raw))
    faded = state * decay[:, :, None, None]
    recalled = jnp.einsum("bhkv,bhk->bhv", faded, key, precision=lax.Precision.HIGHEST)
    change = beta[:, :, None] * (value - recalled)
    new_state = faded + key[:, :, :, None] * change[:, :, None, :]
    readout = jnp.einsum("bhkv,bhk->bhv", new_state, query, precision=lax.Precision.HIGHEST)
    scaled = (
        readout
        * lax.rsqrt(jnp.mean(readout * readout, axis=-1, keepdims=True) + EPSILON)
        * out_gain
    )
    merged = (
        (scaled * jax.nn.silu(gate_raw))
        .reshape(local_rows, local_heads * head_size)
        .astype(jnp.bfloat16)
    )
    partial_out = jnp.dot(
        lax.all_gather(merged, KV, axis=0, tiled=True), w_out, preferred_element_type=jnp.float32
    )
    branch_sum = summed_on_arrival(partial_out, TP, 1)
    residual = (tokens.astype(jnp.float32) + branch_sum).astype(jnp.bfloat16)
    whole_rows = lax.all_gather(residual, KV_TP, axis=1, tiled=True)
    partial_mlp = feed_forward(whole_rows, mlp_gain, w_up, w_down)
    row_branch = lax.psum_scatter(partial_mlp, KV_TP, scatter_dimension=0, tiled=True)
    own_count = row_branch.shape[0]
    own_rows = lax.dynamic_slice_in_dim(whole_rows, lax.axis_index(KV_TP) * own_count, own_count, 0)
    finished = (own_rows.astype(jnp.float32) + row_branch).astype(jnp.bfloat16)
    mixed = exchange_by_chip(finished, (("kv_0", "kv_1", "tp_0"), "tp_1"), (1, 0), 1, 0)
    return (mixed, new_state)


def solution(mesh):
    torus = Mesh(mesh.devices.reshape(4, 4, 4, 2), ("kv_0", "kv_1", "tp_0", "tp_1"))
    in_specs = (
        P(None, KV_TP),
        P(KV),
        P(KV, TP),
        P(KV, TP),
        P(KV, TP),
        P(KV, TP),
        P(KV, None),
        P(KV, None),
        P(TP),
        P(),
        P(KV, TP, None, None),
        P(TP, KV),
        P(),
        P(None, KV_TP),
        P(KV_TP, None),
    )
    out_specs = (P(None, KV_TP), P(KV, TP, None, None))
    return jax.shard_map(local, mesh=torus, in_specs=in_specs, out_specs=out_specs, check_vma=False)
```

profile of v0, /device:TPU:1, one launch (start us, length us, event | category | flops | bytes accessed | tf_op | source)
XLA Modules:
  0.0 419.2 jit_solution(876211718287899662)
XLA Ops:
  7.3 14.8 %all_gather.9 = bf16[256,256]{0,1:T(8,128)(2,1)S(1)} all-gather(bf16[256,32]{0,1:T(8,128)(2,1)} %param.15), channel_id=1, replica_groups=mesh['kv_0'=4,'kv_1'=4,'tp_0'=4,'tp_1'=2] {'tp_0','tp_1'}, dimensions={1}, use_global_device_ids=true | all-gather | bytes 147456 | tf_op jit(solution)/shard_map/all_gather | solution.py:100
  22.0 0.1 fusion.23
  22.1 0.1 copy.42
  22.2 1.3 fusion.51
  23.5 1.3 fusion.49
  24.8 1.3 fusion.47
  26.1 1.3 fusion.53
  27.4 0.3 fusion.32
  27.7 1.4 concatenate.7
  29.2 0.0 all-gather.2.cloned.1.call-start
  29.3 0.6 dynamic-slice
  30.5 87.5 %all-reduce.5.cloned.1.call-done = f32[256,1585]{1,0:T(8,128)} async-done(((f32[256,1585]{1,0:T(8,128)}), f32[256,1585]{1,0:T(8,128)}) %all-reduce.5.cloned.1.call-update) | async-done | bytes 1623056
  118.0 0.9 fusion.43
  118.9 0.9 dynamic-slice_multiply_fusion.1
  119.9 0.1 multiply_reduce_fusion.1
  120.0 0.1 fusion.65
  120.1 0.1 broadcast_multiply_fusion
  120.2 0.1 multiply_reduce_fusion
  120.3 0.1 multiply_bitcast_fusion
  120.5 0.9 dynamic-slice_multiply_fusion.5
  121.4 0.1 add_divide_fusion
  121.5 4.8 %fusion.3 = f32[16,3,1,128]{3,2,1,0:T(1,128)S(1)} fusion(f32[16,3,128,128]{3,2,1,0:T(8,128)} %param.25, f32[16,3]{1,0:T(8,128)S(1)} %get-tuple-element.15, f32[16,3,128,1]{2,1,0,3:T(4,128)S(1)} %fusion.65), kind=kOutput, calls=%fused_computation.6 | convolution fusion | flops 10223616 | bytes 3195072 | tf_op jit(solution)/shard_map/bhkv,bhk->bhv/dot_general | solution.py:138
  126.3 0.1 fusion.30
  126.4 1.1 multiply_add_fusion
  127.5 1.7 copy-done.3
  129.2 2.8 fusion.36
  132.0 0.1 fusion.28
  132.1 0.1 fusion.31
  132.2 16.8 %all_gather.10 = bf16[256,384]{1,0:T(8,128)(2,1)S(1)} all-gather(bf16[16,384]{1,0:T(8,128)(2,1)S(1)} %bitcast.49), channel_id=1, replica_groups=mesh['kv_0'=4,'kv_1'=4,'tp_0'=4,'tp_1'=2] {'kv_0','kv_1'}, dimensions={0}, use_global_device_ids=true | all-gather | bytes 208896 | tf_op jit(solution)/shard_map/all_gather | solution.py:153
  149.0 0.3 fusion.55
  149.3 19.1 %all_to_all.15 = f32[8,256,32]{1,2,0:T(8,128)S(1)} all-to-all(f32[8,256,32]{1,2,0:T(8,128)S(1)} %bitcast.43), channel_id=1, replica_groups=mesh['kv_0'=4,'kv_1'=4,'tp_0'=4,'tp_1'=2] {'tp_0','tp_1'}, dimensions={0} | all-to-all | bytes 524288 | tf_op jit(solution)/shard_map/all_to_all | solution.py:38
  168.4 0.6 add_convert_fusion
  169.0 0.2 all-reduce.7.cloned.1.call-start
  169.2 62.7 %all-gather.2.cloned.1.call-done = bf16[256,4096]{0,1:T(8,128)(2,1)} async-done(((bf16[256,32]{0,1:T(8,128)(2,1)}), bf16[256,4096]{0,1:T(8,128)(2,1)}) %all-gather.2.cloned.1.call-update) | async-done | bytes 2097168 | tf_op jit(solution)/shard_map/all_gather | solution.py:157
  231.9 2.3 fusion
  234.3 5.3 %fusion.20 = f32[256,4096]{1,0:T(8,128)} fusion(bf16[128,4096]{1,0:T(8,128)(2,1)S(1)} %copy-done, bf16[4096,128]{1,0:T(8,128)(2,1)} %param.28, bf16[256,4096]{0,1:T(8,128)(2,1)S(1)} %copy-done.1, f32[4096]{0:T(1024)S(1)} %copy-done.7, f32[256]{0:T(256)S(1)} %add_rsqrt_fusion.3), kind=kOutput, calls=%fused_computation.15 | convolution fusion | flops 541163520 | bytes 8406016 | tf_op jit(solution)/shard_map/dot_general | solution.py:76
  239.6 1.4 constant_dynamic-slice_fusion
  241.1 1.6 copy.52
  242.7 148.4 %all-reduce.7.cloned.1.call-done = f32[256,4096]{1,0:T(8,128)} async-done(((f32[256,4096]{1,0:T(8,128)}), f32[256,4096]{1,0:T(8,128)}) %all-reduce.7.cloned.1.call-update) | async-done | bytes 4194320
  391.1 0.9 fusion.27
  392.0 0.1 reshape.86
  392.1 0.1 copy.44
  392.2 0.1 reshape.94
  392.3 4.1 all_to_all.16
  396.5 0.1 reshape.95
  396.6 0.1 copy.45
  396.7 15.2 %all_to_all.17 = bf16[64,2,2,32]{3,2,1,0:T(2,128)(2,1)S(1)} all-to-all(bf16[64,2,2,32]{3,2,1,0:T(2,128)(2,1)S(1)} %copy.45), channel_id=1, replica_groups=mesh['kv_0'=4,'kv_1'=4,'tp_0'=4,'tp_1'=2] {'kv_0','kv_1','tp_0'}, dimensions={0} | all-to-all | bytes 32768 | tf_op jit(solution)/shard_map/all_to_all | solution.py:52
  411.9 0.7 copy.46
  (40 shorter events, 0.3 us)
Async XLA Ops:
  7.2 227.1 %copy-start = (bf16[128,4096]{1,0:T(8,128)(2,1)S(1)}, bf16[128,4096]{1,0:T(8,128)(2,1)}, u32[]{:S(2)}) copy-start(bf16[128,4096]{1,0:T(8,128)(2,1)} %param.29) | copy-start | bytes 3145732
  7.2 20.2 %copy-start.6 = (f32[256]{0:T(256)S(1)}, f32[256]{0:T(256)}, u32[]{:S(2)}) copy-start(f32[256]{0:T(256)} %param.16) | copy-start | bytes 3076
  7.2 20.2 %copy-start.8 = (bf16[256,24]{0,1:T(8,128)(2,1)S(1)}, bf16[256,24]{0,1:T(8,128)(2,1)}, u32[]{:S(2)}) copy-start(bf16[256,24]{0,1:T(8,128)(2,1)} %param.22) | copy-start | bytes 36868
  7.2 20.2 %copy-start.9 = (bf16[256,24]{0,1:T(8,128)(2,1)S(1)}, bf16[256,24]{0,1:T(8,128)(2,1)}, u32[]{:S(2)}) copy-start(bf16[256,24]{0,1:T(8,128)(2,1)} %param.21) | copy-start | bytes 36868
  7.2 110.8 %all-reduce.5.cloned.1.call-start = ((), (), s32[]{:S(2)}) async-start(), calls=%async_computation.4 | async-start | bytes 3407872
  26.1 3.2 copy-start.11
  26.1 3.2 copy-start.12
  29.2 202.7 %all-gather.2.cloned.1.call-start = ((), (), s32[]{:S(2)}) async-start(), calls=%async_computation.3 | async-start | bytes 2113536 | tf_op jit(solution)/shard_map/all_gather | solution.py:157
  120.5 5.9 %copy-start.2 = (f32[16,3,128,128]{3,2,1,0:T(8,128)S(1)}, f32[16,3,128,128]{3,2,1,0:T(8,128)}, u32[]{:S(2)}) copy-start(f32[16,3,128,128]{3,2,1,0:T(8,128)} %param.25) | copy-start | bytes 9437188
  127.5 1.7 copy-start.3
  129.2 2.9 copy-start.10
  129.2 19.8 %copy-start.4 = (bf16[384,256]{1,0:T(8,128)(2,1)S(1)}, bf16[384,256]{1,0:T(8,128)(2,1)}, u32[]{:S(2)}) copy-start(bf16[384,256]{1,0:T(8,128)(2,1)} %param.26) | copy-start | bytes 589828
  129.2 39.2 %copy-start.5 = (bf16[256,32]{0,1:T(8,128)(2,1)S(1)}, bf16[256,32]{0,1:T(8,128)(2,1)}, u32[]{:S(2)}) copy-start(bf16[256,32]{0,1:T(8,128)(2,1)} %param.15) | copy-start | bytes 49156
  129.2 105.1 %copy-start.7 = (f32[4096]{0:T(1024)S(1)}, f32[4096]{0:T(1024)}, u32[]{:S(2)}) copy-start(f32[4096]{0:T(1024)} %param.27) | copy-start | bytes 49156
  169.0 222.1 %all-reduce.7.cloned.1.call-start = ((), (), s32[]{:S(2)}) async-start(), calls=%async_computation.5 | async-start | bytes 8388608
  231.9 2.3 copy-start.1
Sparse Core Ops, SparseCore 0:
  29.3 88.6 all-reduce.4
  169.1 62.7 all-gather.1
  239.7 151.3 all-reduce.6
where the time goes:
time: 420 us; the launch traced here: 419 us
  waiting for transfers between devices  299 us (71%)
  blocking collectives  70 us (17%)
  matrix products  18.6 us (4%)
  between operations  14.8 us (4%)
  other arithmetic  8.67 us (2%)
  local copies, waits for them, and re-layouts  8.14 us (2%)
    unnamed x5, waiting for transfers between devices  236 us
    all_gather x1, waiting for transfers between devices, local(): whole_rows = lax.all_gather(residual, KV_TP, axis=1, tiled=True)  62.7 us
    all_to_all x2, blocking collectives, exchange_in_order(): filled = lax.all_to_all(filled, axes[k], k, k, tiled=True)  19.4 us
    all_to_all x1, blocking collectives, summed_on_arrival(): lax.all_to_all(in_blocks(value, dim, count), axis, 0, 0, tiled=True)  19.1 us
    all_gather x1, blocking collectives, local(): lax.all_gather(merged, KV, axis=0, tiled=True)  16.8 us
    all_gather x1, blocking collectives, local(): columns = lax.all_gather(tokens, TP, axis=1, tiled=True)  14.8 us
  transfers between devices with their start and end apart: 3, of which 3 were waited for; matrix products, arithmetic and copies ran while one was open for 1% of the time, Pallas kernels for 0%

commit v1 on v0

v1 whole, which is shorter than its diff:
```python
import functools
import math

import jax
import jax.numpy as jnp
from jax import lax
from jax.experimental import pallas as pl
from jax.experimental.pallas import tpu as pltpu
from jax.sharding import Mesh
from jax.sharding import PartitionSpec as P

EPSILON = 1e-06
MESH = pl.DeviceIdType.MESH
KV_TP = ("kv_0", "kv_1", "tp_0", "tp_1")
KV = ("kv_0", "kv_1")
TP = ("tp_0", "tp_1")
F32 = jnp.float32
BF16 = jnp.bfloat16


def silu(v):
    return v / (1.0 + jnp.exp(-v))


def layer_kernel(
    sizes,
    tok_ref,
    mix_gain_ref,
    wq_ref,
    wk_ref,
    wv_ref,
    wg_ref,
    wbeta_ref,
    wdecay_ref,
    rate_ref,
    out_gain_ref,
    state_ref,
    wout_ref,
    mlp_gain_ref,
    wup_ref,
    wdown_ref,
    mixed_ref,
    new_state_ref,
    col_t,
    w_proj,
    w_rates,
    w_out,
    w_up,
    w_down,
    st,
    col_n,
    send_b,
    recv_b,
    key_t,
    query_t,
    rows_s,
    readout_s,
    gate_s,
    merged,
    send_e,
    own_e,
    recv_e,
    res,
    res_t,
    hid,
    acc_up,
    send_d,
    recv_d,
    send_h,
    recv_h1a,
    recv_h1b,
    send_h2a,
    send_h2b,
    recv_h2a,
    recv_h2b,
    send_x,
    recv_x,
    local_sem,
    a_send,
    a_recv,
    b_send,
    b_recv,
    d_send,
    d_recv,
    e_send,
    e_recv,
    f1_send,
    f1_recv,
    fa_send,
    fb_send,
    fa_recv,
    fb_recv,
    fp_send,
    fp_recv,
    hd_send,
    hd_recv,
    h1a_send,
    h1b_send,
    h1a_recv,
    h1b_recv,
    h2_send,
    h2a_recv,
    h2b_recv,
    x_send,
    x_recv,
):
    nz, ny, nx, nc = sizes
    nkv, ntp = nz * ny, nx * nc
    z, y = lax.axis_index("kv_0"), lax.axis_index("kv_1")
    x, c = lax.axis_index("tp_0"), lax.axis_index("tp_1")
    kv, tp = z * ny + y, x * nc + c
    partner = {"tp_1": nc - 1 - c}

    dt, rows = tok_ref.shape
    dk = dt * ntp
    width = dk * nkv
    rb, heads, head = st.shape[0], st.shape[1], st.shape[2]
    proj = heads * head
    rt = rows // ntp
    rh = rows // nc
    rc = rh // 2

    def kv_dev(k):
        return {"kv_0": k // ny, "kv_1": lax.rem(k, ny)}

    def tp_dev(t):
        return {"tp_0": t // nc, "tp_1": lax.rem(t, nc)}

    def remote(src, dst, send_sem, recv_sem, dev):
        return pltpu.make_async_remote_copy(
            src_ref=src,
            dst_ref=dst,
            send_sem=send_sem,
            recv_sem=recv_sem,
            device_id=dev,
            device_id_type=MESH,
        )

    def loop(lo, hi, body):
        def wrapped(i, carry):
            body(i)
            return carry

        lax.fori_loop(lo, hi, wrapped, 0)

    def block(i, n):
        return pl.ds(pl.multiple_of(i * n, n), n)

    own_tok = col_t.at[block(tp, dt), :]
    tok_copy = pltpu.make_async_copy(tok_ref, own_tok, local_sem.at[0])
    tok_copy.start()
    proj_copies = [
        pltpu.make_async_copy(w, w_proj.at[i], local_sem.at[1 + i])
        for i, w in enumerate((wq_ref, wk_ref, wv_ref, wg_ref))
    ]
    for copy in proj_copies:
        copy.start()
    later_copies = [
        pltpu.make_async_copy(state_ref, st, local_sem.at[5]),
        pltpu.make_async_copy(wout_ref, w_out, local_sem.at[6]),
        pltpu.make_async_copy(wup_ref, w_up, local_sem.at[7]),
        pltpu.make_async_copy(wdown_ref, w_down, local_sem.at[8]),
    ]
    for copy in later_copies:
        copy.start()

    barrier = pltpu.get_barrier_semaphore()

    def greet_kv(d):
        k = lax.rem(kv + d, nkv)
        pl.semaphore_signal(barrier, inc=1, device_id=kv_dev(k), device_id_type=MESH)

    def greet_tp(d):
        t = lax.rem(tp + d, ntp)
        pl.semaphore_signal(barrier, inc=1, device_id=tp_dev(t), device_id_type=MESH)

    loop(1, nkv, greet_kv)
    loop(1, ntp, greet_tp)

    n_heads = wbeta_ref.shape[0]
    w_rates[...] = jnp.zeros_like(w_rates)
    w_rates[0:n_heads, :] = wbeta_ref[...]
    w_rates[32 : 32 + n_heads, :] = wdecay_ref[...]

    tok_copy.wait()
    pl.semaphore_wait(barrier, nkv - 1 + ntp - 1)

    def a_copy(d, src_tp, peer):
        blk = col_t.at[block(src_tp, dt), :]
        return remote(blk, blk, a_send.at[d], a_recv.at[src_tp], tp_dev(peer))

    loop(1, ntp, lambda d: a_copy(d, tp, lax.rem(tp + d, ntp)).start())

    def a_wait(d):
        src = lax.rem(tp + ntp - d, ntp)
        a_copy(d, src, src).wait_recv()

    loop(1, ntp, a_wait)

    cols = col_t[...].astype(F32).T
    col_n[...] = cols.astype(BF16)
    normed = (cols * mix_gain_ref[...]).astype(BF16)
    squares = jnp.sum(cols * cols, axis=1, keepdims=True)
    contract_last = (((1,), (1,)), ((), ()))
    rates_part = lax.dot_general(
        normed, w_rates[...], contract_last, preferred_element_type=F32
    )
    lane = lax.broadcasted_iota(jnp.int32, rates_part.shape, 1)
    rates_part = jnp.where(lane == 127, squares, rates_part)
    high = rates_part.astype(BF16)
    send_b[:, 4 * proj : 4 * proj + 128] = high
    send_b[:, 4 * proj + 128 :] = (rates_part - high.astype(F32)).astype(BF16)
    for i in range(4):
        proj_copies[i].wait()
        part = jnp.dot(normed, w_proj[i], preferred_element_type=F32)
        send_b[:, i * proj : (i + 1) * proj] = part.astype(BF16)

    def b_copy(d, dest_kv, src_kv, peer):
        return remote(
            send_b.at[block(dest_kv, rb), :],
            recv_b.at[src_kv],
            b_send.at[d],
            b_recv.at[src_kv],
            kv_dev(peer),
        )

    def b_start(d):
        peer = lax.rem(kv + d, nkv)
        b_copy(d, peer, kv, peer).start()

    loop(1, nkv, b_start)

    def b_add(d, acc):
        src = lax.rem(kv + nkv - d, nkv)
        b_copy(d, kv, src, src).wait_recv()
        return acc + recv_b[src].astype(F32)

    summed = lax.fori_loop(1, nkv, b_add, send_b[block(kv, rb), :].astype(F32))

    rates = summed[:, 4 * proj : 4 * proj + 128] + summed[:, 4 * proj + 128 :]
    lane_b = lax.broadcasted_iota(jnp.int32, rates.shape, 1)

    def pick(i):
        return jnp.sum(jnp.where(lane_b == i, rates, 0.0), axis=1, keepdims=True)

    row_scale = lax.rsqrt(pick(127) / width + EPSILON)
    repeat = 128 // rb
    for h in range(heads):
        at = slice(h * head, (h + 1) * head)
        beta_raw = pick(tp * heads + h) * row_scale
        decay_raw = pick(32 + tp * heads + h) * row_scale
        beta = 1.0 / (1.0 + jnp.exp(-beta_raw))
        softplus = jnp.maximum(decay_raw, 0.0) + jnp.log1p(jnp.exp(-jnp.abs(decay_raw)))
        decay = jnp.exp(-rate_ref[0, h] * softplus)
        query = silu(summed[:, 0 * proj : 1 * proj][:, at] * row_scale)
        query = query * lax.rsqrt(jnp.sum(query * query, axis=1, keepdims=True) + EPSILON)
        query = query * head ** (-0.5)
        key = silu(summed[:, 1 * proj : 2 * proj][:, at] * row_scale)
        key = key * lax.rsqrt(jnp.sum(key * key, axis=1, keepdims=True) + EPSILON)
        value = silu(summed[:, 2 * proj : 3 * proj][:, at] * row_scale)
        gate = summed[:, 3 * proj : 4 * proj][:, at] * row_scale
        key_t[h] = jnp.concatenate([key] * repeat, axis=0).T
        query_t[h] = jnp.concatenate([query] * repeat, axis=0).T
        shape = (rb, head)
        rows_s[0, h] = jnp.broadcast_to(decay, shape)
        rows_s[1, h] = jnp.broadcast_to(beta, shape)
        rows_s[2, h] = value
        rows_s[3, h] = jnp.broadcast_to(
            jnp.sum(key * query, axis=1, keepdims=True), shape
        )
        gate_s[:, at] = silu(gate)

    later_copies[0].wait()

    def delta(b):
        shift = lax.rem(128 - b, 128)
        for h in range(heads):
            state = st[b, h]
            key_b = pltpu.roll(key_t[h], shift, 1)[:, 0:1]
            query_b = pltpu.roll(query_t[h], shift, 1)[:, 0:1]
            decay = rows_s[0, h, pl.ds(b, 1), :]
            beta = rows_s[1, h, pl.ds(b, 1), :]
            value = rows_s[2, h, pl.ds(b, 1), :]
            key_query = rows_s[3, h, pl.ds(b, 1), :]
            recalled = decay * jnp.sum(state * key_b, axis=0, keepdims=True)
            change = beta * (value - recalled)
            old_read = decay * jnp.sum(state * query_b, axis=0, keepdims=True)
            readout_s[h, pl.ds(b, 1), :] = old_read + key_query * change
            st[b, h] = decay * state + key_b * change

    loop(0, rb, delta)
    state_out = pltpu.make_async_copy(st, new_state_ref, local_sem.at[9])
    state_out.start()

    own_rows = block(kv, rb)
    for h in range(heads):
        at = slice(h * head, (h + 1) * head)
        read = readout_s[h]
        scale = lax.rsqrt(jnp.sum(read * read, axis=1, keepdims=True) / head + EPSILON)
        merged[own_rows, at] = (read * scale * out_gain_ref[...] * gate_s[:, at]).astype(BF16)

    def d_copy(d, src_kv, peer):
        blk = merged.at[block(src_kv, rb), :]
        return remote(blk, blk, d_send.at[d], d_recv.at[src_kv], kv_dev(peer))

    loop(1, nkv, lambda d: d_copy(d, kv, lax.rem(kv + d, nkv)).start())

    def d_wait(d):
        src = lax.rem(kv + nkv - d, nkv)
        d_copy(d, src, src).wait_recv()

    later_copies[1].wait()
    loop(1, nkv, d_wait)

    part = jnp.dot(merged[...], w_out[...], preferred_element_type=F32)
    own_e[...] = part
    send_e[...] = part.astype(BF16)

    def e_copy(d, dest_tp, src_tp, peer):
        return remote(
            send_e.at[block(dest_tp, rt), :],
            recv_e.at[src_tp],
            e_send.at[d],
            e_recv.at[src_tp],
            tp_dev(peer),
        )

    def e_start(d):
        peer = lax.rem(tp + d, ntp)
        e_copy(d, peer, tp, peer).start()

    loop(1, ntp, e_start)

    def e_add(d, acc):
        src = lax.rem(tp + ntp - d, ntp)
        e_copy(d, tp, src, src).wait_recv()
        return acc + recv_e[src].astype(F32)

    my_rows = block(tp, rt)
    branch = lax.fori_loop(1, ntp, e_add, own_e[my_rows, :])
    res[kv, my_rows, :] = (col_n[my_rows, :].astype(F32) + branch).astype(BF16)

    def f1_copy(d, src_tp, peer):
        blk = res.at[kv, block(src_tp, rt), :]
        return remote(blk, blk, f1_send.at[d], f1_recv.at[src_tp], tp_dev(peer))

    loop(1, ntp, lambda d: f1_copy(d, tp, lax.rem(tp + d, ntp)).start())

    def f1_wait(d):
        src = lax.rem(tp + ntp - d, ntp)
        f1_copy(d, src, src).wait_recv()

    loop(1, ntp, f1_wait)

    rows_a = pl.ds(pl.multiple_of(c * rh, rc), rc)
    rows_b = pl.ds(pl.multiple_of(c * rh + rc, rc), rc)
    other = nc - 1 - c
    other_a = pl.ds(pl.multiple_of(other * rh, rc), rc)
    other_b = pl.ds(pl.multiple_of(other * rh + rc, rc), rc)

    def fa_copy(k, slot, dev):
        blk = res.at[k, rows_a, :]
        return remote(blk, blk, fa_send.at[slot], fa_recv.at[k], dev)

    def fb_copy(k, slot, dev):
        blk = res.at[k, rows_b, :]
        return remote(blk, blk, fb_send.at[slot], fb_recv.at[k], dev)

    def y_dev(d):
        return {"kv_1": lax.rem(y + d, ny)}

    def z_dev(d):
        return {"kv_0": lax.rem(z + d, nz)}

    def fp_copy(k, half, at):
        blk = res.at[k, at, :]
        return remote(blk, blk, fp_send.at[half, k], fp_recv.at[half, k], partner)

    for d in range(1, ny):
        fa_copy(kv, d - 1, y_dev(d)).start()
    for d in range(1, nz):
        fb_copy(kv, d - 1, z_dev(d)).start()
    a_base, b_base = ny - 1, nz - 1
    for d in range(1, nz):
        fa_copy(kv, a_base + d - 1, z_dev(d)).start()
    for d in range(1, ny):
        fb_copy(kv, b_base + d - 1, y_dev(d)).start()

    res_t[...] = res[kv].astype(F32).T

    for i in range(1, max(ny, nz)):
        if i < ny:
            k = z * ny + lax.rem(y + ny - i, ny)
            fa_copy(k, 0, partner).wait_recv()
            for d in range(1, nz):
                fa_copy(k, a_base + i * (nz - 1) + d - 1, z_dev(d)).start()
            fp_copy(k, 0, rows_a).start()
        if i < nz:
            k = lax.rem(z + nz - i, nz) * ny + y
            fb_copy(k, 0, partner).wait_recv()
            for d in range(1, ny):
                fb_copy(k, b_base + i * (ny - 1) + d - 1, y_dev(d)).start()
            fp_copy(k, 1, rows_b).start()

    def fa_late(i):
        zd, yd = 1 + lax.rem(i, nz - 1), i // (nz - 1)
        k = lax.rem(z + nz - zd, nz) * ny + lax.rem(y + ny - yd, ny)
        fa_copy(k, 0, partner).wait_recv()
        fp_copy(k, 0, rows_a).start()

    def fb_late(i):
        yd, zd = 1 + lax.rem(i, ny - 1), i // (ny - 1)
        k = lax.rem(z + nz - zd, nz) * ny + lax.rem(y + ny - yd, ny)
        fb_copy(k, 0, partner).wait_recv()
        fp_copy(k, 1, rows_b).start()

    loop(0, (nz - 1) * ny, fa_late)
    loop(0, (ny - 1) * nz, fb_late)

    def fp_wait(d):
        k = lax.rem(kv + d, nkv)
        fp_copy(k, 0, other_a).wait_recv()
        fp_copy(k, 1, other_b).wait_recv()

    loop(1, nkv, fp_wait)

    def square_sum(k, acc):
        blk = res[k].astype(F32)
        sq = blk * blk
        for i in range(dk // 128):
            acc = acc + sq[:, i * 128 : (i + 1) * 128]
        return acc

    total = lax.fori_loop(0, nkv, square_sum, jnp.zeros((rows, 128), F32))
    scale = lax.rsqrt(jnp.sum(total, axis=1, keepdims=True) / width + EPSILON)
    later_copies[2].wait()
    acc_up[...] = jnp.zeros_like(acc_up)

    def up(k):
        at = block(k, dk)
        blk = (res[k].astype(F32) * scale * mlp_gain_ref[:, at]).astype(BF16)
        acc_up[...] += jnp.dot(blk, w_up[at, :], preferred_element_type=F32)

    loop(0, nkv, up)
    relu = jnp.maximum(acc_up[...], 0.0)
    hid[...] = (relu * relu).astype(BF16)
    later_copies[3].wait()

    def hd_copy(k):
        return remote(send_d.at[k], recv_d.at[k], hd_send.at[k], hd_recv.at[k], partner)

    half_other = pl.ds(pl.multiple_of(other * rh, rh), rh)
    half_own = pl.ds(pl.multiple_of(c * rh, rh), rh)

    def down_other(i):
        k = lax.rem(kv + 1 + i, nkv)
        out = jnp.dot(hid[half_other, :], w_down[:, block(k, dk)], preferred_element_type=F32)
        send_d[k] = out.astype(BF16)
        hd_copy(k).start()

    loop(0, nkv, down_other)

    part_a, part_b = pl.ds(0, rc), pl.ds(rc, rc)

    def h1a_copy(k, src_z, dev):
        yk = lax.rem(k, ny)
        return remote(
            send_h.at[k, part_a, :],
            recv_h1a.at[src_z, yk],
            h1a_send.at[k],
            h1a_recv.at[src_z, yk],
            dev,
        )

    def h1b_copy(k, src_y, dev):
        zk = k // ny
        return remote(
            send_h.at[k, part_b, :],
            recv_h1b.at[src_y, zk],
            h1b_send.at[k],
            h1b_recv.at[src_y, zk],
            dev,
        )

    def down_own(i):
        k = lax.rem(kv + 1 + i, nkv)
        zk, yk = k // ny, lax.rem(k, ny)
        out = jnp.dot(hid[half_own, :], w_down[:, block(k, dk)], preferred_element_type=F32)
        hd_copy(k).wait_recv()
        send_h[k] = (out + recv_d[k].astype(F32)).astype(BF16)

        @pl.when(zk != z)
        def _():
            h1a_copy(k, z, {"kv_0": zk}).start()

        @pl.when(yk != y)
        def _():
            h1b_copy(k, y, {"kv_1": yk}).start()

    loop(0, nkv, down_own)

    def h1a_sum(yk):
        acc = send_h[z * ny + yk, 0:rc, :].astype(F32)
        for d in range(1, nz):
            src = lax.rem(z + nz - d, nz)
            h1a_copy(z * ny + yk, src, partner).wait_recv()
            acc = acc + recv_h1a[src, yk].astype(F32)
        return acc

    def h1b_sum(zk):
        acc = send_h[zk * ny + y, rc : 2 * rc, :].astype(F32)
        for d in range(1, ny):
            src = lax.rem(y + ny - d, ny)
            h1b_copy(zk * ny + y, src, partner).wait_recv()
            acc = acc + recv_h1b[src, zk].astype(F32)
        return acc

    def h2a_copy(d, yk, src_y, dev):
        return remote(
            send_h2a.at[yk], recv_h2a.at[src_y], h2_send.at[0, d], h2a_recv.at[src_y], dev
        )

    def h2b_copy(d, zk, src_z, dev):
        return remote(
            send_h2b.at[zk], recv_h2b.at[src_z], h2_send.at[1, d], h2b_recv.at[src_z], dev
        )

    for d in range(1, max(ny, nz)):
        if d < ny:
            yk = lax.rem(y + d, ny)
            send_h2a[yk] = h1a_sum(yk).astype(BF16)
            h2a_copy(d, yk, y, {"kv_1": yk}).start()
        if d < nz:
            zk = lax.rem(z + d, nz)
            send_h2b[zk] = h1b_sum(zk).astype(BF16)
            h2b_copy(d, zk, z, {"kv_0": zk}).start()
    sum_a = h1a_sum(y)
    sum_b = h1b_sum(z)
    for d in range(1, ny):
        src = lax.rem(y + ny - d, ny)
        h2a_copy(d, y, src, partner).wait_recv()
        sum_a = sum_a + recv_h2a[src].astype(F32)
    for d in range(1, nz):
        src = lax.rem(z + nz - d, nz)
        h2b_copy(d, z, src, partner).wait_recv()
        sum_b = sum_b + recv_h2b[src].astype(F32)

    own_sum = jnp.concatenate([sum_a, sum_b], axis=0).T.astype(BF16)
    send_x[...] = own_sum

    def x_copy(d, dest_tp, src_tp, peer):
        return remote(
            send_x.at[block(dest_tp, dt), :],
            recv_x.at[src_tp],
            x_send.at[d],
            x_recv.at[src_tp],
            tp_dev(peer),
        )

    def x_start(d):
        peer = lax.rem(tp + d, ntp)
        x_copy(d, peer, tp, peer).start()

    loop(1, ntp, x_start)
    recv_x[tp] = send_x[block(tp, dt), :]

    def x_wait(d):
        src = lax.rem(tp + ntp - d, ntp)
        x_copy(d, tp, src, src).wait_recv()

    loop(1, ntp, x_wait)
    for cc in range(nc):
        at = slice(cc * rh, (cc + 1) * rh)
        acc = res_t[block(tp, dt), at]
        branch = recv_x[cc].astype(F32)
        for xx in range(1, nx):
            branch = branch + recv_x[xx * nc + cc].astype(F32)
        mixed_ref[:, at] = (acc + branch).astype(BF16)

    def tp_sends(d):
        peer = lax.rem(tp + d, ntp)
        a_copy(d, tp, peer).wait_send()
        e_copy(d, peer, tp, peer).wait_send()
        f1_copy(d, tp, peer).wait_send()
        x_copy(d, peer, tp, peer).wait_send()

    loop(1, ntp, tp_sends)

    def kv_sends(d):
        peer = lax.rem(kv + d, nkv)
        b_copy(d, peer, kv, peer).wait_send()
        d_copy(d, kv, peer).wait_send()
        fp_copy(peer, 0, rows_a).wait_send()
        fp_copy(peer, 1, rows_b).wait_send()

    loop(1, nkv, kv_sends)
    loop(0, a_base + ny * (nz - 1), lambda i: fa_copy(kv, i, partner).wait_send())
    loop(0, b_base + nz * (ny - 1), lambda i: fb_copy(kv, i, partner).wait_send())

    def h_sends(k):
        zk, yk = k // ny, lax.rem(k, ny)
        hd_copy(k).wait_send()

        @pl.when(zk != z)
        def _():
            h1a_copy(k, z, {"kv_0": zk}).wait_send()

        @pl.when(yk != y)
        def _():
            h1b_copy(k, y, {"kv_1": yk}).wait_send()

    loop(0, nkv, h_sends)
    for d in range(1, ny):
        h2a_copy(d, lax.rem(y + d, ny), y, partner).wait_send()
    for d in range(1, nz):
        h2b_copy(d, lax.rem(z + d, nz), z, partner).wait_send()
    state_out.wait()


def local(
    sizes,
    tokens,
    mix_gain,
    w_query,
    w_key,
    w_value,
    w_gate,
    w_beta,
    w_decay,
    decay_rate,
    out_gain,
    state,
    w_out,
    mlp_gain,
    w_up,
    w_down,
):
    nz, ny, nx, nc = sizes
    nkv, ntp = nz * ny, nx * nc
    rows, dt = tokens.shape
    dk = dt * ntp
    rb, heads, head, _ = state.shape
    proj = heads * head
    sent = 4 * proj + 256
    ff = w_up.shape[1]
    rt, rh = rows // ntp, rows // nc
    rc = rh // 2
    vmem, dma = pltpu.VMEM, pltpu.SemaphoreType.DMA
    scratch = [
        vmem((dk, rows), BF16),
        vmem((4, dk, proj), BF16),
        vmem((128, dk), BF16),
        vmem(w_out.shape, BF16),
        vmem(w_up.shape, BF16),
        vmem(w_down.shape, BF16),
        vmem(state.shape, F32),
        vmem((rows, dk), BF16),
        vmem((rows, sent), BF16),
        vmem((nkv, rb, sent), BF16),
        vmem((heads, head, 128), F32),
        vmem((heads, head, 128), F32),
        vmem((4, heads, rb, head), F32),
        vmem((heads, rb, head), F32),
        vmem((rb, proj), F32),
        vmem((rows, proj), BF16),
        vmem((rows, dk), BF16),
        vmem((rows, dk), F32),
        vmem((ntp, rt, dk), BF16),
        vmem((nkv, rows, dk), BF16),
        vmem((dk, rows), F32),
        vmem((rows, ff), BF16),
        vmem((rows, ff), F32),
        vmem((nkv, rh, dk), BF16),
        vmem((nkv, rh, dk), BF16),
        vmem((nkv, rh, dk), BF16),
        vmem((nz, ny, rc, dk), BF16),
        vmem((ny, nz, rc, dk), BF16),
        vmem((ny, rc, dk), BF16),
        vmem((nz, rc, dk), BF16),
        vmem((ny, rc, dk), BF16),
        vmem((nz, rc, dk), BF16),
        vmem((dk, rh), BF16),
        vmem((ntp, dt, rh), BF16),
        dma((10,)),
        dma((ntp,)),
        dma((ntp,)),
        dma((nkv,)),
        dma((nkv,)),
        dma((nkv,)),
        dma((nkv,)),
        dma((ntp,)),
        dma((ntp,)),
        dma((ntp,)),
        dma((ntp,)),
        dma((ny - 1 + ny * (nz - 1),)),
        dma((nz - 1 + nz * (ny - 1),)),
        dma((nkv,)),
        dma((nkv,)),
        dma((2, nkv)),
        dma((2, nkv)),
        dma((nkv,)),
        dma((nkv,)),
        dma((nkv,)),
        dma((nkv,)),
        dma((nz, ny)),
        dma((ny, nz)),
        dma((2, max(ny, nz))),
        dma((ny,)),
        dma((nz,)),
        dma((ntp,)),
        dma((ntp,)),
    ]
    in_hbm = pl.BlockSpec(memory_space=pl.ANY)
    in_vmem = pl.BlockSpec(memory_space=pltpu.VMEM)
    in_smem = pl.BlockSpec(memory_space=pltpu.SMEM)
    mixed_t, new_state = pl.pallas_call(
        functools.partial(layer_kernel, sizes),
        out_shape=(
            jax.ShapeDtypeStruct((dt, rows), BF16),
            jax.ShapeDtypeStruct(state.shape, F32),
        ),
        in_specs=[
            in_hbm,
            in_vmem,
            in_hbm,
            in_hbm,
            in_hbm,
            in_hbm,
            in_vmem,
            in_vmem,
            in_smem,
            in_vmem,
            in_hbm,
            in_hbm,
            in_vmem,
            in_hbm,
            in_hbm,
        ],
        out_specs=(in_vmem, in_hbm),
        scratch_shapes=scratch,
        compiler_params=pltpu.CompilerParams(
            collective_id=0, has_side_effects=True, vmem_limit_bytes=67_000_000
        ),
        name="layer",
    )(
        tokens.T,
        mix_gain[None, :],
        w_query,
        w_key,
        w_value,
        w_gate,
        w_beta.T,
        w_decay.T,
        decay_rate[None, :],
        out_gain[None, :],
        state,
        w_out,
        mlp_gain[None, :],
        w_up,
        w_down,
    )
    return mixed_t.T, new_state


def solution(mesh):
    n = dict(mesh.shape)
    sizes = (n["kv"] // 4, 4, n["tp"] // 2, 2) if n["kv"] >= 8 else (2, n["kv"] // 2, n["tp"] // 2, 2)
    torus = Mesh(mesh.devices.reshape(sizes), KV_TP)
    in_specs = (
        P(None, KV_TP),
        P(KV),
        P(KV, TP),
        P(KV, TP),
        P(KV, TP),
        P(KV, TP),
        P(KV, None),
        P(KV, None),
        P(TP),
        P(),
        P(KV, TP, None, None),
        P(TP, KV),
        P(),
        P(None, KV_TP),
        P(KV_TP, None),
    )
    out_specs = (P(None, KV_TP), P(KV, TP, None, None))
    return jax.shard_map(
        functools.partial(local, sizes),
        mesh=torus,
        in_specs=in_specs,
        out_specs=out_specs,
        check_vma=False,
    )
```

time: 420 us -> 92.8 us (0.22)
  waiting for transfers between devices: 299 us -> 0 us
  Pallas kernels: 0 us -> 86.6 us
  blocking collectives: 70 us -> 0 us
  matrix products: 18.6 us -> 0 us
  between operations: 14.8 us -> 0.64 us
  other arithmetic: 8.67 us -> 0 us
    unnamed x5 -> x0, waiting for transfers between devices: 236 us -> none
    pallas_call x0 -> x1, Pallas kernels: none -> 86.6 us  [local(): pl.pallas_call(functools.partial(layer_kernel, sizes), out_shape=(jax.Sha...]
    all_gather x1 -> x0, waiting for transfers between devices: 62.7 us -> none  [local(): whole_rows = lax.all_gather(residual, KV_TP, axis=1, tiled=True)]
    all_to_all x3 -> x0, blocking collectives: 38.4 us -> none  [the longest x2 19.4 us: exchange_in_order(): filled = lax.all_to_all(filled, axes[k], k, k, tiled=True)]
    all_gather x2 -> x0, blocking collectives: 31.6 us -> none  [the longest x1 16.8 us: local(): lax.all_gather(merged, KV, axis=0, tiled=True)]
    dot_general x9 -> x0, matrix products: 18.6 us -> none  [the longest x1 5.33 us: feed_forward(): return jnp.dot(hidden, w_down, preferred_element_type=jnp.float32)]
  transfers between devices with their start and end apart: 3 -> 0, of which waited for: 3 -> 0; matrix products, arithmetic and copies ran while one was open for 1% -> 0% of each run, Pallas kernels for 0% -> 0%
where the time goes in v1:
time: 92.8 us; the launch traced here: 92.4 us
  Pallas kernels  86.6 us (93%)
  local copies, waits for them, and re-layouts  5.23 us (6%)
    pallas_call x1, Pallas kernels, local(): pl.pallas_call(functools.partial(layer_kernel, sizes), out_shape=(jax.Sha...  86.6 us
    unnamed x2, local copies, waits for them, and re-layouts  5.23 us

profile of v1, /device:TPU:1, one launch (start us, length us, event | category | flops | bytes accessed | tf_op | source)
XLA Modules:
  0.0 92.4 jit_solution(11535845582712579147)
XLA Ops:
  0.6 86.6 %layer.1 = (bf16[32,256]{1,0:T(8,128)(2,1)}, f32[16,3,128,128]{3,2,1,0:T(8,128)}) custom-call(bf16[32,256]{1,0:T(8,128)(2,1)} %bitcast.8, f32[1,256]{1,0:T(1,128)} %bitcast.13, bf16[256,384]{1,0:T(8,128)(2,1)} %wq_ref.1, bf16[256,384]{1,0:T(8,128)(2,1)} %wk_ref.1, bf16[256,384]{1,0:T(8,128)(2,1)} %wv_ref.1, bf16[256,384]{1,0:T(8,128)(2,1)} %wg_ref.1, ...), custom_call_target="tpu_custom_call" | custom-call | tf_op jit(solution)/shard_map/layer/pallas_call | solution.py:716
  87.2 1.3 %copy.19 = bf16[256,32]{0,1:T(8,128)(2,1)} copy(bf16[256,32]{0,1:T(8,128)(2,1)} %bitcast.10) | data formatting | bytes 32768
  88.5 3.9 %copy.20 = f32[16,3,128,128]{3,2,1,0:T(8,128)} copy(f32[16,3,128,128]{3,2,1,0:T(8,128)} %get-tuple-element.9) | data formatting | bytes 6291456

commit v2 on v1

v2 whole, which is shorter than its diff:
```python
import functools
import math

import jax
import jax.numpy as jnp
from jax import lax
from jax.experimental import pallas as pl
from jax.experimental.pallas import tpu as pltpu
from jax.sharding import Mesh
from jax.sharding import PartitionSpec as P

EPSILON = 1e-06
MESH = pl.DeviceIdType.MESH
KV_TP = ("kv_0", "kv_1", "tp_0", "tp_1")
KV = ("kv_0", "kv_1")
TP = ("tp_0", "tp_1")
F32 = jnp.float32
BF16 = jnp.bfloat16


def silu(v):
    return v / (1.0 + jnp.exp(-v))


def layer_kernel(
    sizes,
    tok_ref,
    mix_gain_ref,
    wq_ref,
    wk_ref,
    wv_ref,
    wg_ref,
    wbeta_ref,
    wdecay_ref,
    rate_ref,
    out_gain_ref,
    state_ref,
    wout_ref,
    mlp_gain_ref,
    wup_ref,
    wdown_ref,
    mixed_ref,
    new_state_ref,
    col_t,
    w_proj,
    w_rates,
    w_beta,
    w_decay,
    mix_gain,
    out_gain,
    mlp_gain,
    rate,
    w_out,
    w_up,
    w_down,
    st,
    col_n,
    send_b,
    recv_b1a,
    recv_b1b,
    send_b2a,
    send_b2b,
    recv_b2a,
    recv_b2b,
    key_t,
    query_t,
    rows_s,
    merged,
    send_e,
    recv_e,
    recv_ex,
    res,
    res_t,
    hid,
    acc_up,
    total_sq,
    own_d,
    send_d,
    recv_d,
    send_h,
    recv_h1a,
    recv_h1b,
    send_h2a,
    send_h2b,
    recv_h2a,
    recv_h2b,
    send_x,
    recv_x,
    local_sem,
    a_send,
    a_recv,
    b1a_send,
    b1b_send,
    b1a_recv,
    b1b_recv,
    b2_send,
    b2a_recv,
    b2b_recv,
    d_send,
    d_recv,
    e_send,
    e_recv,
    ex_send,
    ex_recv,
    fa_send,
    fb_send,
    fa_recv,
    fb_recv,
    fp_send,
    fp_recv,
    hd_send,
    hd_recv,
    h1a_send,
    h1b_send,
    h1a_recv,
    h1b_recv,
    h2_send,
    h2a_recv,
    h2b_recv,
    x_send,
    x_recv,
):
    nz, ny, nx, nc = sizes
    nkv, ntp = nz * ny, nx * nc
    z, y = lax.axis_index("kv_0"), lax.axis_index("kv_1")
    x, c = lax.axis_index("tp_0"), lax.axis_index("tp_1")
    kv, tp = z * ny + y, x * nc + c
    partner = {"tp_1": nc - 1 - c}

    dt, rows = tok_ref.shape
    dk = dt * ntp
    width = dk * nkv
    rb, heads, head = st.shape[0], st.shape[1], st.shape[2]
    proj = heads * head
    rh = rows // nc
    rc = rh // 2
    cols_a = 2 * proj
    cols_b = 2 * proj + 128
    other = nc - 1 - c

    def kv_dev(k):
        return {"kv_0": k // ny, "kv_1": lax.rem(k, ny)}

    def tp_dev(t):
        return {"tp_0": t // nc, "tp_1": lax.rem(t, nc)}

    def remote(src, dst, send_sem, recv_sem, dev):
        return pltpu.make_async_remote_copy(
            src_ref=src,
            dst_ref=dst,
            send_sem=send_sem,
            recv_sem=recv_sem,
            device_id=dev,
            device_id_type=MESH,
        )

    def loop(lo, hi, body):
        def wrapped(i, carry):
            body(i)
            return carry

        lax.fori_loop(lo, hi, wrapped, 0)

    def block(i, n):
        return pl.ds(pl.multiple_of(i * n, n), n)

    own_tok = col_t.at[block(tp, dt), :]
    first = (
        (tok_ref, own_tok),
        (wbeta_ref, w_beta),
        (wdecay_ref, w_decay),
        (mix_gain_ref, mix_gain),
        (wq_ref, w_proj.at[0]),
        (wk_ref, w_proj.at[1]),
        (wv_ref, w_proj.at[2]),
        (wg_ref, w_proj.at[3]),
        (rate_ref, rate),
        (out_gain_ref, out_gain),
        (mlp_gain_ref, mlp_gain),
        (state_ref, st),
        (wout_ref, w_out),
        (wup_ref, w_up),
        (wdown_ref, w_down),
    )
    copies = [
        pltpu.make_async_copy(src, dst, local_sem.at[i]) for i, (src, dst) in enumerate(first)
    ]
    for copy in copies:
        copy.start()

    barrier = pltpu.get_barrier_semaphore()

    def greet(dev):
        pl.semaphore_signal(barrier, inc=1, device_id=dev, device_id_type=MESH)

    def greet_tp(d):
        greet(tp_dev(lax.rem(tp + d, ntp)))

    loop(1, ntp, greet_tp)
    for d in range(1, ny):
        greet({"kv_1": lax.rem(y + d, ny)})
    for d in range(1, nz):
        greet({"kv_0": lax.rem(z + d, nz)})

    n_heads = wbeta_ref.shape[0]
    copies[1].wait()
    copies[2].wait()
    w_rates[...] = jnp.zeros_like(w_rates)
    w_rates[0:n_heads, :] = w_beta[...]
    w_rates[32 : 32 + n_heads, :] = w_decay[...]

    copies[0].wait()
    copies[3].wait()
    pl.semaphore_wait(barrier, ntp - 1 + ny - 1 + nz - 1)

    def a_copy(d, src_tp, peer):
        blk = col_t.at[block(src_tp, dt), :]
        return remote(blk, blk, a_send.at[d], a_recv.at[src_tp], tp_dev(peer))

    loop(1, ntp, lambda d: a_copy(d, tp, lax.rem(tp + d, ntp)).start())

    def a_wait(d):
        src = lax.rem(tp + ntp - d, ntp)
        a_copy(d, src, src).wait_recv()

    loop(1, ntp, a_wait)

    cols = col_t[...].astype(F32).T
    col_n[...] = cols.astype(BF16)
    normed = (cols * mix_gain[...]).astype(BF16)
    squares = jnp.sum(cols * cols, axis=1, keepdims=True)

    def project(i):
        copies[4 + i].wait()
        return jnp.dot(normed, w_proj[i], preferred_element_type=F32).astype(BF16)

    def b1a_copy(k, src_z, dev):
        yk = lax.rem(k, ny)
        return remote(
            send_b.at[block(k, rb), pl.ds(0, cols_a)],
            recv_b1a.at[src_z, yk],
            b1a_send.at[k],
            b1a_recv.at[src_z, yk],
            dev,
        )

    def b1b_copy(k, src_y, dev):
        zk = k // ny
        return remote(
            send_b.at[block(k, rb), pl.ds(cols_a, cols_b)],
            recv_b1b.at[src_y, zk],
            b1b_send.at[k],
            b1b_recv.at[src_y, zk],
            dev,
        )

    for i in range(2):
        send_b[:, i * proj : (i + 1) * proj] = project(i)

    def b1a_start(i):
        yk, zk = lax.rem(y + 1 + i // (nz - 1), ny), lax.rem(z + 1 + lax.rem(i, nz - 1), nz)
        b1a_copy(zk * ny + yk, z, {"kv_0": zk}).start()

    loop(0, ny * (nz - 1), b1a_start)

    contract_last = (((1,), (1,)), ((), ()))
    rates_part = lax.dot_general(
        normed, w_rates[...], contract_last, preferred_element_type=F32
    )
    lane = lax.broadcasted_iota(jnp.int32, rates_part.shape, 1)
    rates_part = jnp.where(lane == 63, squares, rates_part)
    high = rates_part.astype(BF16).astype(F32)
    low = pltpu.roll(rates_part - high, 64, 1)
    send_b[:, 4 * proj :] = jnp.where(lane < 64, high, low).astype(BF16)
    for i in range(2, 4):
        send_b[:, i * proj : (i + 1) * proj] = project(i)

    def b1b_start(i):
        zk, yk = lax.rem(z + 1 + i // (ny - 1), nz), lax.rem(y + 1 + lax.rem(i, ny - 1), ny)
        b1b_copy(zk * ny + yk, y, {"kv_1": yk}).start()

    loop(0, nz * (ny - 1), b1b_start)

    def b1a_sum(yk):
        k = z * ny + yk
        acc = send_b[block(k, rb), 0:cols_a].astype(F32)
        for d in range(1, nz):
            src = lax.rem(z + nz - d, nz)
            b1a_copy(k, src, partner).wait_recv()
            acc = acc + recv_b1a[src, yk].astype(F32)
        return acc

    def b1b_sum(zk):
        k = zk * ny + y
        acc = send_b[block(k, rb), cols_a : cols_a + cols_b].astype(F32)
        for d in range(1, ny):
            src = lax.rem(y + ny - d, ny)
            b1b_copy(k, src, partner).wait_recv()
            acc = acc + recv_b1b[src, zk].astype(F32)
        return acc

    def b2a_copy(d, yk, src_y, dev):
        return remote(
            send_b2a.at[yk], recv_b2a.at[src_y], b2_send.at[0, d], b2a_recv.at[src_y], dev
        )

    def b2b_copy(d, zk, src_z, dev):
        return remote(
            send_b2b.at[zk], recv_b2b.at[src_z], b2_send.at[1, d], b2b_recv.at[src_z], dev
        )

    for d in range(1, max(ny, nz)):
        if d < ny:
            yk = lax.rem(y + d, ny)
            send_b2a[yk] = b1a_sum(yk).astype(BF16)
            b2a_copy(d, yk, y, {"kv_1": yk}).start()
        if d < nz:
            zk = lax.rem(z + d, nz)
            send_b2b[zk] = b1b_sum(zk).astype(BF16)
            b2b_copy(d, zk, z, {"kv_0": zk}).start()
    sum_a = b1a_sum(y)
    sum_b = b1b_sum(z)

    for d in range(1, nz):
        src = lax.rem(z + nz - d, nz)
        b2b_copy(d, z, src, partner).wait_recv()
        sum_b = sum_b + recv_b2b[src].astype(F32)
    for d in range(1, ny):
        src = lax.rem(y + ny - d, ny)
        b2a_copy(d, y, src, partner).wait_recv()
        sum_a = sum_a + recv_b2a[src].astype(F32)

    rates = sum_b[:, 2 * proj :]
    rates = rates + pltpu.roll(rates, 64, 1)
    lane_b = lax.broadcasted_iota(jnp.int32, rates.shape, 1)

    def pick(i):
        return jnp.sum(jnp.where(lane_b == i, rates, 0.0), axis=1, keepdims=True)

    for i in range(8, 12):
        copies[i].wait()
    row_scale = lax.rsqrt(pick(63) / width + EPSILON)
    repeat = 128 // rb
    group = 4
    gates = []
    for h in range(heads):
        at = slice(h * head, (h + 1) * head)
        beta_raw = pick(tp * heads + h) * row_scale
        decay_raw = pick(32 + tp * heads + h) * row_scale
        beta = 1.0 / (1.0 + jnp.exp(-beta_raw))
        softplus = jnp.maximum(decay_raw, 0.0) + jnp.log1p(jnp.exp(-jnp.abs(decay_raw)))
        decay = jnp.exp(-rate[0:1, h : h + 1] * softplus)
        query = silu(sum_a[:, :proj][:, at] * row_scale)
        query = query * lax.rsqrt(jnp.sum(query * query, axis=1, keepdims=True) + EPSILON)
        query = query * head ** (-0.5)
        key = silu(sum_a[:, proj:][:, at] * row_scale)
        key = key * lax.rsqrt(jnp.sum(key * key, axis=1, keepdims=True) + EPSILON)
        key_tr = jnp.concatenate([key] * repeat, axis=0).T
        query_tr = jnp.concatenate([query] * repeat, axis=0).T
        for g in range(rb // group):
            key_t[g, h] = pltpu.roll(key_tr, (128 - g * group) % 128, 1) if g else key_tr
            query_t[g, h] = pltpu.roll(query_tr, (128 - g * group) % 128, 1) if g else query_tr
        shape = (rb, head)
        rows_s[0, h] = jnp.broadcast_to(decay, shape)
        rows_s[1, h] = jnp.broadcast_to(beta, shape)
        rows_s[2, h] = silu(sum_b[:, :proj][:, at] * row_scale)
        rows_s[3, h] = jnp.broadcast_to(
            jnp.sum(key * query, axis=1, keepdims=True), shape
        )
        gates.append(silu(sum_b[:, proj : 2 * proj][:, at] * row_scale))

    def read_group(g):
        for i in range(group):
            b = g * group + i
            for h in range(heads):
                state = st[b, h]
                rows_s[4, h, pl.ds(b, 1), :] = jnp.sum(
                    state * key_t[g, h, :, i : i + 1], axis=0, keepdims=True
                )
                rows_s[5, h, pl.ds(b, 1), :] = jnp.sum(
                    state * query_t[g, h, :, i : i + 1], axis=0, keepdims=True
                )

    loop(0, rb // group, read_group)

    own_rows = block(kv, rb)
    for h in range(heads):
        at = slice(h * head, (h + 1) * head)
        decay = rows_s[0, h]
        change = rows_s[1, h] * (rows_s[2, h] - decay * rows_s[4, h])
        read = decay * rows_s[5, h] + rows_s[3, h] * change
        rows_s[4, h] = change
        scale = lax.rsqrt(jnp.sum(read * read, axis=1, keepdims=True) / head + EPSILON)
        merged[own_rows, at] = (read * scale * out_gain[...] * gates[h]).astype(BF16)

    def d_copy(d, src_kv, peer):
        blk = merged.at[block(src_kv, rb), :]
        return remote(blk, blk, d_send.at[d], d_recv.at[src_kv], kv_dev(peer))

    loop(1, nkv, lambda d: d_copy(d, kv, lax.rem(kv + d, nkv)).start())

    def d_wait(d):
        src = lax.rem(kv + nkv - d, nkv)
        d_copy(d, src, src).wait_recv()

    def write_group(g):
        for i in range(group):
            b = g * group + i
            for h in range(heads):
                new_state_ref[b, h] = (
                    rows_s[0, h, pl.ds(b, 1), :] * st[b, h]
                    + key_t[g, h, :, i : i + 1] * rows_s[4, h, pl.ds(b, 1), :]
                )

    loop(0, rb // group, write_group)
    copies[12].wait()
    loop(1, nkv, d_wait)

    half_other = pl.ds(pl.multiple_of(other * rh, rh), rh)
    half_own = pl.ds(pl.multiple_of(c * rh, rh), rh)
    e_copy = remote(send_e, recv_e, e_send, e_recv, partner)
    send_e[...] = jnp.dot(
        merged[half_other, :], w_out[...], preferred_element_type=F32
    ).astype(BF16)
    e_copy.start()
    part = jnp.dot(merged[half_own, :], w_out[...], preferred_element_type=F32)
    e_copy.wait_recv()
    recv_ex[x] = (part + recv_e[...].astype(F32)).astype(BF16)

    def ex_copy(d, src_x, dev):
        blk = recv_ex.at[src_x]
        return remote(blk, blk, ex_send.at[d], ex_recv.at[src_x], dev)

    for d in range(1, nx):
        ex_copy(d, x, {"tp_0": lax.rem(x + d, nx)}).start()
    for d in range(1, nx):
        ex_copy(d, lax.rem(x + nx - d, nx), partner).wait_recv()
    branch = recv_ex[0].astype(F32)
    for i in range(1, nx):
        branch = branch + recv_ex[i].astype(F32)
    res[kv, half_own, :] = (col_n[half_own, :].astype(F32) + branch).astype(BF16)

    rows_a = pl.ds(pl.multiple_of(c * rh, rc), rc)
    rows_b = pl.ds(pl.multiple_of(c * rh + rc, rc), rc)
    other_a = pl.ds(pl.multiple_of(other * rh, rc), rc)
    other_b = pl.ds(pl.multiple_of(other * rh + rc, rc), rc)

    def fa_copy(k, slot, dev):
        blk = res.at[k, rows_a, :]
        return remote(blk, blk, fa_send.at[slot], fa_recv.at[k], dev)

    def fb_copy(k, slot, dev):
        blk = res.at[k, rows_b, :]
        return remote(blk, blk, fb_send.at[slot], fb_recv.at[k], dev)

    def y_dev(d):
        return {"kv_1": lax.rem(y + d, ny)}

    def z_dev(d):
        return {"kv_0": lax.rem(z + d, nz)}

    def fp_copy(k, half, at):
        blk = res.at[k, at, :]
        return remote(blk, blk, fp_send.at[half, k], fp_recv.at[half, k], partner)

    for d in range(1, ny):
        fa_copy(kv, d - 1, y_dev(d)).start()
    for d in range(1, nz):
        fb_copy(kv, d - 1, z_dev(d)).start()
    a_base, b_base = ny - 1, nz - 1
    for d in range(1, nz):
        fa_copy(kv, a_base + d - 1, z_dev(d)).start()
    for d in range(1, ny):
        fb_copy(kv, b_base + d - 1, y_dev(d)).start()

    fp_copy(kv, 0, rows_a).start()
    fp_copy(kv, 1, rows_b).start()

    for i in range(1, max(ny, nz)):
        if i < ny:
            k = z * ny + lax.rem(y + ny - i, ny)
            fa_copy(k, 0, partner).wait_recv()
            for d in range(1, nz):
                fa_copy(k, a_base + i * (nz - 1) + d - 1, z_dev(d)).start()
            fp_copy(k, 0, rows_a).start()
        if i < nz:
            k = lax.rem(z + nz - i, nz) * ny + y
            fb_copy(k, 0, partner).wait_recv()
            for d in range(1, ny):
                fb_copy(k, b_base + i * (ny - 1) + d - 1, y_dev(d)).start()
            fp_copy(k, 1, rows_b).start()

    n_late = max((nz - 1) * ny, (ny - 1) * nz)

    def late(i):
        zd, yd = 1 + lax.rem(i, nz - 1), i // (nz - 1)
        k = lax.rem(z + nz - zd, nz) * ny + lax.rem(y + ny - yd, ny)
        fa_copy(k, 0, partner).wait_recv()
        fp_copy(k, 0, rows_a).start()
        yd, zd = 1 + lax.rem(i, ny - 1), i // (ny - 1)
        k = lax.rem(z + nz - zd, nz) * ny + lax.rem(y + ny - yd, ny)
        fb_copy(k, 0, partner).wait_recv()
        fp_copy(k, 1, rows_b).start()

    def up(j):
        k = lax.rem(z + nz - j // ny, nz) * ny + lax.rem(y + ny - lax.rem(j, ny), ny)
        fp_copy(k, 0, other_a).wait_recv()
        fp_copy(k, 1, other_b).wait_recv()
        at = block(k, dk)
        blk = res[k].astype(F32)
        sq = blk * blk
        total = total_sq[...]
        for i in range(dk // 128):
            total = total + sq[:, i * 128 : (i + 1) * 128]
        total_sq[...] = total
        acc_up[...] += jnp.dot(
            (blk * mlp_gain[:, at]).astype(BF16), w_up[at, :], preferred_element_type=F32
        )

    lag = 0
    for j in range(1, nkv):
        zd, yd = j // ny, j % ny
        ready = max(yd * (nz - 1) + zd - 1 if zd else 0, zd * (ny - 1) + yd - 1 if yd else 0)
        lag = max(lag, ready - (j - 1))

    acc_up[...] = jnp.zeros_like(acc_up)
    total_sq[...] = jnp.zeros_like(total_sq)
    copies[13].wait()
    up(0)
    res_t[...] = res[kv].astype(F32).T
    loop(0, lag, late)

    def late_and_up(i):
        late(i)
        up(i - lag + 1)

    loop(lag, n_late, late_and_up)

    loop(n_late - lag + 1, nkv, up)

    copies[14].wait()
    scale = lax.rsqrt(jnp.sum(total_sq[...], axis=1, keepdims=True) / width + EPSILON)
    relu = jnp.maximum(acc_up[...] * scale, 0.0)
    acc_up[...] = relu * relu
    hid[0:rh, :] = acc_up[half_other, :].astype(BF16)
    hid[rh:, :] = acc_up[half_own, :].astype(BF16)

    def hd_copy(k):
        return remote(send_d.at[k], recv_d.at[k], hd_send.at[k], hd_recv.at[k], partner)

    def down(i):
        k = lax.rem(kv + 1 + i, nkv)
        out = jnp.dot(hid[...], w_down[:, block(k, dk)], preferred_element_type=F32)
        send_d[k] = out[:rh].astype(BF16)
        hd_copy(k).start()
        own_d[k] = out[rh:]

    part_a, part_b = pl.ds(0, rc), pl.ds(rc, rc)

    def h1a_copy(k, src_z, dev):
        yk = lax.rem(k, ny)
        return remote(
            send_h.at[k, part_a, :],
            recv_h1a.at[src_z, yk],
            h1a_send.at[k],
            h1a_recv.at[src_z, yk],
            dev,
        )

    def h1b_copy(k, src_y, dev):
        zk = k // ny
        return remote(
            send_h.at[k, part_b, :],
            recv_h1b.at[src_y, zk],
            h1b_send.at[k],
            h1b_recv.at[src_y, zk],
            dev,
        )

    def joined(i):
        k = lax.rem(kv + 1 + i, nkv)
        zk, yk = k // ny, lax.rem(k, ny)
        hd_copy(k).wait_recv()
        send_h[k] = (own_d[k] + recv_d[k].astype(F32)).astype(BF16)

        @pl.when(zk != z)
        def _():
            h1a_copy(k, z, {"kv_0": zk}).start()

        @pl.when(yk != y)
        def _():
            h1b_copy(k, y, {"kv_1": yk}).start()

    behind = min(6, nkv - 1)
    loop(0, behind, down)

    def down_and_joined(i):
        down(i)
        joined(i - behind)

    loop(behind, nkv, down_and_joined)
    loop(nkv - behind, nkv, joined)

    def h1a_sum(yk):
        acc = send_h[z * ny + yk, 0:rc, :].astype(F32)
        for d in range(1, nz):
            src = lax.rem(z + nz - d, nz)
            h1a_copy(z * ny + yk, src, partner).wait_recv()
            acc = acc + recv_h1a[src, yk].astype(F32)
        return acc

    def h1b_sum(zk):
        acc = send_h[zk * ny + y, rc : 2 * rc, :].astype(F32)
        for d in range(1, ny):
            src = lax.rem(y + ny - d, ny)
            h1b_copy(zk * ny + y, src, partner).wait_recv()
            acc = acc + recv_h1b[src, zk].astype(F32)
        return acc

    def h2a_copy(d, yk, src_y, dev):
        return remote(
            send_h2a.at[yk], recv_h2a.at[src_y], h2_send.at[0, d], h2a_recv.at[src_y], dev
        )

    def h2b_copy(d, zk, src_z, dev):
        return remote(
            send_h2b.at[zk], recv_h2b.at[src_z], h2_send.at[1, d], h2b_recv.at[src_z], dev
        )

    for d in range(1, max(ny, nz)):
        if d < ny:
            yk = lax.rem(y + d, ny)
            send_h2a[yk] = h1a_sum(yk).astype(BF16)
            h2a_copy(d, yk, y, {"kv_1": yk}).start()
        if d < nz:
            zk = lax.rem(z + d, nz)
            send_h2b[zk] = h1b_sum(zk).astype(BF16)
            h2b_copy(d, zk, z, {"kv_0": zk}).start()
    sum_a = h1a_sum(y)
    sum_b = h1b_sum(z)
    for d in range(1, ny):
        src = lax.rem(y + ny - d, ny)
        h2a_copy(d, y, src, partner).wait_recv()
        sum_a = sum_a + recv_h2a[src].astype(F32)
    for d in range(1, nz):
        src = lax.rem(z + nz - d, nz)
        h2b_copy(d, z, src, partner).wait_recv()
        sum_b = sum_b + recv_h2b[src].astype(F32)

    own_sum = jnp.concatenate([sum_a, sum_b], axis=0).T.astype(BF16)
    send_x[...] = own_sum

    def x_copy(d, dest_tp, src_tp, peer):
        return remote(
            send_x.at[block(dest_tp, dt), :],
            recv_x.at[src_tp],
            x_send.at[d],
            x_recv.at[src_tp],
            tp_dev(peer),
        )

    def x_start(d):
        peer = lax.rem(tp + d, ntp)
        x_copy(d, peer, tp, peer).start()

    loop(1, ntp, x_start)
    recv_x[tp] = send_x[block(tp, dt), :]

    def x_wait(d):
        src = lax.rem(tp + ntp - d, ntp)
        x_copy(d, tp, src, src).wait_recv()

    loop(1, ntp, x_wait)
    for cc in range(nc):
        at = slice(cc * rh, (cc + 1) * rh)
        acc = res_t[block(tp, dt), at]
        branch = recv_x[cc].astype(F32)
        for xx in range(1, nx):
            branch = branch + recv_x[xx * nc + cc].astype(F32)
        mixed_ref[:, at] = (acc + branch).astype(BF16)

    def tp_sends(d):
        peer = lax.rem(tp + d, ntp)
        a_copy(d, tp, peer).wait_send()
        x_copy(d, peer, tp, peer).wait_send()

    loop(1, ntp, tp_sends)

    def kv_sends(d):
        peer = lax.rem(kv + d, nkv)
        d_copy(d, kv, peer).wait_send()

    loop(1, nkv, kv_sends)
    e_copy.wait_send()
    for d in range(1, nx):
        ex_copy(d, x, partner).wait_send()
    loop(0, a_base + ny * (nz - 1), lambda i: fa_copy(kv, i, partner).wait_send())
    loop(0, b_base + nz * (ny - 1), lambda i: fb_copy(kv, i, partner).wait_send())

    def h_sends(k):
        zk, yk = k // ny, lax.rem(k, ny)
        fp_copy(k, 0, rows_a).wait_send()
        fp_copy(k, 1, rows_b).wait_send()
        hd_copy(k).wait_send()

        @pl.when(zk != z)
        def _():
            b1a_copy(k, z, {"kv_0": zk}).wait_send()
            h1a_copy(k, z, {"kv_0": zk}).wait_send()

        @pl.when(yk != y)
        def _():
            b1b_copy(k, y, {"kv_1": yk}).wait_send()
            h1b_copy(k, y, {"kv_1": yk}).wait_send()

    loop(0, nkv, h_sends)
    for d in range(1, ny):
        b2a_copy(d, lax.rem(y + d, ny), y, partner).wait_send()
        h2a_copy(d, lax.rem(y + d, ny), y, partner).wait_send()
    for d in range(1, nz):
        b2b_copy(d, lax.rem(z + d, nz), z, partner).wait_send()
        h2b_copy(d, lax.rem(z + d, nz), z, partner).wait_send()


def local(
    sizes,
    tokens,
    mix_gain,
    w_query,
    w_key,
    w_value,
    w_gate,
    w_beta,
    w_decay,
    decay_rate,
    out_gain,
    state,
    w_out,
    mlp_gain,
    w_up,
    w_down,
):
    nz, ny, nx, nc = sizes
    nkv, ntp = nz * ny, nx * nc
    rows, dt = tokens.shape
    dk = dt * ntp
    rb, heads, head, _ = state.shape
    proj = heads * head
    sent = 4 * proj + 128
    cols_a, cols_b = 2 * proj, 2 * proj + 128
    n_heads = w_beta.shape[1]
    ff = w_up.shape[1]
    rh = rows // nc
    rc = rh // 2
    vmem, dma = pltpu.VMEM, pltpu.SemaphoreType.DMA
    scratch = [
        vmem((dk, rows), BF16),
        vmem((4, dk, proj), BF16),
        vmem((128, dk), BF16),
        vmem((n_heads, dk), BF16),
        vmem((n_heads, dk), BF16),
        vmem((1, dk), F32),
        vmem((1, head), F32),
        vmem((1, dk * nkv), F32),
        vmem((1, heads), F32),
        vmem(w_out.shape, BF16),
        vmem(w_up.shape, BF16),
        vmem(w_down.shape, BF16),
        vmem(state.shape, F32),
        vmem((rows, dk), BF16),
        vmem((rows, sent), BF16),
        vmem((nz, ny, rb, cols_a), BF16),
        vmem((ny, nz, rb, cols_b), BF16),
        vmem((ny, rb, cols_a), BF16),
        vmem((nz, rb, cols_b), BF16),
        vmem((ny, rb, cols_a), BF16),
        vmem((nz, rb, cols_b), BF16),
        vmem((rb // 4, heads, head, 128), F32),
        vmem((rb // 4, heads, head, 128), F32),
        vmem((6, heads, rb, head), F32),
        vmem((rows, proj), BF16),
        vmem((rh, dk), BF16),
        vmem((rh, dk), BF16),
        vmem((nx, rh, dk), BF16),
        vmem((nkv, rows, dk), BF16),
        vmem((dk, rows), F32),
        vmem((rows, ff), BF16),
        vmem((rows, ff), F32),
        vmem((rows, 128), F32),
        vmem((nkv, rh, dk), F32),
        vmem((nkv, rh, dk), BF16),
        vmem((nkv, rh, dk), BF16),
        vmem((nkv, rh, dk), BF16),
        vmem((nz, ny, rc, dk), BF16),
        vmem((ny, nz, rc, dk), BF16),
        vmem((ny, rc, dk), BF16),
        vmem((nz, rc, dk), BF16),
        vmem((ny, rc, dk), BF16),
        vmem((nz, rc, dk), BF16),
        vmem((dk, rh), BF16),
        vmem((ntp, dt, rh), BF16),
        dma((15,)),
        dma((ntp,)),
        dma((ntp,)),
        dma((nkv,)),
        dma((nkv,)),
        dma((nz, ny)),
        dma((ny, nz)),
        dma((2, max(ny, nz))),
        dma((ny,)),
        dma((nz,)),
        dma((nkv,)),
        dma((nkv,)),
        dma(()),
        dma(()),
        dma((nx,)),
        dma((nx,)),
        dma((ny - 1 + ny * (nz - 1),)),
        dma((nz - 1 + nz * (ny - 1),)),
        dma((nkv,)),
        dma((nkv,)),
        dma((2, nkv)),
        dma((2, nkv)),
        dma((nkv,)),
        dma((nkv,)),
        dma((nkv,)),
        dma((nkv,)),
        dma((nz, ny)),
        dma((ny, nz)),
        dma((2, max(ny, nz))),
        dma((ny,)),
        dma((nz,)),
        dma((ntp,)),
        dma((ntp,)),
    ]
    in_hbm = pl.BlockSpec(memory_space=pl.ANY)
    in_vmem = pl.BlockSpec(memory_space=pltpu.VMEM)
    mixed_t, new_state = pl.pallas_call(
        functools.partial(layer_kernel, sizes),
        out_shape=(
            pltpu.VMEM((dt, rows), BF16),
            pltpu.VMEM(state.shape, F32),
        ),
        in_specs=[in_hbm] * 15,
        out_specs=(in_vmem, in_vmem),
        scratch_shapes=scratch,
        compiler_params=pltpu.CompilerParams(
            collective_id=0, has_side_effects=True, vmem_limit_bytes=63_500_000
        ),
        name="layer",
    )(
        tokens.T,
        mix_gain[None, :],
        w_query,
        w_key,
        w_value,
        w_gate,
        w_beta.T,
        w_decay.T,
        decay_rate[None, :],
        out_gain[None, :],
        state,
        w_out,
        mlp_gain[None, :],
        w_up,
        w_down,
    )
    return mixed_t.T, new_state


def solution(mesh):
    n = dict(mesh.shape)
    sizes = (n["kv"] // 4, 4, n["tp"] // 2, 2) if n["kv"] >= 8 else (2, n["kv"] // 2, n["tp"] // 2, 2)
    torus = Mesh(mesh.devices.reshape(sizes), KV_TP)
    in_specs = (
        P(None, KV_TP),
        P(KV),
        P(KV, TP),
        P(KV, TP),
        P(KV, TP),
        P(KV, TP),
        P(KV, None),
        P(KV, None),
        P(TP),
        P(),
        P(KV, TP, None, None),
        P(TP, KV),
        P(),
        P(None, KV_TP),
        P(KV_TP, None),
    )
    out_specs = (P(None, KV_TP), P(KV, TP, None, None))
    return jax.shard_map(
        functools.partial(local, sizes),
        mesh=torus,
        in_specs=in_specs,
        out_specs=out_specs,
        check_vma=False,
    )
```

time: 92.8 us -> 76.9 us (0.83)
  Pallas kernels: 86.6 us -> 73.9 us
  local copies, waits for them, and re-layouts: 5.23 us -> 2.27 us
    pallas_call x1, Pallas kernels: 86.6 us -> 73.9 us  [local(): pl.pallas_call(functools.partial(layer_kernel, sizes), out_shape=(pltpu.V...]
    unnamed x2, local copies, waits for them, and re-layouts: 5.23 us -> 2.27 us
where the time goes in v2:
time: 76.9 us; the launch traced here: 76.8 us
  Pallas kernels  73.9 us (96%)
  local copies, waits for them, and re-layouts  2.27 us (3%)
    pallas_call x1, Pallas kernels, local(): pl.pallas_call(functools.partial(layer_kernel, sizes), out_shape=(pltpu.V...  73.9 us
    unnamed x2, local copies, waits for them, and re-layouts  2.27 us

profile of v2, /device:TPU:1, one launch (start us, length us, event | category | flops | bytes accessed | tf_op | source)
XLA Modules:
  0.0 76.8 jit_solution(10495812410377979329)
XLA Ops:
  0.6 73.9 %layer.1 = (bf16[32,256]{1,0:T(8,128)(2,1)S(1)}, f32[16,3,128,128]{3,2,1,0:T(8,128)S(1)}) custom-call(bf16[32,256]{1,0:T(8,128)(2,1)} %bitcast.9, f32[1,256]{1,0:T(1,128)} %bitcast.13, bf16[256,384]{1,0:T(8,128)(2,1)} %wq_ref.1, bf16[256,384]{1,0:T(8,128)(2,1)} %wk_ref.1, bf16[256,384]{1,0:T(8,128)(2,1)} %wv_ref.1, bf16[256,384]{1,0:T(8,128)(2,1)} %wg_ref.1, ...), custom_call_target="tpu_custom_call" | custom-call | tf_op jit(solution)/shard_map/layer/pallas_call | solution.py:838
  74.5 0.6 copy.19
  75.1 1.7 %copy.20 = f32[16,3,128,128]{3,2,1,0:T(8,128)} copy(f32[16,3,128,128]{3,2,1,0:T(8,128)S(1)} %get-tuple-element.7) | data formatting | bytes 6291456

commit v3 on v2

--- a/solution.py
+++ b/solution.py
@@ -71,12 +71,10 @@
     recv_ex,
     res,
     res_t,
+    recv_r,
     hid,
     acc_up,
     total_sq,
-    own_d,
-    send_d,
-    recv_d,
     send_h,
     recv_h1a,
     recv_h1b,
@@ -106,10 +104,10 @@
     fb_send,
     fa_recv,
     fb_recv,
-    fp_send,
-    fp_recv,
-    hd_send,
-    hd_recv,
+    r_send,
+    r_recv,
+    swap_send,
+    swap_recv,
     h1a_send,
     h1b_send,
     h1a_recv,
@@ -128,6 +126,7 @@
     partner = {"tp_1": nc - 1 - c}
 
     dt, rows = tok_ref.shape
+    ff = wup_ref.shape[1]
     dk = dt * ntp
     width = dk * nkv
     rb, heads, head = st.shape[0], st.shape[1], st.shape[2]
@@ -179,8 +178,8 @@
         (mlp_gain_ref, mlp_gain),
         (state_ref, st),
         (wout_ref, w_out),
-        (wup_ref, w_up),
-        (wdown_ref, w_down),
+        (wup_ref, w_up.at[:, pl.ds(0, ff)]),
+        (wdown_ref, w_down.at[pl.ds(0, ff), :]),
     )
     copies = [
         pltpu.make_async_copy(src, dst, local_sem.at[i]) for i, (src, dst) in enumerate(first)
@@ -329,6 +328,26 @@
         src = lax.rem(y + ny - d, ny)
         b2a_copy(d, y, src, partner).wait_recv()
         sum_a = sum_a + recv_b2a[src].astype(F32)
+
+    swaps = [
+        remote(
+            w_up.at[:, pl.ds(0, ff)],
+            w_up.at[:, pl.ds(ff, ff)],
+            swap_send.at[0],
+            swap_recv.at[0],
+            partner,
+        ),
+        remote(
+            w_down.at[pl.ds(0, ff), :],
+            w_down.at[pl.ds(ff, ff), :],
+            swap_send.at[1],
+            swap_recv.at[1],
+            partner,
+        ),
+    ]
+    for i in range(2):
+        copies[13 + i].wait()
+        swaps[i].start()
 
     rates = sum_b[:, 2 * proj :]
     rates = rates + pltpu.roll(rates, 64, 1)
@@ -414,6 +433,24 @@
 
     loop(0, rb // group, write_group)
     copies[12].wait()
+
+    def a_b_sends(k):
+        zk, yk = k // ny, lax.rem(k, ny)
+
+        @pl.when(zk != z)
+        def _():
+            b1a_copy(k, z, {"kv_0": zk}).wait_send()
+
+        @pl.when(yk != y)
+        def _():
+            b1b_copy(k, y, {"kv_1": yk}).wait_send()
+
+    loop(0, nkv, a_b_sends)
+    loop(1, ntp, lambda d: a_copy(d, tp, lax.rem(tp + d, ntp)).wait_send())
+    for d in range(1, ny):
+        b2a_copy(d, lax.rem(y + d, ny), y, partner).wait_send()
+    for d in range(1, nz):
+        b2b_copy(d, lax.rem(z + d, nz), z, partner).wait_send()
     loop(1, nkv, d_wait)
 
     half_other = pl.ds(pl.multiple_of(other * rh, rh), rh)
@@ -438,12 +475,9 @@
     branch = recv_ex[0].astype(F32)
     for i in range(1, nx):
         branch = branch + recv_ex[i].astype(F32)
-    res[kv, half_own, :] = (col_n[half_own, :].astype(F32) + branch).astype(BF16)
-
-    rows_a = pl.ds(pl.multiple_of(c * rh, rc), rc)
-    rows_b = pl.ds(pl.multiple_of(c * rh + rc, rc), rc)
-    other_a = pl.ds(pl.multiple_of(other * rh, rc), rc)
-    other_b = pl.ds(pl.multiple_of(other * rh + rc, rc), rc)
+    res[kv] = (col_n[half_own, :].astype(F32) + branch).astype(BF16)
+
+    rows_a, rows_b = pl.ds(0, rc), pl.ds(rc, rc)
 
     def fa_copy(k, slot, dev):
         blk = res.at[k, rows_a, :]
@@ -458,10 +492,6 @@
 
     def z_dev(d):
         return {"kv_0": lax.rem(z + d, nz)}
-
-    def fp_copy(k, half, at):
-        blk = res.at[k, at, :]
-        return remote(blk, blk, fp_send.at[half, k], fp_recv.at[half, k], partner)
 
     for d in range(1, ny):
         fa_copy(kv, d - 1, y_dev(d)).start()
@@ -473,39 +503,15 @@
     for d in range(1, ny):
         fb_copy(kv, b_base + d - 1, y_dev(d)).start()
 
-    fp_copy(kv, 0, rows_a).start()
-    fp_copy(kv, 1, rows_b).start()
-
-    for i in range(1, max(ny, nz)):
-        if i < ny:
-            k = z * ny + lax.rem(y + ny - i, ny)
-            fa_copy(k, 0, partner).wait_recv()
-            for d in range(1, nz):
-                fa_copy(k, a_base + i * (nz - 1) + d - 1, z_dev(d)).start()
-            fp_copy(k, 0, rows_a).start()
-        if i < nz:
-            k = lax.rem(z + nz - i, nz) * ny + y
-            fb_copy(k, 0, partner).wait_recv()
-            for d in range(1, ny):
-                fb_copy(k, b_base + i * (ny - 1) + d - 1, y_dev(d)).start()
-            fp_copy(k, 1, rows_b).start()
-
-    n_late = max((nz - 1) * ny, (ny - 1) * nz)
-
-    def late(i):
-        zd, yd = 1 + lax.rem(i, nz - 1), i // (nz - 1)
-        k = lax.rem(z + nz - zd, nz) * ny + lax.rem(y + ny - yd, ny)
-        fa_copy(k, 0, partner).wait_recv()
-        fp_copy(k, 0, rows_a).start()
-        yd, zd = 1 + lax.rem(i, ny - 1), i // (ny - 1)
-        k = lax.rem(z + nz - zd, nz) * ny + lax.rem(y + ny - yd, ny)
-        fb_copy(k, 0, partner).wait_recv()
-        fp_copy(k, 1, rows_b).start()
+
+    res_t[...] = res[kv].astype(F32).T.astype(BF16)
+    r_copy = remote(
+        res_t.at[block(x * nc + other, dt), :], recv_r, r_send, r_recv, partner
+    )
+    r_copy.start()
 
     def up(j):
         k = lax.rem(z + nz - j // ny, nz) * ny + lax.rem(y + ny - lax.rem(j, ny), ny)
-        fp_copy(k, 0, other_a).wait_recv()
-        fp_copy(k, 1, other_b).wait_recv()
         at = block(k, dk)
         blk = res[k].astype(F32)
         sq = blk * blk
@@ -517,17 +523,44 @@
             (blk * mlp_gain[:, at]).astype(BF16), w_up[at, :], preferred_element_type=F32
         )
 
+    acc_up[...] = jnp.zeros_like(acc_up)
+    total_sq[...] = jnp.zeros_like(total_sq)
+    for swap in swaps:
+        swap.wait_recv()
+    up(0)
+    loop(1, nkv, lambda d: d_copy(d, kv, lax.rem(kv + d, nkv)).wait_send())
+    e_copy.wait_send()
+    for d in range(1, nx):
+        ex_copy(d, x, partner).wait_send()
+
+    for i in range(1, max(ny, nz)):
+        if i < ny:
+            k = z * ny + lax.rem(y + ny - i, ny)
+            fa_copy(k, 0, partner).wait_recv()
+            for d in range(1, nz):
+                fa_copy(k, a_base + i * (nz - 1) + d - 1, z_dev(d)).start()
+        if i < nz:
+            k = lax.rem(z + nz - i, nz) * ny + y
+            fb_copy(k, 0, partner).wait_recv()
+            for d in range(1, ny):
+                fb_copy(k, b_base + i * (ny - 1) + d - 1, y_dev(d)).start()
+
+    n_late = max((nz - 1) * ny, (ny - 1) * nz)
+
+    def late(i):
+        zd, yd = 1 + lax.rem(i, nz - 1), i // (nz - 1)
+        k = lax.rem(z + nz - zd, nz) * ny + lax.rem(y + ny - yd, ny)
+        fa_copy(k, 0, partner).wait_recv()
+        yd, zd = 1 + lax.rem(i, ny - 1), i // (ny - 1)
+        k = lax.rem(z + nz - zd, nz) * ny + lax.rem(y + ny - yd, ny)
+        fb_copy(k, 0, partner).wait_recv()
+
     lag = 0
     for j in range(1, nkv):
         zd, yd = j // ny, j % ny
         ready = max(yd * (nz - 1) + zd - 1 if zd else 0, zd * (ny - 1) + yd - 1 if yd else 0)
         lag = max(lag, ready - (j - 1))
 
-    acc_up[...] = jnp.zeros_like(acc_up)
-    total_sq[...] = jnp.zeros_like(total_sq)
-    copies[13].wait()
-    up(0)
-    res_t[...] = res[kv].astype(F32).T
     loop(0, lag, late)
 
     def late_and_up(i):
@@ -538,22 +571,9 @@
 
     loop(n_late - lag + 1, nkv, up)
 
-    copies[14].wait()
     scale = lax.rsqrt(jnp.sum(total_sq[...], axis=1, keepdims=True) / width + EPSILON)
     relu = jnp.maximum(acc_up[...] * scale, 0.0)
-    acc_up[...] = relu * relu
-    hid[0:rh, :] = acc_up[half_other, :].astype(BF16)
-    hid[rh:, :] = acc_up[half_own, :].astype(BF16)
-
-    def hd_copy(k):
-        return remote(send_d.at[k], recv_d.at[k], hd_send.at[k], hd_recv.at[k], partner)
-
-    def down(i):
-        k = lax.rem(kv + 1 + i, nkv)
-        out = jnp.dot(hid[...], w_down[:, block(k, dk)], preferred_element_type=F32)
-        send_d[k] = out[:rh].astype(BF16)
-        hd_copy(k).start()
-        own_d[k] = out[rh:]
+    hid[...] = (relu * relu).astype(BF16)
 
     part_a, part_b = pl.ds(0, rc), pl.ds(rc, rc)
 
@@ -577,11 +597,11 @@
             dev,
         )
 
-    def joined(i):
+    def down(i):
         k = lax.rem(kv + 1 + i, nkv)
         zk, yk = k // ny, lax.rem(k, ny)
-        hd_copy(k).wait_recv()
-        send_h[k] = (own_d[k] + recv_d[k].astype(F32)).astype(BF16)
+        out = jnp.dot(hid[...], w_down[:, block(k, dk)], preferred_element_type=F32)
+        send_h[k] = out.astype(BF16)
 
         @pl.when(zk != z)
         def _():
@@ -591,15 +611,12 @@
         def _():
             h1b_copy(k, y, {"kv_1": yk}).start()
 
-    behind = min(6, nkv - 1)
-    loop(0, behind, down)
-
-    def down_and_joined(i):
-        down(i)
-        joined(i - behind)
-
-    loop(behind, nkv, down_and_joined)
-    loop(nkv - behind, nkv, joined)
+    loop(0, nkv, down)
+    loop(0, a_base + ny * (nz - 1), lambda i: fa_copy(kv, i, partner).wait_send())
+    loop(0, b_base + nz * (ny - 1), lambda i: fb_copy(kv, i, partner).wait_send())
+    for swap in swaps:
+        swap.wait_send()
+    r_copy.wait_send()
 
     def h1a_sum(yk):
         acc = send_h[z * ny + yk, 0:rc, :].astype(F32)
@@ -671,54 +688,38 @@
         x_copy(d, tp, src, src).wait_recv()
 
     loop(1, ntp, x_wait)
-    for cc in range(nc):
-        at = slice(cc * rh, (cc + 1) * rh)
-        acc = res_t[block(tp, dt), at]
-        branch = recv_x[cc].astype(F32)
+    r_copy.wait_recv()
+
+    def finish(core, residual):
+        total = residual.astype(F32) + recv_x[core].astype(F32)
         for xx in range(1, nx):
-            branch = branch + recv_x[xx * nc + cc].astype(F32)
-        mixed_ref[:, at] = (acc + branch).astype(BF16)
+            total = total + recv_x[xx * nc + core].astype(F32)
+        mixed_ref[:, block(core, rh)] = total.astype(BF16)
+
+    finish(c, res_t[block(tp, dt), :])
+    finish(other, recv_r[...])
 
     def tp_sends(d):
         peer = lax.rem(tp + d, ntp)
-        a_copy(d, tp, peer).wait_send()
         x_copy(d, peer, tp, peer).wait_send()
 
     loop(1, ntp, tp_sends)
-
-    def kv_sends(d):
-        peer = lax.rem(kv + d, nkv)
-        d_copy(d, kv, peer).wait_send()
-
-    loop(1, nkv, kv_sends)
-    e_copy.wait_send()
-    for d in range(1, nx):
-        ex_copy(d, x, partner).wait_send()
-    loop(0, a_base + ny * (nz - 1), lambda i: fa_copy(kv, i, partner).wait_send())
-    loop(0, b_base + nz * (ny - 1), lambda i: fb_copy(kv, i, partner).wait_send())
 
     def h_sends(k):
         zk, yk = k // ny, lax.rem(k, ny)
-        fp_copy(k, 0, rows_a).wait_send()
-        fp_copy(k, 1, rows_b).wait_send()
-        hd_copy(k).wait_send()
 
         @pl.when(zk != z)
         def _():
-            b1a_copy(k, z, {"kv_0": zk}).wait_send()
             h1a_copy(k, z, {"kv_0": zk}).wait_send()
 
         @pl.when(yk != y)
         def _():
-            b1b_copy(k, y, {"kv_1": yk}).wait_send()
             h1b_copy(k, y, {"kv_1": yk}).wait_send()
 
     loop(0, nkv, h_sends)
     for d in range(1, ny):
-        b2a_copy(d, lax.rem(y + d, ny), y, partner).wait_send()
         h2a_copy(d, lax.rem(y + d, ny), y, partner).wait_send()
     for d in range(1, nz):
-        b2b_copy(d, lax.rem(z + d, nz), z, partner).wait_send()
         h2b_copy(d, lax.rem(z + d, nz), z, partner).wait_send()
 
 
@@ -764,8 +765,8 @@
         vmem((1, dk * nkv), F32),
         vmem((1, heads), F32),
         vmem(w_out.shape, BF16),
-        vmem(w_up.shape, BF16),
-        vmem(w_down.shape, BF16),
+        vmem((w_up.shape[0], 2 * ff), BF16),
+        vmem((2 * ff, w_down.shape[1]), BF16),
         vmem(state.shape, F32),
         vmem((rows, dk), BF16),
         vmem((rows, sent), BF16),
@@ -782,14 +783,12 @@
         vmem((rh, dk), BF16),
         vmem((rh, dk), BF16),
         vmem((nx, rh, dk), BF16),
-        vmem((nkv, rows, dk), BF16),
-        vmem((dk, rows), F32),
-        vmem((rows, ff), BF16),
-        vmem((rows, ff), F32),
-        vmem((rows, 128), F32),
-        vmem((nkv, rh, dk), F32),
         vmem((nkv, rh, dk), BF16),
-        vmem((nkv, rh, dk), BF16),
+        vmem((dk, rh), BF16),
+        vmem((dt, rh), BF16),
+        vmem((rh, 2 * ff), BF16),
+        vmem((rh, 2 * ff), F32),
+        vmem((rh, 128), F32),
         vmem((nkv, rh, dk), BF16),
         vmem((nz, ny, rc, dk), BF16),
         vmem((ny, nz, rc, dk), BF16),
@@ -819,10 +818,10 @@
         dma((nz - 1 + nz * (ny - 1),)),
         dma((nkv,)),
         dma((nkv,)),
-        dma((2, nkv)),
-        dma((2, nkv)),
-        dma((nkv,)),
-        dma((nkv,)),
+        dma(()),
+        dma(()),
+        dma((2,)),
+        dma((2,)),
         dma((nkv,)),
         dma((nkv,)),
         dma((nz, ny)),

time: 76.9 us -> 72.1 us (0.938)
  Pallas kernels: 73.9 us -> 69 us
    pallas_call x1, Pallas kernels: 73.9 us -> 69 us  [local(): pl.pallas_call(functools.partial(layer_kernel, sizes), out_shape=(pltpu.V...]
where the time goes in v3:
time: 72.1 us; the launch traced here: 71.9 us
  Pallas kernels  69 us (96%)
  local copies, waits for them, and re-layouts  2.27 us (3%)
    pallas_call x1, Pallas kernels, local(): pl.pallas_call(functools.partial(layer_kernel, sizes), out_shape=(pltpu.V...  69 us
    unnamed x2, local copies, waits for them, and re-layouts  2.27 us

profile of v3, /device:TPU:1, one launch (start us, length us, event | category | flops | bytes accessed | tf_op | source)
XLA Modules:
  0.0 71.9 jit_solution(17018215751279513225)
XLA Ops:
  0.6 69.0 %layer.1 = (bf16[32,256]{1,0:T(8,128)(2,1)S(1)}, f32[16,3,128,128]{3,2,1,0:T(8,128)S(1)}) custom-call(bf16[32,256]{1,0:T(8,128)(2,1)} %bitcast.9, f32[1,256]{1,0:T(1,128)} %bitcast.13, bf16[256,384]{1,0:T(8,128)(2,1)} %wq_ref.1, bf16[256,384]{1,0:T(8,128)(2,1)} %wk_ref.1, bf16[256,384]{1,0:T(8,128)(2,1)} %wv_ref.1, bf16[256,384]{1,0:T(8,128)(2,1)} %wg_ref.1, ...), custom_call_target="tpu_custom_call" | custom-call | tf_op jit(solution)/shard_map/layer/pallas_call | solution.py:837
  69.7 0.6 copy.19
  70.3 1.7 %copy.20 = f32[16,3,128,128]{3,2,1,0:T(8,128)} copy(f32[16,3,128,128]{3,2,1,0:T(8,128)S(1)} %get-tuple-element.7) | data formatting | bytes 6291456

commit v4 on v3

v4 whole, which is shorter than its diff:
```python
import functools

import jax
import jax.numpy as jnp
from jax import lax
from jax.experimental import pallas as pl
from jax.experimental.pallas import tpu as pltpu
from jax.sharding import Mesh
from jax.sharding import PartitionSpec as P

EPSILON = 1e-06
MESH = pl.DeviceIdType.MESH
KV_TP = ("kv_0", "kv_1", "tp_0", "tp_1")
KV = ("kv_0", "kv_1")
TP = ("tp_0", "tp_1")
F32 = jnp.float32
BF16 = jnp.bfloat16


def silu(v):
    return v / (1.0 + jnp.exp(-v))


def layer_kernel(
    sizes,
    tok_ref,
    mix_gain_ref,
    wq_ref,
    wk_ref,
    wv_ref,
    wg_ref,
    wbeta_ref,
    wdecay_ref,
    rate_ref,
    out_gain_ref,
    state_ref,
    wout_ref,
    mlp_gain_ref,
    wup_ref,
    wdown_ref,
    mixed_ref,
    new_state_ref,
    col_t,
    w_proj,
    w_rates,
    w_beta,
    w_decay,
    mix_gain,
    out_gain,
    mlp_gain,
    rate,
    w_out,
    w_up,
    w_down,
    st,
    col_n,
    send_b,
    recv_b1a,
    recv_b1b,
    send_b2a,
    send_b2b,
    recv_b2a,
    recv_b2b,
    key_t,
    query_t,
    rows_s,
    merged,
    send_e,
    recv_e,
    recv_ex,
    res,
    res_t,
    recv_r,
    hid,
    acc_up,
    total_sq,
    send_h,
    recv_h1a,
    recv_h1b,
    send_h2a,
    send_h2b,
    recv_h2a,
    recv_h2b,
    send_x,
    recv_x,
    local_sem,
    a_send,
    a_recv,
    b1a_send,
    b1b_send,
    b1a_recv,
    b1b_recv,
    b2_send,
    b2_recv,
    d_send,
    d_recv,
    e_send,
    e_recv,
    ex_send,
    ex_recv,
    fa_send,
    fb_send,
    fa_recv,
    fb_recv,
    r_send,
    r_recv,
    swap_send,
    swap_recv,
    h1a_send,
    h1b_send,
    h1a_recv,
    h1b_recv,
    h2_send,
    h2_recv,
    x_send,
    x_recv,
):
    nz, ny, nx, nc = sizes
    nkv, ntp = nz * ny, nx * nc
    z, y = lax.axis_index("kv_0"), lax.axis_index("kv_1")
    x, c = lax.axis_index("tp_0"), lax.axis_index("tp_1")
    kv, tp = z * ny + y, x * nc + c
    partner = {"tp_1": nc - 1 - c}

    dt, rows = tok_ref.shape
    ff = wup_ref.shape[1]
    dk = dt * ntp
    width = dk * nkv
    rb, heads, head = st.shape[0], st.shape[1], st.shape[2]
    proj = heads * head
    rh = rows // nc
    rc = rh // 2
    cols_a = 2 * proj
    cols_b = 2 * proj + 128
    other = nc - 1 - c

    def kv_dev(k):
        return {"kv_0": k // ny, "kv_1": lax.rem(k, ny)}

    def tp_dev(t):
        return {"tp_0": t // nc, "tp_1": lax.rem(t, nc)}

    def remote(src, dst, send_sem, recv_sem, dev):
        return pltpu.make_async_remote_copy(
            src_ref=src,
            dst_ref=dst,
            send_sem=send_sem,
            recv_sem=recv_sem,
            device_id=dev,
            device_id_type=MESH,
        )

    def all_received(ref, send_sem, recv_sem):
        remote(ref, ref, send_sem, recv_sem, partner).wait_recv()

    def all_sent(ref, send_sem, recv_sem):
        remote(ref, ref, send_sem, recv_sem, partner).wait_send()

    def loop(lo, hi, body):
        def wrapped(i, carry):
            body(i)
            return carry

        lax.fori_loop(lo, hi, wrapped, 0)

    def ring(n):
        return sorted(range(1, n), key=lambda d: (-min(d, n - d), d))

    def block(i, n):
        return pl.ds(pl.multiple_of(i * n, n), n)

    own_tok = col_t.at[block(tp, dt), :]
    first = (
        (tok_ref, own_tok),
        (wbeta_ref, w_beta),
        (wdecay_ref, w_decay),
        (mix_gain_ref, mix_gain),
        (rate_ref, rate),
        (out_gain_ref, out_gain),
        (mlp_gain_ref, mlp_gain),
        (state_ref, st),
        (wout_ref, w_out),
        (wup_ref, w_up.at[:, pl.ds(0, ff)]),
        (wdown_ref, w_down.at[pl.ds(0, ff), :]),
    )
    copies = [
        pltpu.make_async_copy(src, dst, local_sem.at[i]) for i, (src, dst) in enumerate(first)
    ]
    for copy in copies[:4]:
        copy.start()
    for i, w in enumerate((wq_ref, wk_ref, wv_ref, wg_ref)):
        pltpu.make_async_copy(w, w_proj.at[i], local_sem.at[11]).start()
    for copy in copies[4:]:
        copy.start()

    barrier = pltpu.get_barrier_semaphore()

    def greet(dev):
        pl.semaphore_signal(barrier, inc=1, device_id=dev, device_id_type=MESH)

    def greet_tp(d):
        greet(tp_dev(lax.rem(tp + d, ntp)))

    loop(1, ntp, greet_tp)
    for d in range(1, ny):
        greet({"kv_1": lax.rem(y + d, ny)})
    for d in range(1, nz):
        greet({"kv_0": lax.rem(z + d, nz)})

    n_heads = wbeta_ref.shape[0]
    copies[1].wait()
    copies[2].wait()
    w_rates[...] = jnp.zeros_like(w_rates)
    w_rates[0:n_heads, :] = w_beta[...]
    w_rates[32 : 32 + n_heads, :] = w_decay[...]

    copies[0].wait()
    copies[3].wait()
    pl.semaphore_wait(barrier, ntp - 1 + ny - 1 + nz - 1)

    def tp_peers():
        near = [(0, 1)] if nc == 2 else []
        return [(dx, dc) for dx in ring(nx) for dc in range(nc)] + near

    def tp_peer(dx, dc):
        return lax.rem(x + dx, nx) * nc + lax.rem(c + dc, nc)

    for dx, dc in tp_peers():
        remote(own_tok, own_tok, a_send, a_recv, tp_dev(tp_peer(dx, dc))).start()

    a_all = col_t.at[pl.ds(0, (ntp - 1) * dt), :]
    all_received(a_all, a_send, a_recv)

    cols = col_t[...].astype(F32).T
    col_n[...] = cols.astype(BF16)
    normed = (cols * mix_gain[...]).astype(BF16)
    squares = jnp.sum(cols * cols, axis=1, keepdims=True)

    pltpu.make_async_copy(w_proj, w_proj, local_sem.at[11]).wait()

    def project(i):
        return jnp.dot(normed, w_proj[i], preferred_element_type=F32).astype(BF16)

    def b1a_copy(dz, yk):
        zk = lax.rem(z + dz, nz)
        return remote(
            send_b.at[block(zk * ny + yk, rb), pl.ds(0, cols_a)],
            recv_b1a.at[yk, dz - 1],
            b1a_send,
            b1a_recv.at[yk],
            {"kv_0": zk},
        )

    def b1b_copy(dy, zk):
        yk = lax.rem(y + dy, ny)
        return remote(
            send_b.at[block(zk * ny + yk, rb), pl.ds(cols_a, cols_b)],
            recv_b1b.at[zk, dy - 1],
            b1b_send,
            b1b_recv.at[zk],
            {"kv_1": yk},
        )

    for i in range(2):
        send_b[:, i * proj : (i + 1) * proj] = project(i)

    for dy in [*ring(ny), 0]:
        for dz in ring(nz):
            b1a_copy(dz, lax.rem(y + dy, ny)).start()

    contract_last = (((1,), (1,)), ((), ()))
    rates_part = lax.dot_general(
        normed, w_rates[...], contract_last, preferred_element_type=F32
    )
    lane = lax.broadcasted_iota(jnp.int32, rates_part.shape, 1)
    rates_part = jnp.where(lane == 63, squares, rates_part)
    high = rates_part.astype(BF16).astype(F32)
    low = pltpu.roll(rates_part - high, 64, 1)
    send_b[:, 4 * proj :] = jnp.where(lane < 64, high, low).astype(BF16)
    for i in range(2, 4):
        send_b[:, i * proj : (i + 1) * proj] = project(i)

    for dz in [*ring(nz), 0]:
        for dy in ring(ny):
            b1b_copy(dy, lax.rem(z + dz, nz)).start()

    def b1a_sum(yk):
        acc = send_b[block(z * ny + yk, rb), 0:cols_a].astype(F32)
        all_received(recv_b1a.at[yk], b1a_send, b1a_recv.at[yk])
        for i in range(nz - 1):
            acc = acc + recv_b1a[yk, i].astype(F32)
        return acc

    def b1b_sum(zk):
        acc = send_b[block(zk * ny + y, rb), cols_a : cols_a + cols_b].astype(F32)
        all_received(recv_b1b.at[zk], b1b_send, b1b_recv.at[zk])
        for i in range(ny - 1):
            acc = acc + recv_b1b[zk, i].astype(F32)
        return acc

    def b2a_copy(d):
        blk = send_b2a.at[d - 1]
        dev = {"kv_1": lax.rem(y + d, ny)}
        return remote(blk, recv_b2a.at[d - 1], b2_send.at[0], b2_recv.at[0], dev)

    def b2b_copy(d):
        blk = send_b2b.at[d - 1]
        dev = {"kv_0": lax.rem(z + d, nz)}
        return remote(blk, recv_b2b.at[d - 1], b2_send.at[1], b2_recv.at[1], dev)

    for i in range(max(ny, nz) - 1):
        if i < ny - 1:
            d = ring(ny)[i]
            send_b2a[d - 1] = b1a_sum(lax.rem(y + d, ny)).astype(BF16)
            b2a_copy(d).start()
        if i < nz - 1:
            d = ring(nz)[i]
            send_b2b[d - 1] = b1b_sum(lax.rem(z + d, nz)).astype(BF16)
            b2b_copy(d).start()
    sum_a = b1a_sum(y)
    sum_b = b1b_sum(z)

    all_received(recv_b2b, b2_send.at[1], b2_recv.at[1])
    for i in range(nz - 1):
        sum_b = sum_b + recv_b2b[i].astype(F32)
    all_received(recv_b2a, b2_send.at[0], b2_recv.at[0])
    for i in range(ny - 1):
        sum_a = sum_a + recv_b2a[i].astype(F32)

    swaps = [
        remote(
            w_up.at[:, pl.ds(0, ff)],
            w_up.at[:, pl.ds(ff, ff)],
            swap_send.at[0],
            swap_recv.at[0],
            partner,
        ),
        remote(
            w_down.at[pl.ds(0, ff), :],
            w_down.at[pl.ds(ff, ff), :],
            swap_send.at[1],
            swap_recv.at[1],
            partner,
        ),
    ]
    for i in range(2):
        copies[9 + i].wait()
        swaps[i].start()

    rates = sum_b[:, 2 * proj :]
    rates = rates + pltpu.roll(rates, 64, 1)
    lane_b = lax.broadcasted_iota(jnp.int32, rates.shape, 1)

    def pick(i):
        return jnp.sum(jnp.where(lane_b == i, rates, 0.0), axis=1, keepdims=True)

    for i in range(4, 8):
        copies[i].wait()
    row_scale = lax.rsqrt(pick(63) / width + EPSILON)
    repeat = 128 // rb
    group = 4
    gates = []
    for h in range(heads):
        at = slice(h * head, (h + 1) * head)
        beta_raw = pick(tp * heads + h) * row_scale
        decay_raw = pick(32 + tp * heads + h) * row_scale
        beta = 1.0 / (1.0 + jnp.exp(-beta_raw))
        softplus = jnp.maximum(decay_raw, 0.0) + jnp.log1p(jnp.exp(-jnp.abs(decay_raw)))
        decay = jnp.exp(-rate[0:1, h : h + 1] * softplus)
        query = silu(sum_a[:, :proj][:, at] * row_scale)
        query = query * lax.rsqrt(jnp.sum(query * query, axis=1, keepdims=True) + EPSILON)
        query = query * head ** (-0.5)
        key = silu(sum_a[:, proj:][:, at] * row_scale)
        key = key * lax.rsqrt(jnp.sum(key * key, axis=1, keepdims=True) + EPSILON)
        key_tr = jnp.concatenate([key] * repeat, axis=0).T
        query_tr = jnp.concatenate([query] * repeat, axis=0).T
        for g in range(rb // group):
            key_t[g, h] = pltpu.roll(key_tr, (128 - g * group) % 128, 1) if g else key_tr
            query_t[g, h] = pltpu.roll(query_tr, (128 - g * group) % 128, 1) if g else query_tr
        shape = (rb, head)
        rows_s[0, h] = jnp.broadcast_to(decay, shape)
        rows_s[1, h] = jnp.broadcast_to(beta, shape)
        rows_s[2, h] = silu(sum_b[:, :proj][:, at] * row_scale)
        rows_s[3, h] = jnp.broadcast_to(
            jnp.sum(key * query, axis=1, keepdims=True), shape
        )
        gates.append(silu(sum_b[:, proj : 2 * proj][:, at] * row_scale))

    def read_group(g):
        for i in range(group):
            b = g * group + i
            for h in range(heads):
                state = st[b, h]
                rows_s[4, h, pl.ds(b, 1), :] = jnp.sum(
                    state * key_t[g, h, :, i : i + 1], axis=0, keepdims=True
                )
                rows_s[5, h, pl.ds(b, 1), :] = jnp.sum(
                    state * query_t[g, h, :, i : i + 1], axis=0, keepdims=True
                )

    loop(0, rb // group, read_group)

    own_rows = block(kv, rb)
    for h in range(heads):
        at = slice(h * head, (h + 1) * head)
        decay = rows_s[0, h]
        change = rows_s[1, h] * (rows_s[2, h] - decay * rows_s[4, h])
        read = decay * rows_s[5, h] + rows_s[3, h] * change
        rows_s[4, h] = change
        scale = lax.rsqrt(jnp.sum(read * read, axis=1, keepdims=True) / head + EPSILON)
        merged[own_rows, at] = (read * scale * out_gain[...] * gates[h]).astype(BF16)

    d_own = merged.at[own_rows, :]
    d_all = merged.at[pl.ds(0, (nkv - 1) * rb), :]

    def hops(d):
        dz, dy = d // ny, d % ny
        return min(dz, nz - dz) + min(dy, ny - dy)

    def kv_peer(d):
        return lax.rem(z + d // ny, nz) * ny + lax.rem(y + d % ny, ny)

    for d in sorted(range(1, nkv), key=lambda d: -hops(d)):
        remote(d_own, d_own, d_send, d_recv, kv_dev(kv_peer(d))).start()

    def write_group(g):
        for i in range(group):
            b = g * group + i
            for h in range(heads):
                st[b, h] = (
                    rows_s[0, h, pl.ds(b, 1), :] * st[b, h]
                    + key_t[g, h, :, i : i + 1] * rows_s[4, h, pl.ds(b, 1), :]
                )

    loop(0, rb // group, write_group)
    state_out = pltpu.make_async_copy(st, new_state_ref, local_sem.at[12])
    state_out.start()
    copies[8].wait()

    all_sent(a_all, a_send, a_recv)
    all_sent(recv_b1a, b1a_send, b1a_recv.at[0])
    all_sent(recv_b1b, b1b_send, b1b_recv.at[0])
    all_sent(recv_b2a, b2_send.at[0], b2_recv.at[0])
    all_sent(recv_b2b, b2_send.at[1], b2_recv.at[1])
    all_received(d_all, d_send, d_recv)

    half_other = pl.ds(pl.multiple_of(other * rh, rh), rh)
    half_own = pl.ds(pl.multiple_of(c * rh, rh), rh)
    e_copy = remote(send_e, recv_e, e_send, e_recv, partner)
    send_e[...] = jnp.dot(
        merged[half_other, :], w_out[...], preferred_element_type=F32
    ).astype(BF16)
    e_copy.start()
    part = jnp.dot(merged[half_own, :], w_out[...], preferred_element_type=F32)
    e_copy.wait_recv()
    recv_ex[x] = (part + recv_e[...].astype(F32)).astype(BF16)

    def ex_copy(half, dev):
        blk = recv_ex.at[x, pl.ds(half * rc, rc), :]
        return remote(blk, blk, ex_send.at[half], ex_recv.at[half], dev)

    def ex_all(half):
        return recv_ex.at[pl.ds(0, nx - 1), pl.ds(half * rc, rc), :]

    for half in range(2):
        for d in ring(nx):
            ex_copy(half, {"tp_0": lax.rem(x + d, nx)}).start()

    def residual(half):
        all_received(ex_all(half), ex_send.at[half], ex_recv.at[half])
        at = slice(half * rc, (half + 1) * rc)
        branch = recv_ex[0, at].astype(F32)
        for i in range(1, nx):
            branch = branch + recv_ex[i, at].astype(F32)
        tok = col_n[pl.ds(pl.multiple_of(c * rh + half * rc, rc), rc), :]
        res[kv, at] = (tok.astype(F32) + branch).astype(BF16)

    rows_a, rows_b = pl.ds(0, rc), pl.ds(rc, rc)

    def fa_copy(k, dev):
        blk = res.at[k, rows_a, :]
        return remote(blk, blk, fa_send, fa_recv.at[k], dev)

    def fb_copy(k, dev):
        blk = res.at[k, rows_b, :]
        return remote(blk, blk, fb_send, fb_recv.at[k], dev)

    def y_dev(d):
        return {"kv_1": lax.rem(y + d, ny)}

    def z_dev(d):
        return {"kv_0": lax.rem(z + d, nz)}

    residual(0)
    for d in ring(ny):
        fa_copy(kv, y_dev(d)).start()
    for d in ring(nz):
        fa_copy(kv, z_dev(d)).start()
    residual(1)
    for d in ring(nz):
        fb_copy(kv, z_dev(d)).start()
    for d in ring(ny):
        fb_copy(kv, y_dev(d)).start()

    res_t[...] = res[kv].astype(F32).T.astype(BF16)
    r_copy = remote(
        res_t.at[block(x * nc + other, dt), :], recv_r, r_send, r_recv, partner
    )
    r_copy.start()

    def up(*blocks):
        total, acc = total_sq[...], acc_up[...]
        for j in blocks:
            k = lax.rem(z + nz - j // ny, nz) * ny + lax.rem(y + ny - lax.rem(j, ny), ny)
            at = block(k, dk)
            blk = res[k].astype(F32)
            sq = blk * blk
            for i in range(dk // 128):
                total = total + sq[:, i * 128 : (i + 1) * 128]
            acc = acc + jnp.dot(
                (blk * mlp_gain[:, at]).astype(BF16), w_up[at, :], preferred_element_type=F32
            )
        total_sq[...], acc_up[...] = total, acc

    acc_up[...] = jnp.zeros_like(acc_up)
    total_sq[...] = jnp.zeros_like(total_sq)
    for swap in swaps:
        swap.wait_recv()
    up(0)
    all_sent(d_all, d_send, d_recv)
    e_copy.wait_send()
    for half in range(2):
        all_sent(ex_all(half), ex_send.at[half], ex_recv.at[half])

    for i in range(1, max(ny, nz)):
        if i < ny:
            k = z * ny + lax.rem(y + ny - i, ny)
            fa_copy(k, partner).wait_recv()
            for d in ring(nz):
                fa_copy(k, z_dev(d)).start()
        if i < nz:
            k = lax.rem(z + nz - i, nz) * ny + y
            fb_copy(k, partner).wait_recv()
            for d in ring(ny):
                fb_copy(k, y_dev(d)).start()

    n_late = max((nz - 1) * ny, (ny - 1) * nz)

    def late(i):
        zd, yd = 1 + lax.rem(i, nz - 1), i // (nz - 1)
        k = lax.rem(z + nz - zd, nz) * ny + lax.rem(y + ny - yd, ny)
        fa_copy(k, partner).wait_recv()
        yd, zd = 1 + lax.rem(i, ny - 1), i // (ny - 1)
        k = lax.rem(z + nz - zd, nz) * ny + lax.rem(y + ny - yd, ny)
        fb_copy(k, partner).wait_recv()

    lag = 0
    for j in range(1, nkv):
        zd, yd = j // ny, j % ny
        ready = max(yd * (nz - 1) + zd - 1 if zd else 0, zd * (ny - 1) + yd - 1 if yd else 0)
        lag = max(lag, ready - (j - 1))

    loop(0, lag, late)

    def late_and_up(i):
        late(i)
        up(i - lag + 1)

    loop(lag, n_late, late_and_up)

    up(*range(n_late - lag + 1, nkv))

    scale = lax.rsqrt(jnp.sum(total_sq[...], axis=1, keepdims=True) / width + EPSILON)
    relu = jnp.maximum(acc_up[...] * scale, 0.0)
    hid[...] = (relu * relu).astype(BF16)

    part_a, part_b = pl.ds(0, rc), pl.ds(rc, rc)

    def h1a_copy(dz, k):
        return remote(
            send_h.at[k, part_a, :],
            recv_h1a.at[lax.rem(k, ny), dz - 1],
            h1a_send,
            h1a_recv.at[lax.rem(k, ny)],
            {"kv_0": k // ny},
        )

    def h1b_copy(dy, k):
        return remote(
            send_h.at[k, part_b, :],
            recv_h1b.at[k // ny, dy - 1],
            h1b_send,
            h1b_recv.at[k // ny],
            {"kv_1": lax.rem(k, ny)},
        )

    def down(dz, dy):
        zk, yk = lax.rem(z + dz, nz), lax.rem(y + dy, ny)
        k = zk * ny + yk
        out = jnp.dot(hid[...], w_down[:, block(k, dk)], preferred_element_type=F32)
        send_h[k] = out.astype(BF16)
        if dz:
            h1a_copy(dz, k).start()
        if dy:
            h1b_copy(dy, k).start()

    z_order, y_order = [*ring(nz), 0], [*ring(ny), 0]
    for s in range(max(nz, ny)):
        shell = [(i, s) for i in range(s, nz)] + [(s, i) for i in range(s + 1, ny)]
        for i, j in shell:
            if i < nz and j < ny:
                down(z_order[i], y_order[j])
    all_sent(res.at[pl.ds(0, nkv - 1), rows_a, :], fa_send, fa_recv.at[0])
    all_sent(res.at[pl.ds(0, nkv - 1), rows_b, :], fb_send, fb_recv.at[0])
    for swap in swaps:
        swap.wait_send()
    r_copy.wait_send()

    def h1a_sum(yk):
        acc = send_h[z * ny + yk, 0:rc, :].astype(F32)
        all_received(recv_h1a.at[yk], h1a_send, h1a_recv.at[yk])
        for i in range(nz - 1):
            acc = acc + recv_h1a[yk, i].astype(F32)
        return acc

    def h1b_sum(zk):
        acc = send_h[zk * ny + y, rc : 2 * rc, :].astype(F32)
        all_received(recv_h1b.at[zk], h1b_send, h1b_recv.at[zk])
        for i in range(ny - 1):
            acc = acc + recv_h1b[zk, i].astype(F32)
        return acc

    def h2a_copy(d):
        blk = send_h2a.at[d - 1]
        dev = {"kv_1": lax.rem(y + d, ny)}
        return remote(blk, recv_h2a.at[d - 1], h2_send.at[0], h2_recv.at[0], dev)

    def h2b_copy(d):
        blk = send_h2b.at[d - 1]
        dev = {"kv_0": lax.rem(z + d, nz)}
        return remote(blk, recv_h2b.at[d - 1], h2_send.at[1], h2_recv.at[1], dev)

    for i in range(max(ny, nz) - 1):
        if i < ny - 1:
            d = ring(ny)[i]
            send_h2a[d - 1] = h1a_sum(lax.rem(y + d, ny)).astype(BF16)
            h2a_copy(d).start()
        if i < nz - 1:
            d = ring(nz)[i]
            send_h2b[d - 1] = h1b_sum(lax.rem(z + d, nz)).astype(BF16)
            h2b_copy(d).start()
    sum_a = h1a_sum(y)
    sum_b = h1b_sum(z)
    all_received(recv_h2a, h2_send.at[0], h2_recv.at[0])
    for i in range(ny - 1):
        sum_a = sum_a + recv_h2a[i].astype(F32)
    all_received(recv_h2b, h2_send.at[1], h2_recv.at[1])
    for i in range(nz - 1):
        sum_b = sum_b + recv_h2b[i].astype(F32)

    own_sum = jnp.concatenate([sum_a, sum_b], axis=0).T.astype(BF16)
    send_x[...] = own_sum

    def x_copy(peer):
        blk = send_x.at[block(peer, dt), :]
        return remote(blk, recv_x.at[tp], x_send, x_recv, tp_dev(peer))

    x_all = recv_x.at[pl.ds(0, ntp - 1)]
    for dx, dc in tp_peers():
        x_copy(tp_peer(dx, dc)).start()
    recv_x[tp] = send_x[block(tp, dt), :]

    all_received(x_all, x_send, x_recv)
    r_copy.wait_recv()

    def finish(core, residual):
        total = residual.astype(F32) + recv_x[core].astype(F32)
        for xx in range(1, nx):
            total = total + recv_x[xx * nc + core].astype(F32)
        mixed_ref[:, block(core, rh)] = total.astype(BF16)

    finish(c, res_t[block(tp, dt), :])
    finish(other, recv_r[...])

    all_sent(x_all, x_send, x_recv)
    all_sent(recv_h1a, h1a_send, h1a_recv.at[0])
    all_sent(recv_h1b, h1b_send, h1b_recv.at[0])
    all_sent(recv_h2a, h2_send.at[0], h2_recv.at[0])
    all_sent(recv_h2b, h2_send.at[1], h2_recv.at[1])
    state_out.wait()


def local(
    sizes,
    tokens,
    mix_gain,
    w_query,
    w_key,
    w_value,
    w_gate,
    w_beta,
    w_decay,
    decay_rate,
    out_gain,
    state,
    w_out,
    mlp_gain,
    w_up,
    w_down,
):
    nz, ny, nx, nc = sizes
    nkv, ntp = nz * ny, nx * nc
    rows, dt = tokens.shape
    dk = dt * ntp
    rb, heads, head, _ = state.shape
    proj = heads * head
    sent = 4 * proj + 128
    cols_a, cols_b = 2 * proj, 2 * proj + 128
    n_heads = w_beta.shape[1]
    ff = w_up.shape[1]
    rh = rows // nc
    rc = rh // 2
    vmem, dma = pltpu.VMEM, pltpu.SemaphoreType.DMA
    scratch = [
        vmem((dk, rows), BF16),
        vmem((4, dk, proj), BF16),
        vmem((128, dk), BF16),
        vmem((n_heads, dk), BF16),
        vmem((n_heads, dk), BF16),
        vmem((1, dk), F32),
        vmem((1, head), F32),
        vmem((1, dk * nkv), F32),
        vmem((1, heads), F32),
        vmem(w_out.shape, BF16),
        vmem((w_up.shape[0], 2 * ff), BF16),
        vmem((2 * ff, w_down.shape[1]), BF16),
        vmem(state.shape, F32),
        vmem((rows, dk), BF16),
        vmem((rows, sent), BF16),
        vmem((ny, nz - 1, rb, cols_a), BF16),
        vmem((nz, ny - 1, rb, cols_b), BF16),
        vmem((ny - 1, rb, cols_a), BF16),
        vmem((nz - 1, rb, cols_b), BF16),
        vmem((ny - 1, rb, cols_a), BF16),
        vmem((nz - 1, rb, cols_b), BF16),
        vmem((rb // 4, heads, head, 128), F32),
        vmem((rb // 4, heads, head, 128), F32),
        vmem((6, heads, rb, head), F32),
        vmem((rows, proj), BF16),
        vmem((rh, dk), BF16),
        vmem((rh, dk), BF16),
        vmem((nx, rh, dk), BF16),
        vmem((nkv, rh, dk), BF16),
        vmem((dk, rh), BF16),
        vmem((dt, rh), BF16),
        vmem((rh, 2 * ff), BF16),
        vmem((rh, 2 * ff), F32),
        vmem((rh, 128), F32),
        vmem((nkv, rh, dk), BF16),
        vmem((ny, nz - 1, rc, dk), BF16),
        vmem((nz, ny - 1, rc, dk), BF16),
        vmem((ny - 1, rc, dk), BF16),
        vmem((nz - 1, rc, dk), BF16),
        vmem((ny - 1, rc, dk), BF16),
        vmem((nz - 1, rc, dk), BF16),
        vmem((dk, rh), BF16),
        vmem((ntp, dt, rh), BF16),
        dma((13,)),
        dma(()),
        dma(()),
        dma(()),
        dma(()),
        dma((ny,)),
        dma((nz,)),
        dma((2,)),
        dma((2,)),
        dma(()),
        dma(()),
        dma(()),
        dma(()),
        dma((2,)),
        dma((2,)),
        dma(()),
        dma(()),
        dma((nkv,)),
        dma((nkv,)),
        dma(()),
        dma(()),
        dma((2,)),
        dma((2,)),
        dma(()),
        dma(()),
        dma((ny,)),
        dma((nz,)),
        dma((2,)),
        dma((2,)),
        dma(()),
        dma(()),
    ]
    in_hbm = pl.BlockSpec(memory_space=pl.ANY)
    in_vmem = pl.BlockSpec(memory_space=pltpu.VMEM)
    mixed_t, new_state = pl.pallas_call(
        functools.partial(layer_kernel, sizes),
        out_shape=(
            pltpu.VMEM((dt, rows), BF16),
            pltpu.VMEM(state.shape, F32),
        ),
        in_specs=[in_hbm] * 15,
        out_specs=(in_vmem, in_hbm),
        scratch_shapes=scratch,
        compiler_params=pltpu.CompilerParams(
            collective_id=0, has_side_effects=True, vmem_limit_bytes=63_500_000
        ),
        name="layer",
    )(
        tokens.T,
        mix_gain[None, :],
        w_query,
        w_key,
        w_value,
        w_gate,
        w_beta.T,
        w_decay.T,
        decay_rate[None, :],
        out_gain[None, :],
        state,
        w_out,
        mlp_gain[None, :],
        w_up,
        w_down,
    )
    return mixed_t.T, new_state


def solution(mesh):
    n = dict(mesh.shape)
    sizes = (n["kv"] // 4, 4, n["tp"] // 2, 2) if n["kv"] >= 8 else (2, n["kv"] // 2, n["tp"] // 2, 2)
    torus = Mesh(mesh.devices.reshape(sizes), KV_TP)
    in_specs = (
        P(None, KV_TP),
        P(KV),
        P(KV, TP),
        P(KV, TP),
        P(KV, TP),
        P(KV, TP),
        P(KV, None),
        P(KV, None),
        P(TP),
        P(),
        P(KV, TP, None, None),
        P(TP, KV),
        P(),
        P(None, KV_TP),
        P(KV_TP, None),
    )
    out_specs = (P(None, KV_TP), P(KV, TP, None, None))
    return jax.shard_map(
        functools.partial(local, sizes),
        mesh=torus,
        in_specs=in_specs,
        out_specs=out_specs,
        check_vma=False,
    )
```

time: 72.1 us -> 66.2 us (0.918)
  Pallas kernels: 69 us -> 63.1 us
    pallas_call x1, Pallas kernels: 69 us -> 63.1 us  [local(): pl.pallas_call(functools.partial(layer_kernel, sizes), out_shape=(pltpu.V...]
where the time goes in v4:
time: 66.2 us; the launch traced here: 66 us
  Pallas kernels  63.1 us (95%)
  local copies, waits for them, and re-layouts  2.27 us (3%)
    pallas_call x1, Pallas kernels, local(): pl.pallas_call(functools.partial(layer_kernel, sizes), out_shape=(pltpu.V...  63.1 us
    unnamed x2, local copies, waits for them, and re-layouts  2.27 us

profile of v4, /device:TPU:1, one launch (start us, length us, event | category | flops | bytes accessed | tf_op | source)
XLA Modules:
  0.0 66.0 jit_solution(5776166016394929366)
XLA Ops:
  0.6 63.1 %layer.1 = (bf16[32,256]{1,0:T(8,128)(2,1)S(1)}, f32[16,3,128,128]{3,2,1,0:T(8,128)S(1)}) custom-call(bf16[32,256]{1,0:T(8,128)(2,1)} %bitcast.9, f32[1,256]{1,0:T(1,128)} %bitcast.13, bf16[256,384]{1,0:T(8,128)(2,1)} %wq_ref.1, bf16[256,384]{1,0:T(8,128)(2,1)} %wk_ref.1, bf16[256,384]{1,0:T(8,128)(2,1)} %wv_ref.1, bf16[256,384]{1,0:T(8,128)(2,1)} %wg_ref.1, ...), custom_call_target="tpu_custom_call" | custom-call | tf_op jit(solution)/shard_map/layer/pallas_call | solution.py:802
  63.8 0.6 copy.19
  64.4 1.7 %copy.20 = f32[16,3,128,128]{3,2,1,0:T(8,128)} copy(f32[16,3,128,128]{3,2,1,0:T(8,128)S(1)} %get-tuple-element.7) | data formatting | bytes 6291456

commit v5 on v4

--- a/solution.py
+++ b/solution.py
@@ -55,18 +55,14 @@
     st,
     col_n,
     send_b,
-    recv_b1a,
-    recv_b1b,
-    send_b2a,
-    send_b2b,
-    recv_b2a,
-    recv_b2b,
+    recv_b1,
+    send_b2,
+    recv_b2,
     key_t,
     query_t,
     rows_s,
+    mine,
     merged,
-    send_e,
-    recv_e,
     recv_ex,
     res,
     res_t,
@@ -86,16 +82,12 @@
     local_sem,
     a_send,
     a_recv,
-    b1a_send,
-    b1b_send,
-    b1a_recv,
-    b1b_recv,
+    b1_send,
+    b1_recv,
     b2_send,
     b2_recv,
     d_send,
     d_recv,
-    e_send,
-    e_recv,
     ex_send,
     ex_recv,
     fa_send,
@@ -130,8 +122,6 @@
     proj = heads * head
     rh = rows // nc
     rc = rh // 2
-    cols_a = 2 * proj
-    cols_b = 2 * proj + 128
     other = nc - 1 - c
 
     def kv_dev(k):
@@ -179,7 +169,7 @@
         (out_gain_ref, out_gain),
         (mlp_gain_ref, mlp_gain),
         (state_ref, st),
-        (wout_ref, w_out),
+        (wout_ref, w_out.at[block(c, proj), :]),
         (wup_ref, w_up.at[:, pl.ds(0, ff)]),
         (wdown_ref, w_down.at[pl.ds(0, ff), :]),
     )
@@ -241,33 +231,70 @@
     def project(i):
         return jnp.dot(normed, w_proj[i], preferred_element_type=F32).astype(BF16)
 
-    def b1a_copy(dz, yk):
-        zk = lax.rem(z + dz, nz)
-        return remote(
-            send_b.at[block(zk * ny + yk, rb), pl.ds(0, cols_a)],
-            recv_b1a.at[yk, dz - 1],
-            b1a_send,
-            b1a_recv.at[yk],
-            {"kv_0": zk},
-        )
-
-    def b1b_copy(dy, zk):
-        yk = lax.rem(y + dy, ny)
-        return remote(
-            send_b.at[block(zk * ny + yk, rb), pl.ds(cols_a, cols_b)],
-            recv_b1b.at[zk, dy - 1],
-            b1b_send,
-            b1b_recv.at[zk],
-            {"kv_1": yk},
-        )
-
-    for i in range(2):
-        send_b[:, i * proj : (i + 1) * proj] = project(i)
-
-    for dy in [*ring(ny), 0]:
-        for dz in ring(nz):
-            b1a_copy(dz, lax.rem(y + dy, ny)).start()
-
+    class Reduction:
+        def __init__(self, i, column, columns, z_first):
+            self.i, self.z_first = i, z_first
+            self.n1, self.n2 = (nz, ny) if z_first else (ny, nz)
+            self.at = pl.ds(column, columns)
+            self.recv1, self.send2, self.recv2 = recv_b1[i], send_b2[i], recv_b2[i]
+
+        def place(self, first, second):
+            dz, dy = (first, second) if self.z_first else (second, first)
+            return lax.rem(z + dz, nz), lax.rem(y + dy, ny)
+
+        def rows(self, first, second):
+            zk, yk = self.place(first, second)
+            return send_b.at[block(zk * ny + yk, rb), self.at]
+
+        def start(self):
+            for second in [*ring(self.n2), 0]:
+                for first in ring(self.n1):
+                    zk, yk = self.place(first, second)
+                    line, dev = (yk, {"kv_0": zk}) if self.z_first else (zk, {"kv_1": yk})
+                    remote(
+                        self.rows(first, second),
+                        self.recv1.at[line, first - 1],
+                        b1_send.at[self.i],
+                        b1_recv.at[self.i, line],
+                        dev,
+                    ).start()
+
+        def first_sum(self, second):
+            zk, yk = self.place(0, second)
+            line = yk if self.z_first else zk
+            acc = self.rows(0, second)[...].astype(F32)
+            all_received(self.recv1.at[line], b1_send.at[self.i], b1_recv.at[self.i, line])
+            for k in range(self.n1 - 1):
+                acc = acc + self.recv1[line, k].astype(F32)
+            return acc
+
+        def pass_on(self, second):
+            zk, yk = self.place(0, second)
+            dev = {"kv_1": yk} if self.z_first else {"kv_0": zk}
+            blk = self.send2.at[second - 1]
+            blk[...] = self.first_sum(second).astype(BF16)
+            remote(
+                blk, self.recv2.at[second - 1], b2_send.at[self.i], b2_recv.at[self.i], dev
+            ).start()
+
+        def second_sum(self, acc):
+            all_received(self.recv2, b2_send.at[self.i], b2_recv.at[self.i])
+            for k in range(self.n2 - 1):
+                acc = acc + self.recv2[k].astype(F32)
+            return acc
+
+        def sent(self):
+            all_sent(self.recv1, b1_send.at[self.i], b1_recv.at[self.i, 0])
+            all_sent(self.recv2, b2_send.at[self.i], b2_recv.at[self.i])
+
+    q_end, k_end = proj + 128, 2 * proj + 128
+    for_query = Reduction(0, 0, q_end, True)
+    for_key = Reduction(1, q_end, proj, False)
+    for_value = Reduction(2, k_end, proj, True)
+    for_gate = Reduction(3, k_end + proj, proj, False)
+
+    send_b[:, q_end:k_end] = project(1)
+    for_key.start()
     contract_last = (((1,), (1,)), ((), ()))
     rates_part = lax.dot_general(
         normed, w_rates[...], contract_last, preferred_element_type=F32
@@ -276,78 +303,57 @@
     rates_part = jnp.where(lane == 63, squares, rates_part)
     high = rates_part.astype(BF16).astype(F32)
     low = pltpu.roll(rates_part - high, 64, 1)
-    send_b[:, 4 * proj :] = jnp.where(lane < 64, high, low).astype(BF16)
-    for i in range(2, 4):
-        send_b[:, i * proj : (i + 1) * proj] = project(i)
-
-    for dz in [*ring(nz), 0]:
-        for dy in ring(ny):
-            b1b_copy(dy, lax.rem(z + dz, nz)).start()
-
-    def b1a_sum(yk):
-        acc = send_b[block(z * ny + yk, rb), 0:cols_a].astype(F32)
-        all_received(recv_b1a.at[yk], b1a_send, b1a_recv.at[yk])
-        for i in range(nz - 1):
-            acc = acc + recv_b1a[yk, i].astype(F32)
-        return acc
-
-    def b1b_sum(zk):
-        acc = send_b[block(zk * ny + y, rb), cols_a : cols_a + cols_b].astype(F32)
-        all_received(recv_b1b.at[zk], b1b_send, b1b_recv.at[zk])
-        for i in range(ny - 1):
-            acc = acc + recv_b1b[zk, i].astype(F32)
-        return acc
-
-    def b2a_copy(d):
-        blk = send_b2a.at[d - 1]
-        dev = {"kv_1": lax.rem(y + d, ny)}
-        return remote(blk, recv_b2a.at[d - 1], b2_send.at[0], b2_recv.at[0], dev)
-
-    def b2b_copy(d):
-        blk = send_b2b.at[d - 1]
-        dev = {"kv_0": lax.rem(z + d, nz)}
-        return remote(blk, recv_b2b.at[d - 1], b2_send.at[1], b2_recv.at[1], dev)
-
-    for i in range(max(ny, nz) - 1):
-        if i < ny - 1:
-            d = ring(ny)[i]
-            send_b2a[d - 1] = b1a_sum(lax.rem(y + d, ny)).astype(BF16)
-            b2a_copy(d).start()
-        if i < nz - 1:
-            d = ring(nz)[i]
-            send_b2b[d - 1] = b1b_sum(lax.rem(z + d, nz)).astype(BF16)
-            b2b_copy(d).start()
-    sum_a = b1a_sum(y)
-    sum_b = b1b_sum(z)
-
-    all_received(recv_b2b, b2_send.at[1], b2_recv.at[1])
-    for i in range(nz - 1):
-        sum_b = sum_b + recv_b2b[i].astype(F32)
-    all_received(recv_b2a, b2_send.at[0], b2_recv.at[0])
-    for i in range(ny - 1):
-        sum_a = sum_a + recv_b2a[i].astype(F32)
+    send_b[:, proj:q_end] = jnp.where(lane < 64, high, low).astype(BF16)
+    send_b[:, :proj] = project(0)
+    for_query.start()
+    send_b[:, k_end : k_end + proj] = project(2)
+    for_value.start()
+    send_b[:, k_end + proj :] = project(3)
+    for_gate.start()
+
+    def pass_on_both(by_z, by_y):
+        for i in range(max(ny, nz) - 1):
+            if i < nz - 1:
+                by_y.pass_on(ring(nz)[i])
+            if i < ny - 1:
+                by_z.pass_on(ring(ny)[i])
+        return by_z.first_sum(0), by_y.first_sum(0)
+
+    query_sum, key_sum = pass_on_both(for_query, for_key)
+
+    value_sum, gate_sum = pass_on_both(for_value, for_gate)
+
+    key_sum = for_key.second_sum(key_sum)
+    query_sum = for_query.second_sum(query_sum)
 
     swaps = [
         remote(
-            w_up.at[:, pl.ds(0, ff)],
-            w_up.at[:, pl.ds(ff, ff)],
+            w_out.at[block(c, proj), :],
+            w_out.at[block(c, proj), :],
             swap_send.at[0],
             swap_recv.at[0],
             partner,
         ),
         remote(
-            w_down.at[pl.ds(0, ff), :],
-            w_down.at[pl.ds(ff, ff), :],
+            w_up.at[:, pl.ds(0, ff)],
+            w_up.at[:, pl.ds(ff, ff)],
             swap_send.at[1],
             swap_recv.at[1],
             partner,
         ),
+        remote(
+            w_down.at[pl.ds(0, ff), :],
+            w_down.at[pl.ds(ff, ff), :],
+            swap_send.at[2],
+            swap_recv.at[2],
+            partner,
+        ),
     ]
-    for i in range(2):
-        copies[9 + i].wait()
+    for i in range(3):
+        copies[8 + i].wait()
         swaps[i].start()
 
-    rates = sum_b[:, 2 * proj :]
+    rates = query_sum[:, proj:]
     rates = rates + pltpu.roll(rates, 64, 1)
     lane_b = lax.broadcasted_iota(jnp.int32, rates.shape, 1)
 
@@ -359,7 +365,6 @@
     row_scale = lax.rsqrt(pick(63) / width + EPSILON)
     repeat = 128 // rb
     group = 4
-    gates = []
     for h in range(heads):
         at = slice(h * head, (h + 1) * head)
         beta_raw = pick(tp * heads + h) * row_scale
@@ -367,10 +372,10 @@
         beta = 1.0 / (1.0 + jnp.exp(-beta_raw))
         softplus = jnp.maximum(decay_raw, 0.0) + jnp.log1p(jnp.exp(-jnp.abs(decay_raw)))
         decay = jnp.exp(-rate[0:1, h : h + 1] * softplus)
-        query = silu(sum_a[:, :proj][:, at] * row_scale)
+        query = silu(query_sum[:, at] * row_scale)
         query = query * lax.rsqrt(jnp.sum(query * query, axis=1, keepdims=True) + EPSILON)
         query = query * head ** (-0.5)
-        key = silu(sum_a[:, proj:][:, at] * row_scale)
+        key = silu(key_sum[:, at] * row_scale)
         key = key * lax.rsqrt(jnp.sum(key * key, axis=1, keepdims=True) + EPSILON)
         key_tr = jnp.concatenate([key] * repeat, axis=0).T
         query_tr = jnp.concatenate([query] * repeat, axis=0).T
@@ -380,38 +385,44 @@
         shape = (rb, head)
         rows_s[0, h] = jnp.broadcast_to(decay, shape)
         rows_s[1, h] = jnp.broadcast_to(beta, shape)
-        rows_s[2, h] = silu(sum_b[:, :proj][:, at] * row_scale)
-        rows_s[3, h] = jnp.broadcast_to(
+        rows_s[2, h] = jnp.broadcast_to(
             jnp.sum(key * query, axis=1, keepdims=True), shape
         )
-        gates.append(silu(sum_b[:, proj : 2 * proj][:, at] * row_scale))
 
     def read_group(g):
         for i in range(group):
             b = g * group + i
             for h in range(heads):
                 state = st[b, h]
-                rows_s[4, h, pl.ds(b, 1), :] = jnp.sum(
+                rows_s[3, h, pl.ds(b, 1), :] = jnp.sum(
                     state * key_t[g, h, :, i : i + 1], axis=0, keepdims=True
                 )
-                rows_s[5, h, pl.ds(b, 1), :] = jnp.sum(
+                rows_s[4, h, pl.ds(b, 1), :] = jnp.sum(
                     state * query_t[g, h, :, i : i + 1], axis=0, keepdims=True
                 )
 
     loop(0, rb // group, read_group)
 
-    own_rows = block(kv, rb)
+    value_sum = for_value.second_sum(value_sum)
+    gate_sum = for_gate.second_sum(gate_sum)
     for h in range(heads):
         at = slice(h * head, (h + 1) * head)
         decay = rows_s[0, h]
-        change = rows_s[1, h] * (rows_s[2, h] - decay * rows_s[4, h])
-        read = decay * rows_s[5, h] + rows_s[3, h] * change
-        rows_s[4, h] = change
+        value = silu(value_sum[:, at] * row_scale)
+        change = rows_s[1, h] * (value - decay * rows_s[3, h])
+        read = decay * rows_s[4, h] + rows_s[2, h] * change
+        rows_s[3, h] = change
         scale = lax.rsqrt(jnp.sum(read * read, axis=1, keepdims=True) / head + EPSILON)
-        merged[own_rows, at] = (read * scale * out_gain[...] * gates[h]).astype(BF16)
-
-    d_own = merged.at[own_rows, :]
-    d_all = merged.at[pl.ds(0, (nkv - 1) * rb), :]
+        gate = silu(gate_sum[:, at] * row_scale)
+        mine[:, at] = (read * scale * out_gain[...] * gate).astype(BF16)
+
+    per_half = nkv // nc
+    home = kv // per_half
+    my_rows = block(lax.rem(kv, per_half), rb)
+    slot = merged.at[my_rows, block(c, proj)]
+
+    def d_bytes(n):
+        return send_b.at[pl.ds(0, n * rb), pl.ds(0, proj)]
 
     def hops(d):
         dz, dy = d // ny, d % ny
@@ -421,7 +432,16 @@
         return lax.rem(z + d // ny, nz) * ny + lax.rem(y + d % ny, ny)
 
     for d in sorted(range(1, nkv), key=lambda d: -hops(d)):
-        remote(d_own, d_own, d_send, d_recv, kv_dev(kv_peer(d))).start()
+        dev = {**kv_dev(kv_peer(d)), "tp_1": home}
+        remote(mine, slot, d_send, d_recv, dev).start()
+
+    @pl.when(home != c)
+    def _():
+        remote(mine, slot, d_send, d_recv, {"tp_1": home}).start()
+
+    @pl.when(home == c)
+    def _():
+        merged[my_rows, block(c, proj)] = mine[...]
 
     def write_group(g):
         for i in range(group):
@@ -429,31 +449,25 @@
             for h in range(heads):
                 st[b, h] = (
                     rows_s[0, h, pl.ds(b, 1), :] * st[b, h]
-                    + key_t[g, h, :, i : i + 1] * rows_s[4, h, pl.ds(b, 1), :]
+                    + key_t[g, h, :, i : i + 1] * rows_s[3, h, pl.ds(b, 1), :]
                 )
 
     loop(0, rb // group, write_group)
     state_out = pltpu.make_async_copy(st, new_state_ref, local_sem.at[12])
     state_out.start()
-    copies[8].wait()
-
     all_sent(a_all, a_send, a_recv)
-    all_sent(recv_b1a, b1a_send, b1a_recv.at[0])
-    all_sent(recv_b1b, b1b_send, b1b_recv.at[0])
-    all_sent(recv_b2a, b2_send.at[0], b2_recv.at[0])
-    all_sent(recv_b2b, b2_send.at[1], b2_recv.at[1])
-    all_received(d_all, d_send, d_recv)
-
-    half_other = pl.ds(pl.multiple_of(other * rh, rh), rh)
-    half_own = pl.ds(pl.multiple_of(c * rh, rh), rh)
-    e_copy = remote(send_e, recv_e, e_send, e_recv, partner)
-    send_e[...] = jnp.dot(
-        merged[half_other, :], w_out[...], preferred_element_type=F32
-    ).astype(BF16)
-    e_copy.start()
-    part = jnp.dot(merged[half_own, :], w_out[...], preferred_element_type=F32)
-    e_copy.wait_recv()
-    recv_ex[x] = (part + recv_e[...].astype(F32)).astype(BF16)
+    for reduction in (for_query, for_key, for_value, for_gate):
+        reduction.sent()
+
+    @pl.when(home == c)
+    def _():
+        all_received(d_bytes(nkv - 1), d_send, d_recv)
+
+    @pl.when(home != c)
+    def _():
+        all_received(d_bytes(nkv), d_send, d_recv)
+
+    swaps[0].wait_recv()
 
     def ex_copy(half, dev):
         blk = recv_ex.at[x, pl.ds(half * rc, rc), :]
@@ -463,6 +477,9 @@
         return recv_ex.at[pl.ds(0, nx - 1), pl.ds(half * rc, rc), :]
 
     for half in range(2):
+        at = slice(half * rc, (half + 1) * rc)
+        part = jnp.dot(merged[at, :], w_out[...], preferred_element_type=F32)
+        recv_ex[x, at] = part.astype(BF16)
         for d in ring(nx):
             ex_copy(half, {"tp_0": lax.rem(x + d, nx)}).start()
 
@@ -524,11 +541,18 @@
 
     acc_up[...] = jnp.zeros_like(acc_up)
     total_sq[...] = jnp.zeros_like(total_sq)
-    for swap in swaps:
+    for swap in swaps[1:]:
         swap.wait_recv()
     up(0)
-    all_sent(d_all, d_send, d_recv)
-    e_copy.wait_send()
+
+    @pl.when(home == c)
+    def _():
+        all_sent(d_bytes(nkv - 1), d_send, d_recv)
+
+    @pl.when(home != c)
+    def _():
+        all_sent(d_bytes(nkv), d_send, d_recv)
+
     for half in range(2):
         all_sent(ex_all(half), ex_send.at[half], ex_recv.at[half])
 
@@ -715,7 +739,9 @@
     rb, heads, head, _ = state.shape
     proj = heads * head
     sent = 4 * proj + 128
-    cols_a, cols_b = 2 * proj, 2 * proj + 128
+    reductions = ((proj + 128, True), (proj, False), (proj, True), (proj, False))
+    first = [(ny, nz) if by_z else (nz, ny) for _, by_z in reductions]
+    widths = [w for w, _ in reductions]
     n_heads = w_beta.shape[1]
     ff = w_up.shape[1]
     rh = rows // nc
@@ -731,24 +757,20 @@
         vmem((1, head), F32),
         vmem((1, dk * nkv), F32),
         vmem((1, heads), F32),
-        vmem(w_out.shape, BF16),
+        vmem((nc * proj, dk), BF16),
         vmem((w_up.shape[0], 2 * ff), BF16),
         vmem((2 * ff, w_down.shape[1]), BF16),
         vmem(state.shape, F32),
         vmem((rows, dk), BF16),
         vmem((rows, sent), BF16),
-        vmem((ny, nz - 1, rb, cols_a), BF16),
-        vmem((nz, ny - 1, rb, cols_b), BF16),
-        vmem((ny - 1, rb, cols_a), BF16),
-        vmem((nz - 1, rb, cols_b), BF16),
-        vmem((ny - 1, rb, cols_a), BF16),
-        vmem((nz - 1, rb, cols_b), BF16),
+        [vmem((n2, n1 - 1, rb, w), BF16) for (n2, n1), w in zip(first, widths)],
+        [vmem((n2 - 1, rb, w), BF16) for (n2, n1), w in zip(first, widths)],
+        [vmem((n2 - 1, rb, w), BF16) for (n2, n1), w in zip(first, widths)],
         vmem((rb // 4, heads, head, 128), F32),
         vmem((rb // 4, heads, head, 128), F32),
-        vmem((6, heads, rb, head), F32),
-        vmem((rows, proj), BF16),
-        vmem((rh, dk), BF16),
-        vmem((rh, dk), BF16),
+        vmem((5, heads, rb, head), F32),
+        vmem((rb, proj), BF16),
+        vmem((rh, nc * proj), BF16),
         vmem((nx, rh, dk), BF16),
         vmem((nkv, rh, dk), BF16),
         vmem((dk, rh), BF16),
@@ -768,26 +790,22 @@
         dma((13,)),
         dma(()),
         dma(()),
-        dma(()),
-        dma(()),
-        dma((ny,)),
-        dma((nz,)),
+        dma((4,)),
+        dma((4, max(ny, nz))),
+        dma((4,)),
+        dma((4,)),
+        dma(()),
+        dma(()),
         dma((2,)),
         dma((2,)),
         dma(()),
         dma(()),
-        dma(()),
-        dma(()),
-        dma((2,)),
-        dma((2,)),
-        dma(()),
-        dma(()),
         dma((nkv,)),
         dma((nkv,)),
         dma(()),
         dma(()),
-        dma((2,)),
-        dma((2,)),
+        dma((3,)),
+        dma((3,)),
         dma(()),
         dma(()),
         dma((ny,)),

time: 66.2 us -> 62 us (0.937)
  Pallas kernels: 63.1 us -> 59 us
    pallas_call x1, Pallas kernels: 63.1 us -> 59 us  [local(): pl.pallas_call(functools.partial(layer_kernel, sizes), out_shape=(pltpu.V...]
where the time goes in v5:
time: 62 us; the launch traced here: 61.9 us
  Pallas kernels  59 us (95%)
  local copies, waits for them, and re-layouts  2.27 us (4%)
  between operations  0.64 us (1%)
    pallas_call x1, Pallas kernels, local(): pl.pallas_call(functools.partial(layer_kernel, sizes), out_shape=(pltpu.V...  59 us
    unnamed x2, local copies, waits for them, and re-layouts  2.27 us

profile of v5, /device:TPU:1, one launch (start us, length us, event | category | flops | bytes accessed | tf_op | source)
XLA Modules:
  0.0 61.9 jit_solution(6289912126457795274)
XLA Ops:
  0.6 59.0 %layer.1 = (bf16[32,256]{1,0:T(8,128)(2,1)S(1)}, f32[16,3,128,128]{3,2,1,0:T(8,128)S(1)}) custom-call(bf16[32,256]{1,0:T(8,128)(2,1)} %bitcast.9, f32[1,256]{1,0:T(1,128)} %bitcast.13, bf16[256,384]{1,0:T(8,128)(2,1)} %wq_ref.1, bf16[256,384]{1,0:T(8,128)(2,1)} %wk_ref.1, bf16[256,384]{1,0:T(8,128)(2,1)} %wv_ref.1, bf16[256,384]{1,0:T(8,128)(2,1)} %wg_ref.1, ...), custom_call_target="tpu_custom_call" | custom-call | tf_op jit(solution)/shard_map/layer/pallas_call | solution.py:820
  59.6 0.6 copy.19
  60.2 1.7 %copy.20 = f32[16,3,128,128]{3,2,1,0:T(8,128)} copy(f32[16,3,128,128]{3,2,1,0:T(8,128)S(1)} %get-tuple-element.7) | data formatting | bytes 6291456

commit v6 on v5

--- a/solution.py
+++ b/solution.py
@@ -73,12 +73,10 @@
     send_h,
     recv_h1a,
     recv_h1b,
-    send_h2a,
-    send_h2b,
-    recv_h2a,
-    recv_h2b,
-    send_x,
+    send_xa,
+    send_xb,
     recv_x,
+    bytes_x,
     local_sem,
     a_send,
     a_recv,
@@ -102,8 +100,6 @@
     h1b_send,
     h1a_recv,
     h1b_recv,
-    h2_send,
-    h2_recv,
     x_send,
     x_recv,
 ):
@@ -598,11 +594,12 @@
     relu = jnp.maximum(acc_up[...] * scale, 0.0)
     hid[...] = (relu * relu).astype(BF16)
 
-    part_a, part_b = pl.ds(0, rc), pl.ds(rc, rc)
+    hw = dk // 2
+    part_a, part_b = pl.ds(0, hw), pl.ds(hw, hw)
 
     def h1a_copy(dz, k):
         return remote(
-            send_h.at[k, part_a, :],
+            send_h.at[k, :, part_a],
             recv_h1a.at[lax.rem(k, ny), dz - 1],
             h1a_send,
             h1a_recv.at[lax.rem(k, ny)],
@@ -611,7 +608,7 @@
 
     def h1b_copy(dy, k):
         return remote(
-            send_h.at[k, part_b, :],
+            send_h.at[k, :, part_b],
             recv_h1b.at[k // ny, dy - 1],
             h1b_send,
             h1b_recv.at[k // ny],
@@ -641,77 +638,93 @@
     r_copy.wait_send()
 
     def h1a_sum(yk):
-        acc = send_h[z * ny + yk, 0:rc, :].astype(F32)
+        acc = send_h[z * ny + yk, :, 0:hw].astype(F32)
         all_received(recv_h1a.at[yk], h1a_send, h1a_recv.at[yk])
         for i in range(nz - 1):
             acc = acc + recv_h1a[yk, i].astype(F32)
         return acc
 
     def h1b_sum(zk):
-        acc = send_h[zk * ny + y, rc : 2 * rc, :].astype(F32)
+        acc = send_h[zk * ny + y, :, hw : 2 * hw].astype(F32)
         all_received(recv_h1b.at[zk], h1b_send, h1b_recv.at[zk])
         for i in range(ny - 1):
             acc = acc + recv_h1b[zk, i].astype(F32)
         return acc
 
-    def h2a_copy(d):
-        blk = send_h2a.at[d - 1]
-        dev = {"kv_1": lax.rem(y + d, ny)}
-        return remote(blk, recv_h2a.at[d - 1], h2_send.at[0], h2_recv.at[0], dev)
-
-    def h2b_copy(d):
-        blk = send_h2b.at[d - 1]
-        dev = {"kv_0": lax.rem(z + d, nz)}
-        return remote(blk, recv_h2b.at[d - 1], h2_send.at[1], h2_recv.at[1], dev)
-
-    for i in range(max(ny, nz) - 1):
-        if i < ny - 1:
-            d = ring(ny)[i]
-            send_h2a[d - 1] = h1a_sum(lax.rem(y + d, ny)).astype(BF16)
-            h2a_copy(d).start()
-        if i < nz - 1:
-            d = ring(nz)[i]
-            send_h2b[d - 1] = h1b_sum(lax.rem(z + d, nz)).astype(BF16)
-            h2b_copy(d).start()
-    sum_a = h1a_sum(y)
-    sum_b = h1b_sum(z)
-    all_received(recv_h2a, h2_send.at[0], h2_recv.at[0])
-    for i in range(ny - 1):
-        sum_a = sum_a + recv_h2a[i].astype(F32)
-    all_received(recv_h2b, h2_send.at[1], h2_recv.at[1])
-    for i in range(nz - 1):
-        sum_b = sum_b + recv_h2b[i].astype(F32)
-
-    own_sum = jnp.concatenate([sum_a, sum_b], axis=0).T.astype(BF16)
-    send_x[...] = own_sum
-
-    def x_copy(peer):
-        blk = send_x.at[block(peer, dt), :]
-        return remote(blk, recv_x.at[tp], x_send, x_recv, tp_dev(peer))
-
-    x_all = recv_x.at[pl.ds(0, ntp - 1)]
-    for dx, dc in tp_peers():
-        x_copy(tp_peer(dx, dc)).start()
-    recv_x[tp] = send_x[block(tp, dt), :]
-
-    all_received(x_all, x_send, x_recv)
+    pieces = ntp // 2
+
+    def deliver(d, upper):
+        if upper:
+            total, line, buf = h1b_sum(lax.rem(z + d, nz)), z, send_xb.at[d]
+            dev = {"kv_0": lax.rem(z + d, nz)}
+        else:
+            total, line, buf = h1a_sum(lax.rem(y + d, ny)), y, send_xa.at[d]
+            dev = {"kv_1": lax.rem(y + d, ny)}
+        buf[...] = total.T.astype(BF16)
+        for piece in range(pieces):
+            t = piece + pieces if upper else piece
+            at = pl.ds(piece * dt, dt)
+
+            def send(at=at, t=t):
+                to = {**dev, "tp_0": t // nc, "tp_1": t % nc}
+                remote(buf.at[at], recv_x.at[line, tp], x_send, x_recv, to).start()
+
+            if d:
+                send()
+            else:
+
+                @pl.when(tp != t)
+                def _():
+                    send()
+
+                @pl.when(tp == t)
+                def _():
+                    recv_x[line, tp] = buf[at]
+
+    for i in range(max(ny, nz)):
+        if i < ny:
+            deliver([*ring(ny), 0][i], False)
+        if i < nz:
+            deliver([*ring(nz), 0][i], True)
+
+    def finish(lines):
+        all_received(bytes_x.at[pl.ds(0, lines * ntp - 1)], x_send, x_recv)
+        for core, residual in ((c, res_t[block(tp, dt), :]), (other, recv_r[...])):
+            total = residual.astype(F32)
+            for i in range(lines):
+                for xx in range(nx):
+                    total = total + recv_x[i, xx * nc + core].astype(F32)
+            mixed_ref[:, block(core, rh)] = total.astype(BF16)
+
     r_copy.wait_recv()
 
-    def finish(core, residual):
-        total = residual.astype(F32) + recv_x[core].astype(F32)
-        for xx in range(1, nx):
-            total = total + recv_x[xx * nc + core].astype(F32)
-        mixed_ref[:, block(core, rh)] = total.astype(BF16)
-
-    finish(c, res_t[block(tp, dt), :])
-    finish(other, recv_r[...])
-
-    all_sent(x_all, x_send, x_recv)
+    @pl.when(tp < pieces)
+    def _():
+        finish(ny)
+
+    @pl.when(tp >= pieces)
+    def _():
+        finish(nz)
+
+    all_sent(bytes_x.at[pl.ds(0, (ny + nz) * pieces - 1)], x_send, x_recv)
     all_sent(recv_h1a, h1a_send, h1a_recv.at[0])
     all_sent(recv_h1b, h1b_send, h1b_recv.at[0])
-    all_sent(recv_h2a, h2_send.at[0], h2_recv.at[0])
-    all_sent(recv_h2b, h2_send.at[1], h2_recv.at[1])
     state_out.wait()
+
+
+STORES = 8
+
+
+def store_kernel(mixed_ref, state_ref, mixed_out, state_out, sem):
+    n = state_ref.shape[0] // STORES
+    copies = [pltpu.make_async_copy(mixed_ref, mixed_out, sem.at[0])]
+    for i in range(STORES):
+        at = pl.ds(i * n, n)
+        copies.append(pltpu.make_async_copy(state_ref.at[at], state_out.at[at], sem.at[1 + i]))
+    for copy in copies:
+        copy.start()
+    for copy in copies:
+        copy.wait()
 
 
 def local(
@@ -779,14 +792,12 @@
         vmem((rh, 2 * ff), F32),
         vmem((rh, 128), F32),
         vmem((nkv, rh, dk), BF16),
-        vmem((ny, nz - 1, rc, dk), BF16),
-        vmem((nz, ny - 1, rc, dk), BF16),
-        vmem((ny - 1, rc, dk), BF16),
-        vmem((nz - 1, rc, dk), BF16),
-        vmem((ny - 1, rc, dk), BF16),
-        vmem((nz - 1, rc, dk), BF16),
-        vmem((dk, rh), BF16),
-        vmem((ntp, dt, rh), BF16),
+        vmem((ny, nz - 1, rh, dk // 2), BF16),
+        vmem((nz, ny - 1, rh, dk // 2), BF16),
+        vmem((ny, dk // 2, rh), BF16),
+        vmem((nz, dk // 2, rh), BF16),
+        vmem((max(ny, nz), ntp, dt, rh), BF16),
+        vmem((max(ny, nz) * ntp, dt, rh), BF16),
         dma((13,)),
         dma(()),
         dma(()),
@@ -810,8 +821,6 @@
         dma(()),
         dma((ny,)),
         dma((nz,)),
-        dma((2,)),
-        dma((2,)),
         dma(()),
         dma(()),
     ]
@@ -847,6 +856,18 @@
         w_up,
         w_down,
     )
+    mixed_t, new_state = pl.pallas_call(
+        store_kernel,
+        out_shape=(
+            jax.ShapeDtypeStruct((dt, rows), BF16),
+            jax.ShapeDtypeStruct(state.shape, F32),
+        ),
+        in_specs=[in_hbm] * 2,
+        out_specs=(in_hbm, in_hbm),
+        scratch_shapes=[dma((1 + STORES,))],
+        compiler_params=pltpu.CompilerParams(vmem_limit_bytes=1_000_000),
+        name="store",
+    )(mixed_t, new_state)
     return mixed_t.T, new_state
 
 

time: 62 us -> 59.5 us (0.960)
  local copies, waits for them, and re-layouts: 2.27 us -> 0 us
    unnamed x2 -> x0, local copies, waits for them, and re-layouts: 2.27 us -> none
    pallas_call x1, Pallas kernels: 59 us -> 57 us  [local(): pl.pallas_call(functools.partial(layer_kernel, sizes), out_shape=(pltpu.V...]
    pallas_call x0 -> x1, Pallas kernels: none -> 1.74 us  [local(): pl.pallas_call(store_kernel, out_shape=(jax.ShapeDtypeStruct((dt, rows),...]
where the time goes in v6:
time: 59.5 us; the launch traced here: 59.4 us
  Pallas kernels  58.7 us (99%)
  between operations  0.64 us (1%)
    pallas_call x1, Pallas kernels, local(): pl.pallas_call(functools.partial(layer_kernel, sizes), out_shape=(pltpu.V...  57 us
    pallas_call x1, Pallas kernels, local(): pl.pallas_call(store_kernel, out_shape=(jax.ShapeDtypeStruct((dt, rows),...  1.74 us

profile of v6, /device:TPU:1, one launch (start us, length us, event | category | flops | bytes accessed | tf_op | source)
XLA Modules:
  0.0 59.4 jit_solution(4063041986817744719)
XLA Ops:
  0.6 57.0 %layer.1 = (bf16[32,256]{1,0:T(8,128)(2,1)S(1)}, f32[16,3,128,128]{3,2,1,0:T(8,128)S(1)}) custom-call(bf16[32,256]{1,0:T(8,128)(2,1)} %bitcast.8, f32[1,256]{1,0:T(1,128)} %bitcast.12, bf16[256,384]{1,0:T(8,128)(2,1)} %wq_ref.1, bf16[256,384]{1,0:T(8,128)(2,1)} %wk_ref.1, bf16[256,384]{1,0:T(8,128)(2,1)} %wv_ref.1, bf16[256,384]{1,0:T(8,128)(2,1)} %wg_ref.1, ...), custom_call_target="tpu_custom_call" | custom-call | tf_op jit(solution)/shard_map/layer/pallas_call | solution.py:829
  57.6 1.7 %store.1 = (bf16[32,256]{1,0:T(8,128)(2,1)}, f32[16,3,128,128]{3,2,1,0:T(8,128)}) custom-call(bf16[32,256]{1,0:T(8,128)(2,1)S(1)} %get-tuple-element.6.mixed_ref, f32[16,3,128,128]{3,2,1,0:T(8,128)S(1)} %get-tuple-element.7.state_ref), custom_call_target="tpu_custom_call" | custom-call | tf_op jit(solution)/shard_map/store/pallas_call | solution.py:859

commit v7 on v6

--- a/solution.py
+++ b/solution.py
@@ -43,6 +43,7 @@
     col_t,
     w_proj,
     w_rates,
+    perm,
     w_beta,
     w_decay,
     mix_gain,
@@ -155,6 +156,20 @@
     def block(i, n):
         return pl.ds(pl.multiple_of(i * n, n), n)
 
+    barrier = pltpu.get_barrier_semaphore()
+
+    def greet(dev):
+        pl.semaphore_signal(barrier, inc=1, device_id=dev, device_id_type=MESH)
+
+    for dx in range(nx):
+        for dc in range(nc):
+            if dx or dc:
+                greet({"tp_0": lax.rem(x + dx, nx), "tp_1": lax.rem(c + dc, nc)})
+    for d in range(1, ny):
+        greet({"kv_1": lax.rem(y + d, ny)})
+    for d in range(1, nz):
+        greet({"kv_0": lax.rem(z + d, nz)})
+
     own_tok = col_t.at[block(tp, dt), :]
     first = (
         (tok_ref, own_tok),
@@ -179,26 +194,18 @@
     for copy in copies[4:]:
         copy.start()
 
-    barrier = pltpu.get_barrier_semaphore()
-
-    def greet(dev):
-        pl.semaphore_signal(barrier, inc=1, device_id=dev, device_id_type=MESH)
-
-    def greet_tp(d):
-        greet(tp_dev(lax.rem(tp + d, ntp)))
-
-    loop(1, ntp, greet_tp)
-    for d in range(1, ny):
-        greet({"kv_1": lax.rem(y + d, ny)})
-    for d in range(1, nz):
-        greet({"kv_0": lax.rem(z + d, nz)})
-
     n_heads = wbeta_ref.shape[0]
     copies[1].wait()
     copies[2].wait()
     w_rates[...] = jnp.zeros_like(w_rates)
     w_rates[0:n_heads, :] = w_beta[...]
     w_rates[32 : 32 + n_heads, :] = w_decay[...]
+
+    width_x = nx * dt
+    column = lax.broadcasted_iota(jnp.int32, (dk, dk), 1)
+    source = (lax.rem(column, width_x) // dt * nc + column // width_x) * dt + lax.rem(column, dt)
+    row = lax.broadcasted_iota(jnp.int32, (dk, dk), 0)
+    perm[...] = jnp.where(row == source, 1.0, 0.0).astype(BF16)
 
     copies[0].wait()
     copies[3].wait()
@@ -306,6 +313,14 @@
     for_value.start()
     send_b[:, k_end + proj :] = project(3)
     for_gate.start()
+
+    copies[10].wait()
+
+    def reorder(k):
+        at = (pl.ds(0, ff), block(k, dk))
+        w_down[at] = jnp.dot(w_down[at], perm[...], preferred_element_type=F32).astype(BF16)
+
+    loop(0, nkv, reorder)
 
     def pass_on_both(by_z, by_y):
         for i in range(max(ny, nz) - 1):
@@ -345,9 +360,10 @@
             partner,
         ),
     ]
-    for i in range(3):
-        copies[8 + i].wait()
-        swaps[i].start()
+    copies[8].wait()
+    copies[9].wait()
+    for swap in swaps:
+        swap.start()
 
     rates = query_sum[:, proj:]
     rates = rates + pltpu.roll(rates, 64, 1)
@@ -360,7 +376,7 @@
         copies[i].wait()
     row_scale = lax.rsqrt(pick(63) / width + EPSILON)
     repeat = 128 // rb
-    group = 4
+    group = 8
     for h in range(heads):
         at = slice(h * head, (h + 1) * head)
         beta_raw = pick(tp * heads + h) * row_scale
@@ -413,7 +429,7 @@
         mine[:, at] = (read * scale * out_gain[...] * gate).astype(BF16)
 
     per_half = nkv // nc
-    home = kv // per_half
+    keeper = kv // per_half
     my_rows = block(lax.rem(kv, per_half), rb)
     slot = merged.at[my_rows, block(c, proj)]
 
@@ -428,14 +444,14 @@
         return lax.rem(z + d // ny, nz) * ny + lax.rem(y + d % ny, ny)
 
     for d in sorted(range(1, nkv), key=lambda d: -hops(d)):
-        dev = {**kv_dev(kv_peer(d)), "tp_1": home}
+        dev = {**kv_dev(kv_peer(d)), "tp_1": keeper}
         remote(mine, slot, d_send, d_recv, dev).start()
 
-    @pl.when(home != c)
+    @pl.when(keeper != c)
     def _():
-        remote(mine, slot, d_send, d_recv, {"tp_1": home}).start()
-
-    @pl.when(home == c)
+        remote(mine, slot, d_send, d_recv, {"tp_1": keeper}).start()
+
+    @pl.when(keeper == c)
     def _():
         merged[my_rows, block(c, proj)] = mine[...]
 
@@ -455,11 +471,11 @@
     for reduction in (for_query, for_key, for_value, for_gate):
         reduction.sent()
 
-    @pl.when(home == c)
+    @pl.when(keeper == c)
     def _():
         all_received(d_bytes(nkv - 1), d_send, d_recv)
 
-    @pl.when(home != c)
+    @pl.when(keeper != c)
     def _():
         all_received(d_bytes(nkv), d_send, d_recv)
 
@@ -490,13 +506,31 @@
 
     rows_a, rows_b = pl.ds(0, rc), pl.ds(rc, rc)
 
-    def fa_copy(k, dev):
+    y_arrival, z_arrival = [0, *ring(ny)[::-1]], [0, *ring(nz)[::-1]]
+    y_last, z_last = y_arrival[-1], z_arrival[-1]
+
+    def fa_copy(k, sem, dev):
         blk = res.at[k, rows_a, :]
-        return remote(blk, blk, fa_send, fa_recv.at[k], dev)
-
-    def fb_copy(k, dev):
+        return remote(blk, blk, fa_send, fa_recv.at[sem], dev)
+
+    def fb_copy(k, sem, dev):
         blk = res.at[k, rows_b, :]
-        return remote(blk, blk, fb_send, fb_recv.at[k], dev)
+        return remote(blk, blk, fb_send, fb_recv.at[sem], dev)
+
+    def near_a(d):
+        return d - 1
+
+    def near_b(d):
+        return d - 1
+
+    def late_a(dy, dz):
+        return ny - 1 + (ny - 1 + dz if dy == y_last else y_arrival.index(dy))
+
+    def late_b(dz, dy):
+        return nz - 1 + (nz - 1 + dy if dz == z_last else z_arrival.index(dz))
+
+    def home(dz, dy):
+        return lax.rem(z + nz - dz, nz) * ny + lax.rem(y + ny - dy, ny)
 
     def y_dev(d):
         return {"kv_1": lax.rem(y + d, ny)}
@@ -506,14 +540,14 @@
 
     residual(0)
     for d in ring(ny):
-        fa_copy(kv, y_dev(d)).start()
+        fa_copy(kv, near_a(d), y_dev(d)).start()
     for d in ring(nz):
-        fa_copy(kv, z_dev(d)).start()
+        fa_copy(kv, late_a(0, d), z_dev(d)).start()
     residual(1)
     for d in ring(nz):
-        fb_copy(kv, z_dev(d)).start()
+        fb_copy(kv, near_b(d), z_dev(d)).start()
     for d in ring(ny):
-        fb_copy(kv, y_dev(d)).start()
+        fb_copy(kv, late_b(0, d), y_dev(d)).start()
 
     res_t[...] = res[kv].astype(F32).T.astype(BF16)
     r_copy = remote(
@@ -523,8 +557,8 @@
 
     def up(*blocks):
         total, acc = total_sq[...], acc_up[...]
-        for j in blocks:
-            k = lax.rem(z + nz - j // ny, nz) * ny + lax.rem(y + ny - lax.rem(j, ny), ny)
+        for dz, dy in blocks:
+            k = home(dz, dy)
             at = block(k, dk)
             blk = res[k].astype(F32)
             sq = blk * blk
@@ -539,13 +573,13 @@
     total_sq[...] = jnp.zeros_like(total_sq)
     for swap in swaps[1:]:
         swap.wait_recv()
-    up(0)
-
-    @pl.when(home == c)
+    up((0, 0))
+
+    @pl.when(keeper == c)
     def _():
         all_sent(d_bytes(nkv - 1), d_send, d_recv)
 
-    @pl.when(home != c)
+    @pl.when(keeper != c)
     def _():
         all_sent(d_bytes(nkv), d_send, d_recv)
 
@@ -554,41 +588,50 @@
 
     for i in range(1, max(ny, nz)):
         if i < ny:
-            k = z * ny + lax.rem(y + ny - i, ny)
-            fa_copy(k, partner).wait_recv()
+            dy = y_arrival[i]
+            fa_copy(home(0, dy), near_a(dy), partner).wait_recv()
             for d in ring(nz):
-                fa_copy(k, z_dev(d)).start()
+                fa_copy(home(0, dy), late_a(dy, d), z_dev(d)).start()
         if i < nz:
-            k = lax.rem(z + nz - i, nz) * ny + y
-            fb_copy(k, partner).wait_recv()
+            dz = z_arrival[i]
+            fb_copy(home(dz, 0), near_b(dz), partner).wait_recv()
             for d in ring(ny):
-                fb_copy(k, y_dev(d)).start()
-
-    n_late = max((nz - 1) * ny, (ny - 1) * nz)
-
-    def late(i):
-        zd, yd = 1 + lax.rem(i, nz - 1), i // (nz - 1)
-        k = lax.rem(z + nz - zd, nz) * ny + lax.rem(y + ny - yd, ny)
-        fa_copy(k, partner).wait_recv()
-        yd, zd = 1 + lax.rem(i, ny - 1), i // (ny - 1)
-        k = lax.rem(z + nz - zd, nz) * ny + lax.rem(y + ny - yd, ny)
-        fb_copy(k, partner).wait_recv()
-
-    lag = 0
-    for j in range(1, nkv):
-        zd, yd = j // ny, j % ny
-        ready = max(yd * (nz - 1) + zd - 1 if zd else 0, zd * (ny - 1) + yd - 1 if yd else 0)
-        lag = max(lag, ready - (j - 1))
-
-    loop(0, lag, late)
-
-    def late_and_up(i):
-        late(i)
-        up(i - lag + 1)
-
-    loop(lag, n_late, late_and_up)
-
-    up(*range(n_late - lag + 1, nkv))
+                fb_copy(home(dz, 0), late_b(dz, d), y_dev(d)).start()
+
+    got_a = {(0, dy) for dy in range(ny)}
+    got_b = {(dz, 0) for dz in range(nz)}
+    done = {(0, 0)}
+
+    def up_ready():
+        ready = sorted((got_a & got_b) - done)
+        done.update(ready)
+        for i in range(0, len(ready), 2):
+            up(*ready[i : i + 2])
+
+    for i in range(max(ny, nz)):
+        if i < ny - 1:
+            dy = y_arrival[i]
+            all_received(
+                res.at[pl.ds(0, nz - 1), rows_a, :], fa_send, fa_recv.at[late_a(dy, 1)]
+            )
+            got_a |= {(dz, dy) for dz in range(1, nz)}
+        if i < nz - 1:
+            dz = z_arrival[i]
+            all_received(
+                res.at[pl.ds(0, ny - 1), rows_b, :], fb_send, fb_recv.at[late_b(dz, 1)]
+            )
+            got_b |= {(dz, dy) for dy in range(1, ny)}
+        up_ready()
+    for i in range(1, max(ny, nz)):
+        if i < nz:
+            dz = z_arrival[i]
+            fa_copy(home(dz, y_last), late_a(y_last, dz), partner).wait_recv()
+            got_a.add((dz, y_last))
+        if i < ny:
+            dy = y_arrival[i]
+            fb_copy(home(z_last, dy), late_b(z_last, dy), partner).wait_recv()
+            got_b.add((z_last, dy))
+        up_ready()
 
     scale = lax.rsqrt(jnp.sum(total_sq[...], axis=1, keepdims=True) / width + EPSILON)
     relu = jnp.maximum(acc_up[...] * scale, 0.0)
@@ -651,41 +694,39 @@
             acc = acc + recv_h1b[zk, i].astype(F32)
         return acc
 
-    pieces = ntp // 2
-
-    def deliver(d, upper):
-        if upper:
+    def deliver(d, core):
+        if core:
             total, line, buf = h1b_sum(lax.rem(z + d, nz)), z, send_xb.at[d]
-            dev = {"kv_0": lax.rem(z + d, nz)}
+            dev = {"kv_0": lax.rem(z + d, nz), "tp_1": core}
         else:
             total, line, buf = h1a_sum(lax.rem(y + d, ny)), y, send_xa.at[d]
-            dev = {"kv_1": lax.rem(y + d, ny)}
+            dev = {"kv_1": lax.rem(y + d, ny), "tp_1": core}
         buf[...] = total.T.astype(BF16)
-        for piece in range(pieces):
-            t = piece + pieces if upper else piece
-            at = pl.ds(piece * dt, dt)
-
-            def send(at=at, t=t):
-                to = {**dev, "tp_0": t // nc, "tp_1": t % nc}
+        for dx in [*ring(nx), 0]:
+            to_x = lax.rem(x + dx, nx)
+            at = block(to_x, dt)
+
+            def send(at=at, to_x=to_x):
+                to = {**dev, "tp_0": to_x}
                 remote(buf.at[at], recv_x.at[line, tp], x_send, x_recv, to).start()
 
-            if d:
+            if d or dx:
                 send()
             else:
 
-                @pl.when(tp != t)
+                @pl.when(c != core)
                 def _():
                     send()
 
-                @pl.when(tp == t)
+                @pl.when(c == core)
                 def _():
                     recv_x[line, tp] = buf[at]
 
     for i in range(max(ny, nz)):
         if i < ny:
-            deliver([*ring(ny), 0][i], False)
+            deliver([*ring(ny), 0][i], 0)
         if i < nz:
-            deliver([*ring(nz), 0][i], True)
+            deliver([*ring(nz), 0][i], 1)
 
     def finish(lines):
         all_received(bytes_x.at[pl.ds(0, lines * ntp - 1)], x_send, x_recv)
@@ -698,15 +739,15 @@
 
     r_copy.wait_recv()
 
-    @pl.when(tp < pieces)
+    @pl.when(c == 0)
     def _():
         finish(ny)
 
-    @pl.when(tp >= pieces)
+    @pl.when(c == 1)
     def _():
         finish(nz)
 
-    all_sent(bytes_x.at[pl.ds(0, (ny + nz) * pieces - 1)], x_send, x_recv)
+    all_sent(bytes_x.at[pl.ds(0, (ny + nz) * nx - 1)], x_send, x_recv)
     all_sent(recv_h1a, h1a_send, h1a_recv.at[0])
     all_sent(recv_h1b, h1b_send, h1b_recv.at[0])
     state_out.wait()
@@ -764,6 +805,7 @@
         vmem((dk, rows), BF16),
         vmem((4, dk, proj), BF16),
         vmem((128, dk), BF16),
+        vmem((dk, dk), BF16),
         vmem((n_heads, dk), BF16),
         vmem((n_heads, dk), BF16),
         vmem((1, dk), F32),
@@ -779,8 +821,8 @@
         [vmem((n2, n1 - 1, rb, w), BF16) for (n2, n1), w in zip(first, widths)],
         [vmem((n2 - 1, rb, w), BF16) for (n2, n1), w in zip(first, widths)],
         [vmem((n2 - 1, rb, w), BF16) for (n2, n1), w in zip(first, widths)],
-        vmem((rb // 4, heads, head, 128), F32),
-        vmem((rb // 4, heads, head, 128), F32),
+        vmem((rb // 8, heads, head, 128), F32),
+        vmem((rb // 8, heads, head, 128), F32),
         vmem((5, heads, rb, head), F32),
         vmem((rb, proj), BF16),
         vmem((rh, nc * proj), BF16),
@@ -811,8 +853,8 @@
         dma((2,)),
         dma(()),
         dma(()),
-        dma((nkv,)),
-        dma((nkv,)),
+        dma((2 * (ny - 1) + nz,)),
+        dma((2 * (nz - 1) + ny,)),
         dma(()),
         dma(()),
         dma((3,)),

time: 59.5 us -> 59.1 us (level)
  no operation moved by 1% of the time
where the time goes in v7:
time: 59.1 us; the launch traced here: 58.9 us
  Pallas kernels  58.3 us (99%)
  between operations  0.64 us (1%)
    pallas_call x1, Pallas kernels, local(): pl.pallas_call(functools.partial(layer_kernel, sizes), out_shape=(pltpu.V...  56.6 us
    pallas_call x1, Pallas kernels, local(): pl.pallas_call(store_kernel, out_shape=(jax.ShapeDtypeStruct((dt, rows),...  1.74 us

profile of v7, /device:TPU:1, one launch (start us, length us, event | category | flops | bytes accessed | tf_op | source)
XLA Modules:
  0.0 58.9 jit_solution(8220425999442737986)
XLA Ops:
  0.6 56.6 %layer.1 = (bf16[32,256]{1,0:T(8,128)(2,1)S(1)}, f32[16,3,128,128]{3,2,1,0:T(8,128)S(1)}) custom-call(bf16[32,256]{1,0:T(8,128)(2,1)} %bitcast.8, f32[1,256]{1,0:T(1,128)} %bitcast.12, bf16[256,384]{1,0:T(8,128)(2,1)} %wq_ref.1, bf16[256,384]{1,0:T(8,128)(2,1)} %wk_ref.1, bf16[256,384]{1,0:T(8,128)(2,1)} %wv_ref.1, bf16[256,384]{1,0:T(8,128)(2,1)} %wg_ref.1, ...), custom_call_target="tpu_custom_call" | custom-call | tf_op jit(solution)/shard_map/layer/pallas_call | solution.py:871
  57.2 1.7 %store.1 = (bf16[32,256]{1,0:T(8,128)(2,1)}, f32[16,3,128,128]{3,2,1,0:T(8,128)}) custom-call(bf16[32,256]{1,0:T(8,128)(2,1)S(1)} %get-tuple-element.6.mixed_ref, f32[16,3,128,128]{3,2,1,0:T(8,128)S(1)} %get-tuple-element.7.state_ref), custom_call_target="tpu_custom_call" | custom-call | tf_op jit(solution)/shard_map/store/pallas_call | solution.py:901

commit v8 on v7

--- a/solution.py
+++ b/solution.py
@@ -60,7 +60,9 @@
     send_b2,
     recv_b2,
     key_t,
-    query_t,
+    key_s,
+    lhs_s,
+    st_terms,
     rows_s,
     mine,
     merged,
@@ -322,6 +324,22 @@
 
     loop(0, nkv, reorder)
 
+    copies[7].wait()
+
+    def split(x):
+        high = x.astype(BF16)
+        return high, (x - high.astype(F32)).astype(BF16)
+
+    def split_state(g):
+        for h in range(heads):
+            for i in range(2):
+                high, low = split(st[2 * g + i, h])
+                at = slice(i * head, (i + 1) * head)
+                st_terms[g, h, :head, at] = high
+                st_terms[g, h, head:, at] = low
+
+    loop(0, rb // 2, split_state)
+
     def pass_on_both(by_z, by_y):
         for i in range(max(ny, nz) - 1):
             if i < nz - 1:
@@ -372,11 +390,9 @@
     def pick(i):
         return jnp.sum(jnp.where(lane_b == i, rates, 0.0), axis=1, keepdims=True)
 
-    for i in range(4, 8):
+    for i in range(4, 7):
         copies[i].wait()
     row_scale = lax.rsqrt(pick(63) / width + EPSILON)
-    repeat = 128 // rb
-    group = 8
     for h in range(heads):
         at = slice(h * head, (h + 1) * head)
         beta_raw = pick(tp * heads + h) * row_scale
@@ -389,11 +405,9 @@
         query = query * head ** (-0.5)
         key = silu(key_sum[:, at] * row_scale)
         key = key * lax.rsqrt(jnp.sum(key * key, axis=1, keepdims=True) + EPSILON)
-        key_tr = jnp.concatenate([key] * repeat, axis=0).T
-        query_tr = jnp.concatenate([query] * repeat, axis=0).T
-        for g in range(rb // group):
-            key_t[g, h] = pltpu.roll(key_tr, (128 - g * group) % 128, 1) if g else key_tr
-            query_t[g, h] = pltpu.roll(query_tr, (128 - g * group) % 128, 1) if g else query_tr
+        key_s[h] = key
+        terms = jnp.concatenate([*split(key), *split(query)], axis=0)
+        lhs_s[h] = jnp.concatenate([terms, terms], axis=1)
         shape = (rb, head)
         rows_s[0, h] = jnp.broadcast_to(decay, shape)
         rows_s[1, h] = jnp.broadcast_to(beta, shape)
@@ -401,19 +415,27 @@
             jnp.sum(key * query, axis=1, keepdims=True), shape
         )
 
-    def read_group(g):
-        for i in range(group):
-            b = g * group + i
-            for h in range(heads):
-                state = st[b, h]
-                rows_s[3, h, pl.ds(b, 1), :] = jnp.sum(
-                    state * key_t[g, h, :, i : i + 1], axis=0, keepdims=True
-                )
-                rows_s[4, h, pl.ds(b, 1), :] = jnp.sum(
-                    state * query_t[g, h, :, i : i + 1], axis=0, keepdims=True
-                )
-
-    loop(0, rb // group, read_group)
+    row = lax.broadcasted_iota(jnp.int32, (rb, head), 0)
+
+    def read_pair(g, sums):
+        out = []
+        for h in range(heads):
+            got = jnp.dot(lhs_s[h], st_terms[g, h], preferred_element_type=F32)
+            for k in range(2):
+                both = got[2 * k * rb : (2 * k + 1) * rb] + got[(2 * k + 1) * rb : (2 * k + 2) * rb]
+                acc = sums[2 * h + k]
+                for i in range(2):
+                    acc = jnp.where(row == 2 * g + i, both[:, i * head : (i + 1) * head], acc)
+                out.append(acc)
+        return out
+
+    def read_pairs(g, sums):
+        for i in range(2):
+            sums = read_pair(2 * g + i, sums)
+        return sums
+
+    zero = jnp.zeros((rb, head), F32)
+    read_sums = lax.fori_loop(0, rb // 4, read_pairs, [zero] * (2 * heads))
 
     value_sum = for_value.second_sum(value_sum)
     gate_sum = for_gate.second_sum(gate_sum)
@@ -421,8 +443,8 @@
         at = slice(h * head, (h + 1) * head)
         decay = rows_s[0, h]
         value = silu(value_sum[:, at] * row_scale)
-        change = rows_s[1, h] * (value - decay * rows_s[3, h])
-        read = decay * rows_s[4, h] + rows_s[2, h] * change
+        change = rows_s[1, h] * (value - decay * read_sums[2 * h])
+        read = decay * read_sums[2 * h + 1] + rows_s[2, h] * change
         rows_s[3, h] = change
         scale = lax.rsqrt(jnp.sum(read * read, axis=1, keepdims=True) / head + EPSILON)
         gate = silu(gate_sum[:, at] * row_scale)
@@ -454,6 +476,12 @@
     @pl.when(keeper == c)
     def _():
         merged[my_rows, block(c, proj)] = mine[...]
+
+    group, repeat = 8, 128 // rb
+    for h in range(heads):
+        key_tr = jnp.concatenate([key_s[h]] * repeat, axis=0).T
+        for g in range(rb // group):
+            key_t[g, h] = pltpu.roll(key_tr, (128 - g * group) % 128, 1) if g else key_tr
 
     def write_group(g):
         for i in range(group):
@@ -509,25 +537,30 @@
     y_arrival, z_arrival = [0, *ring(ny)[::-1]], [0, *ring(nz)[::-1]]
     y_last, z_last = y_arrival[-1], z_arrival[-1]
 
-    def fa_copy(k, sem, dev):
-        blk = res.at[k, rows_a, :]
+    rq = rc // 2
+
+    def part_of(base, part):
+        return pl.ds(base, rc) if part is None else pl.ds(base + part * rq, rq)
+
+    def fa_copy(k, sem, dev, part=None):
+        blk = res.at[k, part_of(0, part), :]
         return remote(blk, blk, fa_send, fa_recv.at[sem], dev)
 
-    def fb_copy(k, sem, dev):
-        blk = res.at[k, rows_b, :]
+    def fb_copy(k, sem, dev, part=None):
+        blk = res.at[k, part_of(rc, part), :]
         return remote(blk, blk, fb_send, fb_recv.at[sem], dev)
 
-    def near_a(d):
-        return d - 1
-
-    def near_b(d):
-        return d - 1
+    def near_a(d, part):
+        return part * (ny - 1) + d - 1
+
+    def near_b(d, part):
+        return part * (nz - 1) + d - 1
 
     def late_a(dy, dz):
-        return ny - 1 + (ny - 1 + dz if dy == y_last else y_arrival.index(dy))
+        return 2 * (ny - 1) + (ny - 1 + dz if dy == y_last else y_arrival.index(dy))
 
     def late_b(dz, dy):
-        return nz - 1 + (nz - 1 + dy if dz == z_last else z_arrival.index(dz))
+        return 2 * (nz - 1) + (nz - 1 + dy if dz == z_last else z_arrival.index(dz))
 
     def home(dz, dy):
         return lax.rem(z + nz - dz, nz) * ny + lax.rem(y + ny - dy, ny)
@@ -539,13 +572,15 @@
         return {"kv_0": lax.rem(z + d, nz)}
 
     residual(0)
-    for d in ring(ny):
-        fa_copy(kv, near_a(d), y_dev(d)).start()
+    for part in range(2):
+        for d in ring(ny):
+            fa_copy(kv, near_a(d, part), y_dev(d), part).start()
     for d in ring(nz):
         fa_copy(kv, late_a(0, d), z_dev(d)).start()
     residual(1)
-    for d in ring(nz):
-        fb_copy(kv, near_b(d), z_dev(d)).start()
+    for part in range(2):
+        for d in ring(nz):
+            fb_copy(kv, near_b(d, part), z_dev(d), part).start()
     for d in ring(ny):
         fb_copy(kv, late_b(0, d), y_dev(d)).start()
 
@@ -586,17 +621,18 @@
     for half in range(2):
         all_sent(ex_all(half), ex_send.at[half], ex_recv.at[half])
 
-    for i in range(1, max(ny, nz)):
-        if i < ny:
-            dy = y_arrival[i]
-            fa_copy(home(0, dy), near_a(dy), partner).wait_recv()
-            for d in ring(nz):
-                fa_copy(home(0, dy), late_a(dy, d), z_dev(d)).start()
-        if i < nz:
-            dz = z_arrival[i]
-            fb_copy(home(dz, 0), near_b(dz), partner).wait_recv()
-            for d in ring(ny):
-                fb_copy(home(dz, 0), late_b(dz, d), y_dev(d)).start()
+    for part in range(2):
+        for i in range(1, max(ny, nz)):
+            if i < ny:
+                dy = y_arrival[i]
+                fa_copy(home(0, dy), near_a(dy, part), partner, part).wait_recv()
+                for d in ring(nz):
+                    fa_copy(home(0, dy), late_a(dy, d), z_dev(d), part).start()
+            if i < nz:
+                dz = z_arrival[i]
+                fb_copy(home(dz, 0), near_b(dz, part), partner, part).wait_recv()
+                for d in ring(ny):
+                    fb_copy(home(dz, 0), late_b(dz, d), y_dev(d), part).start()
 
     got_a = {(0, dy) for dy in range(ny)}
     got_b = {(dz, 0) for dz in range(nz)}
@@ -753,7 +789,7 @@
     state_out.wait()
 
 
-STORES = 8
+STORES = 4
 
 
 def store_kernel(mixed_ref, state_ref, mixed_out, state_out, sem):
@@ -822,8 +858,10 @@
         [vmem((n2 - 1, rb, w), BF16) for (n2, n1), w in zip(first, widths)],
         [vmem((n2 - 1, rb, w), BF16) for (n2, n1), w in zip(first, widths)],
         vmem((rb // 8, heads, head, 128), F32),
-        vmem((rb // 8, heads, head, 128), F32),
-        vmem((5, heads, rb, head), F32),
+        vmem((heads, rb, head), F32),
+        vmem((heads, 4 * rb, 2 * head), BF16),
+        vmem((rb // 2, heads, 2 * head, 2 * head), BF16),
+        vmem((4, heads, rb, head), F32),
         vmem((rb, proj), BF16),
         vmem((rh, nc * proj), BF16),
         vmem((nx, rh, dk), BF16),
@@ -853,8 +891,8 @@
         dma((2,)),
         dma(()),
         dma(()),
-        dma((2 * (ny - 1) + nz,)),
-        dma((2 * (nz - 1) + ny,)),
+        dma((3 * (ny - 1) + nz,)),
+        dma((3 * (nz - 1) + ny,)),
         dma(()),
         dma(()),
         dma((3,)),

time: 59.1 us -> 57.4 us (0.971)
  Pallas kernels: 58.3 us -> 56.6 us
    pallas_call x1, Pallas kernels: 56.6 us -> 54.9 us  [local(): pl.pallas_call(functools.partial(layer_kernel, sizes), out_shape=(pltpu.V...]
where the time goes in v8:
time: 57.4 us; the launch traced here: 57.3 us
  Pallas kernels  56.6 us (99%)
  between operations  0.64 us (1%)
    pallas_call x1, Pallas kernels, local(): pl.pallas_call(functools.partial(layer_kernel, sizes), out_shape=(pltpu.V...  54.9 us
    pallas_call x1, Pallas kernels, local(): pl.pallas_call(store_kernel, out_shape=(jax.ShapeDtypeStruct((dt, rows),...  1.71 us

profile of v8, /device:TPU:1, one launch (start us, length us, event | category | flops | bytes accessed | tf_op | source)
XLA Modules:
  0.0 57.3 jit_solution(13588050593206177108)
XLA Ops:
  0.6 54.9 %layer.1 = (bf16[32,256]{1,0:T(8,128)(2,1)S(1)}, f32[16,3,128,128]{3,2,1,0:T(8,128)S(1)}) custom-call(bf16[32,256]{1,0:T(8,128)(2,1)} %bitcast.8, f32[1,256]{1,0:T(1,128)} %bitcast.12, bf16[256,384]{1,0:T(8,128)(2,1)} %wq_ref.1, bf16[256,384]{1,0:T(8,128)(2,1)} %wk_ref.1, bf16[256,384]{1,0:T(8,128)(2,1)} %wv_ref.1, bf16[256,384]{1,0:T(8,128)(2,1)} %wg_ref.1, ...), custom_call_target="tpu_custom_call" | custom-call | tf_op jit(solution)/shard_map/layer/pallas_call | solution.py:909
  55.6 1.7 %store.1 = (bf16[32,256]{1,0:T(8,128)(2,1)}, f32[16,3,128,128]{3,2,1,0:T(8,128)}) custom-call(bf16[32,256]{1,0:T(8,128)(2,1)S(1)} %get-tuple-element.6.mixed_ref, f32[16,3,128,128]{3,2,1,0:T(8,128)S(1)} %get-tuple-element.7.state_ref), custom_call_target="tpu_custom_call" | custom-call | tf_op jit(solution)/shard_map/store/pallas_call | solution.py:939

commit v9 on v8

--- a/solution.py
+++ b/solution.py
@@ -509,35 +509,44 @@
 
     swaps[0].wait_recv()
 
-    def ex_copy(half, dev):
-        blk = recv_ex.at[x, pl.ds(half * rc, rc), :]
-        return remote(blk, blk, ex_send.at[half], ex_recv.at[half], dev)
-
-    def ex_all(half):
-        return recv_ex.at[pl.ds(0, nx - 1), pl.ds(half * rc, rc), :]
-
-    for half in range(2):
-        at = slice(half * rc, (half + 1) * rc)
+    rq = rc // 2
+
+    def ex_rows(order, part):
+        return pl.ds(order * rc + part * rq, rq)
+
+    def ex_start(order, part):
+        blk = recv_ex.at[x, ex_rows(order, part), :]
+        i = 2 * order + part
+        for d in ring(nx):
+            to = {"tp_0": lax.rem(x + d, nx)}
+            remote(blk, blk, ex_send.at[i], ex_recv.at[i], to).start()
+
+    def ex_all(order, part):
+        return recv_ex.at[pl.ds(0, nx - 1), ex_rows(order, part), :]
+
+    for order in range(2):
+        at = slice(order * rc, (order + 1) * rc)
         part = jnp.dot(merged[at, :], w_out[...], preferred_element_type=F32)
         recv_ex[x, at] = part.astype(BF16)
-        for d in ring(nx):
-            ex_copy(half, {"tp_0": lax.rem(x + d, nx)}).start()
-
-    def residual(half):
-        all_received(ex_all(half), ex_send.at[half], ex_recv.at[half])
-        at = slice(half * rc, (half + 1) * rc)
+        ex_start(order, 0)
+    for order in range(2):
+        ex_start(order, 1)
+
+    def residual(order, part):
+        i = 2 * order + part
+        all_received(ex_all(order, part), ex_send.at[i], ex_recv.at[i])
+        at = ex_rows(order, part)
         branch = recv_ex[0, at].astype(F32)
         for i in range(1, nx):
             branch = branch + recv_ex[i, at].astype(F32)
-        tok = col_n[pl.ds(pl.multiple_of(c * rh + half * rc, rc), rc), :]
+        start = c * rh + order * rc + part * rq
+        tok = col_n[pl.ds(pl.multiple_of(start, rq), rq), :]
         res[kv, at] = (tok.astype(F32) + branch).astype(BF16)
 
     rows_a, rows_b = pl.ds(0, rc), pl.ds(rc, rc)
 
     y_arrival, z_arrival = [0, *ring(ny)[::-1]], [0, *ring(nz)[::-1]]
     y_last, z_last = y_arrival[-1], z_arrival[-1]
-
-    rq = rc // 2
 
     def part_of(base, part):
         return pl.ds(base, rc) if part is None else pl.ds(base + part * rq, rq)
@@ -571,16 +580,15 @@
     def z_dev(d):
         return {"kv_0": lax.rem(z + d, nz)}
 
-    residual(0)
     for part in range(2):
+        residual(0, part)
         for d in ring(ny):
             fa_copy(kv, near_a(d, part), y_dev(d), part).start()
+        residual(1, part)
+        for d in ring(nz):
+            fb_copy(kv, near_b(d, part), z_dev(d), part).start()
     for d in ring(nz):
         fa_copy(kv, late_a(0, d), z_dev(d)).start()
-    residual(1)
-    for part in range(2):
-        for d in ring(nz):
-            fb_copy(kv, near_b(d, part), z_dev(d), part).start()
     for d in ring(ny):
         fb_copy(kv, late_b(0, d), y_dev(d)).start()
 
@@ -618,8 +626,8 @@
     def _():
         all_sent(d_bytes(nkv), d_send, d_recv)
 
-    for half in range(2):
-        all_sent(ex_all(half), ex_send.at[half], ex_recv.at[half])
+    for i in range(4):
+        all_sent(ex_all(i // 2, i % 2), ex_send.at[i], ex_recv.at[i])
 
     for part in range(2):
         for i in range(1, max(ny, nz)):
@@ -887,8 +895,8 @@
         dma((4,)),
         dma(()),
         dma(()),
-        dma((2,)),
-        dma((2,)),
+        dma((4,)),
+        dma((4,)),
         dma(()),
         dma(()),
         dma((3 * (ny - 1) + nz,)),

time: 57.4 us -> 56.8 us (0.990)
  no operation moved by 1% of the time
where the time goes in v9:
time: 56.8 us; the launch traced here: 56.7 us
  Pallas kernels  56.1 us (99%)
  between operations  0.64 us (1%)
    pallas_call x1, Pallas kernels, local(): pl.pallas_call(functools.partial(layer_kernel, sizes), out_shape=(pltpu.V...  54.4 us
    pallas_call x1, Pallas kernels, local(): pl.pallas_call(store_kernel, out_shape=(jax.ShapeDtypeStruct((dt, rows),...  1.71 us

profile of v9, /device:TPU:1, one launch (start us, length us, event | category | flops | bytes accessed | tf_op | source)
XLA Modules:
  0.0 56.7 jit_solution(9083529195429458077)
XLA Ops:
  0.6 54.4 %layer.1 = (bf16[32,256]{1,0:T(8,128)(2,1)S(1)}, f32[16,3,128,128]{3,2,1,0:T(8,128)S(1)}) custom-call(bf16[32,256]{1,0:T(8,128)(2,1)} %bitcast.8, f32[1,256]{1,0:T(1,128)} %bitcast.12, bf16[256,384]{1,0:T(8,128)(2,1)} %wq_ref.1, bf16[256,384]{1,0:T(8,128)(2,1)} %wk_ref.1, bf16[256,384]{1,0:T(8,128)(2,1)} %wv_ref.1, bf16[256,384]{1,0:T(8,128)(2,1)} %wg_ref.1, ...), custom_call_target="tpu_custom_call" | custom-call | tf_op jit(solution)/shard_map/layer/pallas_call | solution.py:917
  55.0 1.7 %store.1 = (bf16[32,256]{1,0:T(8,128)(2,1)}, f32[16,3,128,128]{3,2,1,0:T(8,128)}) custom-call(bf16[32,256]{1,0:T(8,128)(2,1)S(1)} %get-tuple-element.6.mixed_ref, f32[16,3,128,128]{3,2,1,0:T(8,128)S(1)} %get-tuple-element.7.state_ref), custom_call_target="tpu_custom_call" | custom-call | tf_op jit(solution)/shard_map/store/pallas_call | solution.py:947

commit v10 on v9

--- a/solution.py
+++ b/solution.py
@@ -163,7 +163,7 @@
     def greet(dev):
         pl.semaphore_signal(barrier, inc=1, device_id=dev, device_id_type=MESH)
 
-    for dx in range(nx):
+    for dx in [*ring(nx), 0]:
         for dc in range(nc):
             if dx or dc:
                 greet({"tp_0": lax.rem(x + dx, nx), "tp_1": lax.rem(c + dc, nc)})
@@ -298,8 +298,6 @@
     for_value = Reduction(2, k_end, proj, True)
     for_gate = Reduction(3, k_end + proj, proj, False)
 
-    send_b[:, q_end:k_end] = project(1)
-    for_key.start()
     contract_last = (((1,), (1,)), ((), ()))
     rates_part = lax.dot_general(
         normed, w_rates[...], contract_last, preferred_element_type=F32
@@ -311,6 +309,8 @@
     send_b[:, proj:q_end] = jnp.where(lane < 64, high, low).astype(BF16)
     send_b[:, :proj] = project(0)
     for_query.start()
+    send_b[:, q_end:k_end] = project(1)
+    for_key.start()
     send_b[:, k_end : k_end + proj] = project(2)
     for_value.start()
     send_b[:, k_end + proj :] = project(3)

time: 56.8 us -> 56.6 us (level)
  no operation moved by 1% of the time
where the time goes in v10:
time: 56.6 us; the launch traced here: 56.4 us
  Pallas kernels  55.8 us (99%)
  between operations  0.64 us (1%)
    pallas_call x1, Pallas kernels, local(): pl.pallas_call(functools.partial(layer_kernel, sizes), out_shape=(pltpu.V...  54.1 us
    pallas_call x1, Pallas kernels, local(): pl.pallas_call(store_kernel, out_shape=(jax.ShapeDtypeStruct((dt, rows),...  1.71 us

profile of v10, /device:TPU:1, one launch (start us, length us, event | category | flops | bytes accessed | tf_op | source)
XLA Modules:
  0.0 56.4 jit_solution(15828150892473434367)
XLA Ops:
  0.6 54.1 %layer.1 = (bf16[32,256]{1,0:T(8,128)(2,1)S(1)}, f32[16,3,128,128]{3,2,1,0:T(8,128)S(1)}) custom-call(bf16[32,256]{1,0:T(8,128)(2,1)} %bitcast.8, f32[1,256]{1,0:T(1,128)} %bitcast.12, bf16[256,384]{1,0:T(8,128)(2,1)} %wq_ref.1, bf16[256,384]{1,0:T(8,128)(2,1)} %wk_ref.1, bf16[256,384]{1,0:T(8,128)(2,1)} %wv_ref.1, bf16[256,384]{1,0:T(8,128)(2,1)} %wg_ref.1, ...), custom_call_target="tpu_custom_call" | custom-call | tf_op jit(solution)/shard_map/layer/pallas_call | solution.py:917
  54.7 1.7 %store.1 = (bf16[32,256]{1,0:T(8,128)(2,1)}, f32[16,3,128,128]{3,2,1,0:T(8,128)}) custom-call(bf16[32,256]{1,0:T(8,128)(2,1)S(1)} %get-tuple-element.6.mixed_ref, f32[16,3,128,128]{3,2,1,0:T(8,128)S(1)} %get-tuple-element.7.state_ref), custom_call_target="tpu_custom_call" | custom-call | tf_op jit(solution)/shard_map/store/pallas_call | solution.py:947

commit v11 on v10

--- a/solution.py
+++ b/solution.py
@@ -587,10 +587,10 @@
         residual(1, part)
         for d in ring(nz):
             fb_copy(kv, near_b(d, part), z_dev(d), part).start()
-    for d in ring(nz):
-        fa_copy(kv, late_a(0, d), z_dev(d)).start()
-    for d in ring(ny):
-        fb_copy(kv, late_b(0, d), y_dev(d)).start()
+        for d in ring(nz):
+            fa_copy(kv, late_a(0, d), z_dev(d), part).start()
+        for d in ring(ny):
+            fb_copy(kv, late_b(0, d), y_dev(d), part).start()
 
     res_t[...] = res[kv].astype(F32).T.astype(BF16)
     r_copy = remote(

time: 56.6 us -> 56.3 us (level)
  no operation moved by 1% of the time
where the time goes in v11:
time: 56.3 us; the launch traced here: 56.1 us
  Pallas kernels  55.5 us (99%)
  between operations  0.64 us (1%)
    pallas_call x1, Pallas kernels, local(): pl.pallas_call(functools.partial(layer_kernel, sizes), out_shape=(pltpu.V...  53.8 us
    pallas_call x1, Pallas kernels, local(): pl.pallas_call(store_kernel, out_shape=(jax.ShapeDtypeStruct((dt, rows),...  1.71 us

profile of v11, /device:TPU:1, one launch (start us, length us, event | category | flops | bytes accessed | tf_op | source)
XLA Modules:
  0.0 56.1 jit_solution(12011496149371864115)
XLA Ops:
  0.6 53.8 %layer.1 = (bf16[32,256]{1,0:T(8,128)(2,1)S(1)}, f32[16,3,128,128]{3,2,1,0:T(8,128)S(1)}) custom-call(bf16[32,256]{1,0:T(8,128)(2,1)} %bitcast.8, f32[1,256]{1,0:T(1,128)} %bitcast.12, bf16[256,384]{1,0:T(8,128)(2,1)} %wq_ref.1, bf16[256,384]{1,0:T(8,128)(2,1)} %wk_ref.1, bf16[256,384]{1,0:T(8,128)(2,1)} %wv_ref.1, bf16[256,384]{1,0:T(8,128)(2,1)} %wg_ref.1, ...), custom_call_target="tpu_custom_call" | custom-call | tf_op jit(solution)/shard_map/layer/pallas_call | solution.py:917
  54.4 1.7 %store.1 = (bf16[32,256]{1,0:T(8,128)(2,1)}, f32[16,3,128,128]{3,2,1,0:T(8,128)}) custom-call(bf16[32,256]{1,0:T(8,128)(2,1)S(1)} %get-tuple-element.6.mixed_ref, f32[16,3,128,128]{3,2,1,0:T(8,128)S(1)} %get-tuple-element.7.state_ref), custom_call_target="tpu_custom_call" | custom-call | tf_op jit(solution)/shard_map/store/pallas_call | solution.py:947
